TPU v7x, 512 devices: a whole 4x4x16 slice. The times are simulated.
512 devices in a mesh: sp: 64 (over z, y), tp: 8 (over x, core).
Axes of the slice: x: 4, y: 4, z: 16, core: 2. Of those that a mesh axis runs over, the one named last changes fastest.
Arguments:
- residual: bfloat16 [8192, 2048], P(('sp', 'tp')), may hold values from -24 to 24
- query_small: bfloat16 [8192, 768], P('sp', 'tp'), may hold values from -64 to 64
- query_large: bfloat16 [8192, 1280], P('sp', 'tp'), may hold values from -64 to 64
- latent: bfloat16 [8192, 256], P('sp'), may hold values from -6 to 6
- rope_key: bfloat16 [8192, 32], P('sp'), may hold values from -48 to 48
- key_up_small: bfloat16 [256, 512], P(None, 'tp'), may hold values from -0.375 to 0.375
- value_up_small: bfloat16 [256, 512], P(None, 'tp'), may hold values from -0.375 to 0.375
- key_up_large: bfloat16 [256, 1024], P(None, 'tp'), may hold values from -0.375 to 0.375
- value_up_large: bfloat16 [256, 1024], P(None, 'tp'), may hold values from -0.375 to 0.375
- out_small: bfloat16 [512, 2048], P('tp'), may hold values from -0.625 to 0.625
- out_large: bfloat16 [1024, 2048], P('tp'), may hold values from -0.625 to 0.625
- norm_gain: bfloat16 [2048], replicated, may hold values from 0.099609375 to 1.8984375
- gate_weight: bfloat16 [2048, 5632], P('sp', 'tp'), may hold values from -0.125 to 0.125
- up_weight: bfloat16 [2048, 5632], P('sp', 'tp'), may hold values from -0.125 to 0.125
- down_weight: bfloat16 [2048, 5632], P('sp', 'tp'), may hold values from -0.21875 to 0.21875
Outputs:
- layer_out: bfloat16 [8192, 2048], P(('sp', 'tp'))
All inputs are finite; a program needn't handle non-finite values.
Results may differ from a plain program's by a relative error of at most 0.017.
Values may be sent and summed in bfloat16 or wider, within the bound.
No kernel may reach another device: no remote copies, remote signals or barrier semaphores. Data moves between devices by JAX's collectives and lax.ppermute only.
A program may use at most 64 MiB of HBM per device.

v0:
```python
import jax
import jax.numpy as jnp
from jax import lax
from jax.sharding import PartitionSpec as P

HEAD_SMALL = 64
HEAD_LARGE = 128
ROPE = 32


big_negative = -1e30
rope_base = 500000.0
norm_eps = 1e-06


def cut_along(shard, dim, count):
    before, after = (shard.shape[:dim], shard.shape[dim + 1 :])
    return jnp.moveaxis(shard.reshape(*before, count, -1, *after), dim, 0)


def sent_and_summed(shard, axis, dim):
    count = lax.axis_size(axis)
    tiles = lax.all_to_all(cut_along(shard, dim, count), axis, 0, 0, tiled=True)
    return jnp.sum(tiles.astype(jnp.float32), axis=0)


def sent_together(arrays, axis, dim, along):
    widths = [a.shape[along] for a in arrays]
    both = jnp.concatenate(arrays, axis=along)
    whole = lax.all_gather(both, axis, axis=dim, tiled=True)
    return tuple(jnp.split(whole, [sum(widths[:k]) for k in range(1, len(widths))], axis=along))


def laid_out(tiles, dim):
    lengths = list(tiles.shape[1:])
    lengths[dim] *= tiles.shape[0]
    return jnp.moveaxis(tiles, 0, dim).reshape(lengths)


def from_everyone(shard, axis):
    copies = jnp.broadcast_to(shard, (lax.axis_size(axis), *shard.shape))
    return lax.all_to_all(copies, axis, split_axis=0, concat_axis=0, tiled=True)


def collect(shard, axis, dim):
    return laid_out(from_everyone(shard, axis), dim)


def rotate(vectors, positions):
    span_width = vectors.shape[-1]
    half_width = span_width // 2
    inverse = 1.0 / rope_base ** (jnp.arange(0, span_width, 2, dtype=jnp.float32) / span_width)
    angles = positions.astype(jnp.float32)[:, None] * inverse[None, :]
    angle_shape = (vectors.shape[0],) + (1,) * (vectors.ndim - 2) + (half_width,)
    cosine = jnp.cos(angles).reshape(angle_shape)
    sine_table = jnp.sin(angles).reshape(angle_shape)
    leading = vectors[..., :half_width].astype(jnp.float32)
    trailing = vectors[..., half_width:].astype(jnp.float32)
    turned = jnp.concatenate(
        [leading * cosine - trailing * sine_table, trailing * cosine + leading * sine_table],
        axis=-1,
    )
    return turned.astype(jnp.bfloat16)


def group_update(
    running, nope_part, turned_query, key_rows, value_rows, turned_key, visible, head_size
):
    maxima, totals, summed = running
    head_count = nope_part.shape[0]
    key_count = key_rows.shape[0]
    key_rows = key_rows.reshape(key_count, head_count, head_size)
    value_rows = value_rows.reshape(key_count, head_count, head_size)
    scores = jnp.einsum("hqe,khe->hqk", nope_part, key_rows, preferred_element_type=jnp.float32)
    scores = scores + jnp.einsum(
        "hqr,kr->hqk", turned_query, turned_key, preferred_element_type=jnp.float32
    )
    scores = scores * (head_size + ROPE) ** (-0.5)
    masked = jnp.where(visible[None, :, :], scores, big_negative)
    new_maxima = jnp.maximum(maxima, jnp.max(masked, axis=2))
    weights = jnp.where(visible[None, :, :], jnp.exp(masked - new_maxima[:, :, None]), 0.0)
    totals = jnp.sum(weights, axis=2)
    summed = jnp.einsum(
        "hqk,khe->hqe", weights.astype(jnp.bfloat16), value_rows, preferred_element_type=jnp.float32
    )
    return (new_maxima, totals, summed)


def finish(running):
    maxima, totals, summed = running
    head_count, row_count, head_size = summed.shape
    result = summed / totals[:, :, None]
    return (
        jnp.transpose(result, (1, 0, 2))
        .reshape(row_count, head_count * head_size)
        .astype(jnp.bfloat16)
    )


def shards(
    residual,
    query_small,
    query_large,
    latent,
    rope_key,
    key_up_small,
    value_up_small,
    key_up_large,
    value_up_large,
    out_small,
    out_large,
    norm_gain,
    gate_weight,
    up_weight,
    down_weight,
):
    row_count = query_small.shape[0]
    first_row = lax.axis_index("sp") * row_count
    query_pos = first_row + jnp.arange(row_count, dtype=jnp.int32)
    heads_small = key_up_small.shape[1] // HEAD_SMALL
    heads_large = key_up_large.shape[1] // HEAD_LARGE

    def split_query(query, head_count, head_size):
        shaped = query.reshape(row_count, head_count, head_size + ROPE)
        nope_part = jnp.transpose(shaped[..., :head_size], (1, 0, 2))
        turned = jnp.transpose(rotate(shaped[..., head_size:], query_pos), (1, 0, 2))
        return (nope_part, turned)

    nope_small, turned_small = split_query(query_small, heads_small, HEAD_SMALL)
    nope_large, turned_large = split_query(query_large, heads_large, HEAD_LARGE)

    def initial(head_count, head_size):
        return (
            jnp.full((head_count, row_count), big_negative, jnp.float32),
            jnp.zeros((head_count, row_count), jnp.float32),
            jnp.zeros((head_count, row_count, head_size), jnp.float32),
        )

    starting = (initial(heads_small, HEAD_SMALL), initial(heads_large, HEAD_LARGE))
    part_latent = lax.all_gather(latent, "sp", axis=0, tiled=True)
    part_rope = lax.all_gather(rope_key, "sp", axis=0, tiled=True)
    key_count = part_latent.shape[0]
    key_pos = jnp.arange(key_count, dtype=jnp.int32)

    def compute(running):
        turned_key = rotate(part_rope, key_pos)
        visible = key_pos[None, :] <= query_pos[:, None]
        key_small = jnp.dot(part_latent, key_up_small, preferred_element_type=jnp.float32).astype(
            jnp.bfloat16
        )
        value_small = jnp.dot(
            part_latent, value_up_small, preferred_element_type=jnp.float32
        ).astype(jnp.bfloat16)
        key_large = jnp.dot(part_latent, key_up_large, preferred_element_type=jnp.float32).astype(
            jnp.bfloat16
        )
        value_large = jnp.dot(
            part_latent, value_up_large, preferred_element_type=jnp.float32
        ).astype(jnp.bfloat16)
        small_state = group_update(
            running[0],
            nope_small,
            turned_small,
            key_small,
            value_small,
            turned_key,
            visible,
            HEAD_SMALL,
        )
        large_state = group_update(
            running[1],
            nope_large,
            turned_large,
            key_large,
            value_large,
            turned_key,
            visible,
            HEAD_LARGE,
        )
        return (small_state, large_state)

    def keep(running):
        return running

    running = lax.cond(jnp.int32(0) <= query_pos[-1], compute, keep, starting)
    attended_small = finish(running[0])
    attended_large = finish(running[1])
    mixed = sent_and_summed(
        (
            jnp.dot(attended_small, out_small, preferred_element_type=jnp.float32)
            + jnp.dot(attended_large, out_large, preferred_element_type=jnp.float32)
        ).astype(jnp.bfloat16),
        "tp",
        0,
    ).astype(jnp.bfloat16)
    stream = (residual.astype(jnp.float32) + mixed.astype(jnp.float32)).astype(jnp.bfloat16)
    as_float = stream.astype(jnp.float32)
    normed = as_float * lax.rsqrt(jnp.mean(as_float * as_float, axis=-1, keepdims=True) + norm_eps)
    normed = (normed * norm_gain.astype(jnp.float32)[None, :]).astype(jnp.bfloat16)
    gate_full, up_full, down_full = sent_together((gate_weight, up_weight, down_weight), "sp", 0, 1)
    piece = collect(normed, "tp", 0)
    gate_part = jnp.dot(piece, gate_full, preferred_element_type=jnp.float32)
    up_part = jnp.dot(piece, up_full, preferred_element_type=jnp.float32)
    hidden = (jax.nn.silu(gate_part) * up_part).astype(jnp.bfloat16)
    channel = sent_and_summed(
        lax.dot_general(
            hidden, down_full, (((1,), (1,)), ((), ())), preferred_element_type=jnp.float32
        ).astype(jnp.bfloat16),
        "tp",
        0,
    ).astype(jnp.bfloat16)
    return (as_float + 0.5 * channel.astype(jnp.float32)).astype(jnp.bfloat16)


def solution(mesh):
    placed = (
        P(("sp", "tp"), None),
        P("sp", "tp"),
        P("sp", "tp"),
        P("sp", None),
        P("sp", None),
        P(None, "tp"),
        P(None, "tp"),
        P(None, "tp"),
        P(None, "tp"),
        P("tp", None),
        P("tp", None),
        P(),
        P("sp", "tp"),
        P("sp", "tp"),
        P("sp", "tp"),
    )
    return jax.shard_map(
        shards, mesh=mesh, in_specs=placed, out_specs=P(("sp", "tp"), None), check_vma=False
    )
```

profile of v0, /device:TPU:1, one launch (start us, length us, event | category | flops | bytes accessed | tf_op | source)
XLA Modules:
  0.0 348.7 jit_solution(13543055869742643674)
XLA Ops:
  6.5 0.7 all-gather.3.cloned.1.call-update
  7.3 1.6 concatenate.47
  8.9 0.6 slice.35
  10.2 0.9 fusion.87
  11.1 86.3 %all_gather.10 = bf16[8192,32]{0,1:T(8,128)(2,1)S(1)} all-gather(bf16[128,32]{0,1:T(8,128)(2,1)} %param.21), channel_id=1, replica_groups=mesh['sp'=64,'tp'=8] {'sp'}, dimensions={0}, use_global_device_ids=true | all-gather | bytes 532480 | tf_op jit(solution)/shard_map/all_gather | solution.py:141
  97.3 54.7 %all-gather.3.cloned.1.call-done = bf16[8192,256]{1,0:T(8,128)(2,1)} async-done(((bf16[128,256]{1,0:T(8,128)(2,1)}), bf16[8192,256]{1,0:T(8,128)(2,1)}) %all-gather.3.cloned.1.call-update) | async-done | bytes 4194320 | tf_op jit(solution)/shard_map/all_gather | solution.py:140
  152.0 49.8 %conditional.1 = (f32[1,128]{1,0:T(1,128)S(1)}, f32[1,128,64]{1,2,0:T(8,128)S(1)}, f32[1,128]{1,0:T(1,128)S(1)}, f32[1,128,128]{2,1,0:T(8,128)S(1)}) conditional(s32[]{:T(128)} %bitcast.10, () %tuple.13, (s32[8192]{0:T(1024)S(1)}, s32[128]{0:T(128)S(1)}, bf16[8192,256]{1,0:T(8,128)(2,1)}, bf16[256,64]{0,1:T(8,128)(2,1)}, ...), branch_computations={%region_0.0_spmd, %region_1.6_spmd} | conditional | flops 2583461632 | bytes 62645008 | solution.py:185
  152.0 6.2 %fusion.20 = f32[8192,128]{1,0:T(8,128)} fusion(bf16[8192,256]{1,0:T(8,128)(2,1)} %get-tuple-element.39, bf16[256,64]{0,1:T(8,128)(2,1)} %get-tuple-element.104, bf16[128,1,96]{0,2,1:T(8,128)(2,1)} %get-tuple-element.41), kind=kOutput, calls=%fused_computation.26 | convolution fusion | flops 403177472 | bytes 8437760 | tf_op jit(solution)/shard_map/cond/branch_1_fun/hqe,khe->hqk/dot_general | solution.py:74
  158.3 7.2 %fusion.28 = (bf16[8192,16]{0,1:T(8,128)(2,1)S(1)}, bf16[8192,16]{0,1:T(8,128)(2,1)S(1)}) fusion(f32[8192]{0:T(1024)S(1)} %convert_element_type.101, f32[16]{0:T(128)S(1)} %negate_power_fusion, f32[8192]{0:T(1024)S(1)} %convert_element_type.99, bf16[8192,32]{0,1:T(8,128)(2,1)S(1)} %get-tuple-element.42, f32[8192]{0:T(1024)S(1)} %convert_element_type.103, ...), kind=kLoop, calls=%fused_computation.34 | loop fusion | flops 1835008 | bytes 1179712 | tf_op jit(solution)/shard_map/convert.2
  165.5 5.8 %fusion.93 = (f32[128]{0:T(128)S(1)}, f32[128,8192]{0,1:T(8,128)}) fusion(f32[8192,128]{1,0:T(8,128)} %fusion.20, bf16[1,128,32]{1,2,0:T(8,128)(2,1)S(1)} %get-tuple-element.111, bf16[8192,16]{0,1:T(8,128)(2,1)S(1)} %get-tuple-element.120, bf16[8192,16]{0,1:T(8,128)(2,1)S(1)} %get-tuple-element.119, s32[128]{0:T(128)S(1)} %get-tuple-element.38, ...), kind=kOutput, calls=%fused_computation.110 | convolution fusion | flops 73400192 | bytes 8954880 | tf_op jit(solution)/shard_map/cond/branch_1_fun/hqr,kr->hqk/dot_general | solution.py:75
  171.4 6.3 %fusion.19 = f32[8192,128]{1,0:T(8,128)} fusion(bf16[8192,256]{1,0:T(8,128)(2,1)} %get-tuple-element.39, bf16[256,128]{1,0:T(8,128)(2,1)S(1)} %copy-done.3, bf16[128,1,160]{2,0,1:T(8,128)(2,1)S(1)} %copy.38), kind=kOutput, calls=%fused_computation.25 | convolution fusion | flops 806354944 | bytes 8486912 | tf_op jit(solution)/shard_map/cond/branch_1_fun/hqe,khe->hqk/dot_general | solution.py:74
  177.7 5.8 %fusion.92 = (f32[128]{0:T(128)S(1)}, f32[128,8192]{0,1:T(8,128)}) fusion(f32[8192,128]{1,0:T(8,128)} %fusion.19, bf16[1,128,32]{1,2,0:T(8,128)(2,1)S(1)} %get-tuple-element.115, bf16[8192,16]{0,1:T(8,128)(2,1)S(1)} %get-tuple-element.120, bf16[8192,16]{0,1:T(8,128)(2,1)S(1)} %get-tuple-element.119, s32[128]{0:T(128)S(1)} %get-tuple-element.38, ...), kind=kOutput, calls=%fused_computation.109 | convolution fusion | flops 73400192 | bytes 8954880 | tf_op jit(solution)/shard_map/cond/branch_1_fun/hqr,kr->hqk/dot_general | solution.py:75
  183.5 6.0 %fusion.21 = f32[1,128,128]{2,1,0:T(8,128)S(1)} fusion(bf16[8192,256]{1,0:T(8,128)(2,1)} %get-tuple-element.39, bf16[256,128]{1,0:T(8,128)(2,1)S(1)} %copy-done.6, f32[128,8192]{0,1:T(8,128)} %get-tuple-element.122, f32[128]{0:T(128)S(1)} %get-tuple-element.125, s32[128]{0:T(128)S(1)} %get-tuple-element.38, s32[8192]{0:T(1024)S(1)} %get-tuple-element.46), kind=kOutput, calls=%fused_computation.27 | convolution fusion | flops 810549248 | bytes 8553472 | tf_op jit(solution)/shard_map/cond/branch_1_fun/hqk,khe->hqe/dot_general | solution.py:83
  189.5 5.7 %fusion.24 = f32[1,128,64]{1,2,0:T(8,128)S(1)} fusion(f32[128,8192]{0,1:T(8,128)} %get-tuple-element.124, f32[128]{0:T(128)S(1)} %get-tuple-element.126, s32[128]{0:T(128)S(1)} %get-tuple-element.38, s32[8192]{0:T(1024)S(1)} %get-tuple-element.46, bf16[8192,256]{1,0:T(8,128)(2,1)} %get-tuple-element.39, bf16[256,64]{0,1:T(8,128)(2,1)S(1)} %copy-done.7), kind=kOutput, calls=%fused_computation.28 | convolution fusion | flops 407371776 | bytes 8487936 | tf_op jit(solution)/shard_map/cond/branch_1_fun/hqk,khe->hqe/dot_general | solution.py:83
  195.2 6.6 %fusion.9 = (f32[128]{0:T(128)S(1)}, f32[128]{0:T(128)S(1)}) fusion(f32[128,8192]{0,1:T(8,128)} %get-tuple-element.122, f32[128]{0:T(128)S(1)} %get-tuple-element.125, s32[128]{0:T(128)S(1)} %get-tuple-element.38, s32[8192]{0:T(1024)S(1)} %get-tuple-element.46, f32[128,8192]{0,1:T(8,128)} %get-tuple-element.124, f32[128]{0:T(128)S(1)} %get-tuple-element.126), kind=kLoop, calls=%fused_computation.17 | loop fusion | flops 7339776 | bytes 8423936 | tf_op jit(solution)/shard_map/cond/branch_1_fun/reduce_sum | solution.py:82
  202.2 1.2 fusion.45
  203.3 14.8 %all-to-all-start = ((bf16[8,16,2048]{2,1,0:T(8,128)(2,1)}), bf16[8,16,2048]{2,1,0:T(8,128)(2,1)S(1)}, u32[]{:S(2)}, u32[]{:S(2)}) async-start(bf16[8,16,2048]{2,1,0:T(8,128)(2,1)} %bitcast.21), calls=%async_computation | async-start | bytes 1048576 | tf_op jit(solution)/shard_map/all_to_all | solution.py:23
  218.1 9.3 %all-to-all-done = bf16[8,16,2048]{2,1,0:T(8,128)(2,1)S(1)} async-done(((bf16[8,16,2048]{2,1,0:T(8,128)(2,1)}), bf16[8,16,2048]{2,1,0:T(8,128)(2,1)S(1)}, u32[]{:S(2)}, u32[]{:S(2)}) %all-to-all-start) | async-done | bytes 524320 | tf_op jit(solution)/shard_map/all_to_all | solution.py:23
  227.8 12.9 %all_to_all.15 = bf16[8,16,2048]{2,1,0:T(8,128)(2,1)S(1)} all-to-all(bf16[8,16,2048]{2,1,0:T(8,128)(2,1)S(1)} %broadcast_in_dim.17), channel_id=1, replica_groups=mesh['sp'=64,'tp'=8] {'tp'}, dimensions={0} | all-to-all | bytes 1048576 | tf_op jit(solution)/shard_map/all_to_all | solution.py:42
  240.7 68.3 %all-gather.5.cloned.1.call-done = bf16[2048,2112]{1,0:T(8,128)(2,1)} async-done(((bf16[32,2112]{1,0:T(8,128)(2,1)}), bf16[2048,2112]{1,0:T(8,128)(2,1)}) %all-gather.5.cloned.1.call-update) | async-done | bytes 8650768 | tf_op jit(solution)/shard_map/all_gather | solution.py:30
  309.0 3.2 fusion.43
  312.2 7.2 %fusion.46 = bf16[128,2048]{1,0:T(8,128)(2,1)S(1)} fusion(bf16[2048,2112]{1,0:T(8,128)(2,1)} %all-gather.5.cloned.1.call-done, bf16[128,2048]{1,0:T(8,128)(2,1)S(1)} %bitcast.67, f32[128,704]{0,1:T(8,128)S(1)} %fusion.43), kind=kOutput, calls=%fused_computation.58 | convolution fusion | flops 739000320 | bytes 7700480 | tf_op jit(solution)/shard_map/dot_general | solution.py:206
  319.5 21.6 %all_to_all.16 = bf16[8,16,2048]{2,1,0:T(8,128)(2,1)S(1)} all-to-all(bf16[8,16,2048]{2,1,0:T(8,128)(2,1)S(1)} %bitcast.68), channel_id=1, replica_groups=mesh['sp'=64,'tp'=8] {'tp'}, dimensions={0} | all-to-all | bytes 1048576 | tf_op jit(solution)/shard_map/all_to_all | solution.py:23
  341.2 0.7 fusion.66
  (39 shorter events, 1.0 us)
Async XLA Ops:
  6.5 195.6 %copy-start = (bf16[128,2048]{1,0:T(8,128)(2,1)S(1)}, bf16[128,2048]{1,0:T(8,128)(2,1)}, u32[]{:S(2)}) copy-start(bf16[128,2048]{1,0:T(8,128)(2,1)} %param.27) | copy-start | bytes 1572868
  6.5 145.5 %all-gather.3.cloned.1.call-start = ((), (), s32[]{:S(2)}) async-start(), calls=%async_computation.3 | async-start | bytes 4259840 | tf_op jit(solution)/shard_map/all_gather | solution.py:140
  7.3 301.8 %all-gather.5.cloned.1.call-start = ((), (), s32[]{:S(2)}) async-start(), calls=%async_computation.4 | async-start | bytes 9052160 | tf_op jit(solution)/shard_map/all_gather | solution.py:30
  152.0 49.8 %copy-start.2 = (bf16[64,2048]{1,0:T(8,128)(2,1)S(1)}, bf16[64,2048]{1,0:T(8,128)(2,1)}, u32[]{:S(2)}) copy-start(bf16[64,2048]{1,0:T(8,128)(2,1)} %param.26) | copy-start | bytes 786436
  165.4 5.8 %copy-start.4 = (bf16[128,1,160]{0,2,1:T(8,128)(2,1)S(1)}, bf16[128,1,160]{0,2,1:T(8,128)(2,1)}, u32[]{:S(2)}) copy-start(bf16[128,1,160]{0,2,1:T(8,128)(2,1)} %get-tuple-element.114) | copy-start | bytes 122884 | tf_op jit(solution)/shard_map/cond
  165.5 5.9 %copy-start.3 = (bf16[256,128]{1,0:T(8,128)(2,1)S(1)}, bf16[256,128]{1,0:T(8,128)(2,1)}, u32[]{:S(2)}) copy-start(bf16[256,128]{1,0:T(8,128)(2,1)} %get-tuple-element.67) | copy-start | bytes 196612 | tf_op jit(solution)/shard_map/cond
  177.7 5.8 %copy-start.6 = (bf16[256,128]{1,0:T(8,128)(2,1)S(1)}, bf16[256,128]{1,0:T(8,128)(2,1)}, u32[]{:S(2)}) copy-start(bf16[256,128]{1,0:T(8,128)(2,1)} %get-tuple-element.68) | copy-start | bytes 196612 | tf_op jit(solution)/shard_map/cond
  183.5 6.0 %copy-start.7 = (bf16[256,64]{0,1:T(8,128)(2,1)S(1)}, bf16[256,64]{0,1:T(8,128)(2,1)}, u32[]{:S(2)}) copy-start(bf16[256,64]{0,1:T(8,128)(2,1)} %get-tuple-element.112) | copy-start | bytes 98308 | tf_op jit(solution)/shard_map/cond
  201.8 16.3 %copy-start.5 = (bf16[2048]{0:T(1024)(128)(2,1)S(1)}, bf16[2048]{0:T(1024)(128)(2,1)}, u32[]{:S(2)}) copy-start(bf16[2048]{0:T(1024)(128)(2,1)} %param.28) | copy-start | bytes 12292
  201.8 25.7 %copy-start.1 = (bf16[16,2048]{1,0:T(8,128)(2,1)S(1)}, bf16[16,2048]{1,0:T(8,128)(2,1)}, u32[]{:S(2)}) copy-start(bf16[16,2048]{1,0:T(8,128)(2,1)} %param.17) | copy-start | bytes 196612
  203.3 24.1 %all-to-all-start = ((bf16[8,16,2048]{2,1,0:T(8,128)(2,1)}), bf16[8,16,2048]{2,1,0:T(8,128)(2,1)S(1)}, u32[]{:S(2)}, u32[]{:S(2)}) async-start(bf16[8,16,2048]{2,1,0:T(8,128)(2,1)} %bitcast.21), calls=%async_computation | async-start | bytes 1048576 | tf_op jit(solution)/shard_map/all_to_all | solution.py:23
Sparse Core Ops, SparseCore 0:
  10.3 141.7 all-gather.2
  155.0 154.0 all-gather.4
where the time goes:
time: 349 us
  waiting for transfers between devices  133 us (38%)
  blocking collectives  121 us (35%)
  matrix products  47.6 us (14%)
  other arithmetic  15.8 us (5%)
  starting transfers between devices  14.8 us (4%)
  between operations  14.2 us (4%)
    all_gather x1, blocking collectives, shards(): part_rope = lax.all_gather(rope_key, 'sp', axis=0, tiled=True)  86.3 us
    all_gather x1, waiting for transfers between devices, sent_together(): whole = lax.all_gather(both, axis, axis=dim, tiled=True)  68.3 us
    all_gather x1, waiting for transfers between devices, shards(): part_latent = lax.all_gather(latent, 'sp', axis=0, tiled=True)  54.7 us
    all_to_all x1, blocking collectives, sent_and_summed(): tiles = lax.all_to_all(cut_along(shard, dim, count), axis, 0, 0, tiled=True)  21.6 us
    all_to_all x1, starting transfers between devices, sent_and_summed(): tiles = lax.all_to_all(cut_along(shard, dim, count), axis, 0, 0, tiled=True)  14.8 us
    all_to_all x1, blocking collectives, from_everyone(): return lax.all_to_all(copies, axis, split_axis=0, concat_axis=0, tiled=True)  12.9 us
    dot_general x2, matrix products, group_update(): jnp.einsum('hqe,khe->hqk', nope_part, key_rows, preferred_element_type=jn...  12.5 us
    dot_general x2, matrix products, group_update(): jnp.einsum('hqk,khe->hqe', weights.astype(jnp.bfloat16), value_rows, pref...  11.7 us
  transfers between devices with their start and end apart: 3, of which 3 were waited for; matrix products, arithmetic and copies ran while one was open for 16% of the time, Pallas kernels for 0%

commit v1 on v0

v1 whole, which is shorter than its diff:
```python
import jax
import jax.numpy as jnp
from jax import lax
from jax.experimental import pallas as pl
from jax.experimental.pallas import tpu as pltpu
from jax.sharding import Mesh
from jax.sharding import PartitionSpec as P

HEAD_SMALL = 64
HEAD_LARGE = 128
ROPE = 32
SCALE_SMALL = (HEAD_SMALL + ROPE) ** (-0.5)
SCALE_LARGE = (HEAD_LARGE + ROPE) ** (-0.5)

big_negative = -1e30
rope_base = 500000.0
norm_eps = 1e-06

NT = (((1,), (1,)), ((), ()))


def rotate(vectors, positions):
    span_width = vectors.shape[-1]
    half_width = span_width // 2
    inverse = 1.0 / rope_base ** (jnp.arange(0, span_width, 2, dtype=jnp.float32) / span_width)
    angles = positions.astype(jnp.float32)[:, None] * inverse[None, :]
    cosine = jnp.cos(angles)
    sine = jnp.sin(angles)
    leading = vectors[..., :half_width].astype(jnp.float32)
    trailing = vectors[..., half_width:].astype(jnp.float32)
    turned = jnp.concatenate(
        [leading * cosine - trailing * sine, trailing * cosine + leading * sine], axis=-1
    )
    return turned.astype(jnp.bfloat16)


def from_everyone(shard, axis):
    copies = jnp.broadcast_to(shard, (lax.axis_size(axis), *shard.shape))
    return lax.all_to_all(copies, axis, split_axis=0, concat_axis=0, tiled=True)


def exchanged(chunks, axis):
    return lax.all_to_all(chunks, axis, split_axis=0, concat_axis=0, tiled=True)


def partner(x):
    return lax.ppermute(x, "c", [(0, 1), (1, 0)])


def three_parts(v):
    high = v.astype(jnp.bfloat16).astype(jnp.float32)
    rest = v - high
    middle = rest.astype(jnp.bfloat16).astype(jnp.float32)
    low = (rest - middle).astype(jnp.bfloat16).astype(jnp.float32)
    return [high, middle, low]


def attention_kernel(
    place, query, mine, other, key_up_s, key_up_l, value_up_s, value_up_l, out, keys, turned
):
    z = place[0]
    y = place[1]
    c = place[2]
    n_x, n_z = mine.shape[0], mine.shape[1]
    for x in range(n_x):
        for k in range(n_z):
            lanes = pl.ds(128 * k, 128)
            here = pl.multiple_of(64 * x + 32 * c, 32)
            there = pl.multiple_of(64 * x + 32 * (1 - c), 32)
            keys[pl.ds(here, 32), lanes] = mine[x, k, 0:32, :]
            keys[pl.ds(there, 32), lanes] = other[x, k, 0:32, :]
    for k in range(n_z):
        rows = [mine[x, k, 32:40, :].astype(jnp.float32) for x in range(n_x)]
        turned[:, pl.ds(128 * k, 128)] = jnp.concatenate(rows, axis=0).astype(jnp.bfloat16)
    n_keys = 128 * n_z
    n_y = query.shape[0] // 128
    column = lax.broadcasted_iota(jnp.int32, (1, n_keys), 1)
    key_pos = (column // 128) * (128 * n_y) + y * 128 + column % 128
    key_up_small = key_up_s[...]
    key_up_large = key_up_l[...]
    value_up_small = value_up_s[...]
    value_up_large = value_up_l[...]
    lane = lax.broadcasted_iota(jnp.int32, (128, 64), 1)

    def head(nope, rope, key_up, value_up, scale, visible):
        wide = lax.dot_general(nope, key_up, NT, preferred_element_type=jnp.float32)
        score = jnp.dot(
            wide.astype(jnp.bfloat16), keys[...], preferred_element_type=jnp.float32
        ) + jnp.dot(rope, turned[...], preferred_element_type=jnp.float32)
        score = jnp.where(visible, score * scale, big_negative)
        top = jnp.max(score, axis=1, keepdims=True)
        weight = jnp.exp(score - top)
        total = jnp.sum(weight, axis=1, keepdims=True)
        summed = lax.dot_general(
            weight.astype(jnp.bfloat16), keys[...], NT, preferred_element_type=jnp.float32
        )
        summed = (summed / total).astype(jnp.bfloat16)
        value = jnp.dot(summed, value_up, preferred_element_type=jnp.float32)
        return value, top, total

    for j in range(n_y):
        rows = pl.ds(128 * j, 128)
        row = lax.broadcasted_iota(jnp.int32, (128, 1), 0)
        visible = key_pos <= z * (128 * n_y) + j * 128 + row
        q = query[rows, :]
        value_l, top_l, total_l = head(
            q[:, 0:128], q[:, 224:256], key_up_large, value_up_large, SCALE_LARGE, visible
        )
        value_s, top_s, total_s = head(
            q[:, 128:192], q[:, 192:224], key_up_small, value_up_small, SCALE_SMALL, visible
        )
        stats = jnp.zeros((128, 64), jnp.float32)
        parts = three_parts(top_l) + three_parts(total_l) + three_parts(top_s) + three_parts(total_s)
        for i, part in enumerate(parts):
            stats = jnp.where(lane == i, part, stats)
        out[rows, 0:128] = value_l.astype(jnp.bfloat16)
        out[rows, 128:256] = jnp.concatenate([value_s, stats], axis=1).astype(jnp.bfloat16)


def attention(place, query, mine, other, key_up_s, key_up_l, value_up_s, value_up_l):
    n_keys = 128 * mine.shape[1]
    vmem = pl.BlockSpec(memory_space=pltpu.VMEM)
    return pl.pallas_call(
        attention_kernel,
        out_shape=jax.ShapeDtypeStruct(query.shape, jnp.bfloat16),
        in_specs=[pl.BlockSpec(memory_space=pltpu.SMEM)] + [vmem] * 7,
        out_specs=vmem,
        scratch_shapes=[
            pltpu.VMEM((256, n_keys), jnp.bfloat16),
            pltpu.VMEM((ROPE, n_keys), jnp.bfloat16),
        ],
        compiler_params=pltpu.CompilerParams(vmem_limit_bytes=56 * 1024 * 1024),
        name="attend",
    )(place, query, mine, other, key_up_s, key_up_l, value_up_s, value_up_l)


def merge_kernel(parts, out_s, out_l, out):
    n = parts.shape[0]

    def merged(first, width, stat):
        def stat_of(i, k):
            at = 192 + stat + 3 * k
            return (
                parts[i, :, at : at + 1].astype(jnp.float32)
                + parts[i, :, at + 1 : at + 2].astype(jnp.float32)
            ) + parts[i, :, at + 2 : at + 3].astype(jnp.float32)

        tops = [stat_of(i, 0) for i in range(n)]
        top = tops[0]
        for t in tops[1:]:
            top = jnp.maximum(top, t)
        shares = [stat_of(i, 1) * jnp.exp(tops[i] - top) for i in range(n)]
        total = sum(shares[1:], shares[0])
        acc = 0.0
        for i in range(n):
            acc = acc + parts[i, :, first : first + width].astype(jnp.float32) * (shares[i] / total)
        return acc.astype(jnp.bfloat16)

    large = merged(0, 128, 0)
    small = merged(128, 64, 6)
    mixed = jnp.dot(small, out_s[...], preferred_element_type=jnp.float32) + jnp.dot(
        large, out_l[...], preferred_element_type=jnp.float32
    )
    out[...] = mixed.astype(jnp.bfloat16)


def merge(parts, out_s, out_l):
    vmem = pl.BlockSpec(memory_space=pltpu.VMEM)
    return pl.pallas_call(
        merge_kernel,
        out_shape=jax.ShapeDtypeStruct((parts.shape[1], out_s.shape[1]), jnp.bfloat16),
        in_specs=[vmem] * 3,
        out_specs=vmem,
        name="merge",
    )(parts, out_s, out_l)


def shards(
    residual,
    query_small,
    query_large,
    latent,
    rope_key,
    key_up_small,
    value_up_small,
    key_up_large,
    value_up_large,
    out_small,
    out_large,
    norm_gain,
    gate_weight,
    up_weight,
    down_weight,
):
    n_y = lax.axis_size("y")
    n_x = lax.axis_size("x")
    z = lax.axis_index("z")
    y = lax.axis_index("y")
    x = lax.axis_index("x")
    c = lax.axis_index("c")
    row_count = query_small.shape[0]
    positions = (z * n_y + y) * row_count + jnp.arange(row_count, dtype=jnp.int32)

    query = jnp.concatenate(
        [
            query_large[:, :HEAD_LARGE],
            query_small[:, :HEAD_SMALL],
            rotate(query_small[:, HEAD_SMALL:], positions),
            rotate(query_large[:, HEAD_LARGE:], positions),
        ],
        axis=1,
    )
    width = query.shape[1]
    depth = gate_weight.shape[0]
    groups = row_count // depth
    query_wide = jnp.concatenate(
        [query[depth * g : depth * (g + 1)] for g in range(groups)], axis=1
    )
    cut = gate_weight.shape[1] // n_y
    chunks = jnp.stack(
        [
            jnp.concatenate(
                [query_wide]
                + [w[:, cut * j : cut * (j + 1)] for w in (gate_weight, up_weight, down_weight)],
                axis=1,
            )
            for j in range(n_y)
        ]
    )
    first = exchanged(chunks, "y")
    weights = lax.all_gather(
        first[:, :, width * groups :].reshape(n_y * depth, 3 * cut), "z", axis=0, tiled=True
    )
    queries = jnp.concatenate(
        [
            first[i, :, width * g : width * (g + 1)]
            for i in range(n_y)
            for g in range(groups)
        ],
        axis=0,
    )

    t = x * 2 + c
    turned_key = rotate(rope_key, positions)
    slice_latent = lax.dynamic_slice_in_dim(latent, 32 * t, 32, 1).T
    slice_turned = lax.dynamic_slice_in_dim(turned_key, 8 * x, 8, 1).T
    packed = jnp.concatenate([slice_latent, slice_turned], axis=0)
    along_z = from_everyone(packed, "z")
    mine = from_everyone(along_z, "x")
    other = partner(mine)

    place = jnp.stack([z, y, c]).astype(jnp.int32)
    partial = attention(
        place, queries, mine, other, key_up_small, key_up_large, value_up_small, value_up_large
    )
    parts = exchanged(partial.reshape(n_y, row_count, partial.shape[1]), "y")
    mixed_part = merge(parts, out_small, out_large)
    rows = residual.shape[0]
    d = residual.shape[1]
    tiles = exchanged(mixed_part.reshape(row_count // rows, rows, d), ("x", "c"))
    mixed = jnp.sum(tiles.astype(jnp.float32), axis=0).astype(jnp.bfloat16)
    stream = (residual.astype(jnp.float32) + mixed.astype(jnp.float32)).astype(jnp.bfloat16)
    as_float = stream.astype(jnp.float32)
    normed = as_float * lax.rsqrt(jnp.mean(as_float * as_float, axis=-1, keepdims=True) + norm_eps)
    normed = (normed * norm_gain.astype(jnp.float32)[None, :]).astype(jnp.bfloat16)

    here = from_everyone(normed, ("y", "x")).reshape(n_y * n_x * rows, d)
    there = partner(here)
    gate_full = weights[:, :cut]
    up_full = weights[:, cut : 2 * cut]
    down_full = weights[:, 2 * cut :]

    def mixer(piece):
        gate_part = jnp.dot(piece, gate_full, preferred_element_type=jnp.float32)
        up_part = jnp.dot(piece, up_full, preferred_element_type=jnp.float32)
        hidden = (jax.nn.silu(gate_part) * up_part).astype(jnp.bfloat16)
        return lax.dot_general(hidden, down_full, NT, preferred_element_type=jnp.float32)

    sent = partner(mixer(there).astype(jnp.bfloat16))
    both = (mixer(here) + sent.astype(jnp.float32)).astype(jnp.bfloat16)
    pieces = exchanged(both.reshape(n_y * n_x, rows, d), ("y", "x"))
    channel = jnp.sum(pieces.astype(jnp.float32), axis=0).astype(jnp.bfloat16)
    return (as_float + 0.5 * channel.astype(jnp.float32)).astype(jnp.bfloat16)


def solution(mesh):
    fine = Mesh(mesh.devices.reshape(-1, 4, 4, 2), ("z", "y", "x", "c"))
    sp = ("z", "y")
    tp = ("x", "c")
    both = ("z", "y", "x", "c")
    placed = (
        P(both, None),
        P(sp, tp),
        P(sp, tp),
        P(sp, None),
        P(sp, None),
        P(None, tp),
        P(None, tp),
        P(None, tp),
        P(None, tp),
        P(tp, None),
        P(tp, None),
        P(),
        P(sp, tp),
        P(sp, tp),
        P(sp, tp),
    )
    return jax.shard_map(
        shards, mesh=fine, in_specs=placed, out_specs=P(both, None), check_vma=False
    )
```

time: 349 us -> 187 us (0.54)
  waiting for transfers between devices: 133 us -> 36.4 us
  blocking collectives: 121 us -> 48.5 us
  matrix products: 47.6 us -> 12.5 us
  starting transfers between devices: 14.8 us -> 43.9 us
  Pallas kernels: 0 us -> 16.7 us
  other arithmetic: 15.8 us -> 3.93 us
  local copies, waits for them, and re-layouts: 2.37 us -> 10.7 us
    all_gather x2 -> x1, waiting for transfers between devices: 123 us -> 0.02 us  [shards(): lax.all_gather(first[:, :, width * groups:].reshape(n_y * depth, 3 * cut)...]
    all_gather x1 -> x0, blocking collectives: 86.3 us -> none  [shards(): part_rope = lax.all_gather(rope_key, 'sp', axis=0, tiled=True)]
    dot_general x10 -> x4, matrix products: 47.6 us -> 12.5 us  [the longest x2 8.31 us: mixer(): lax.dot_general(hidden, down_full, NT, preferred_element_type=jnp.float32)]
    all_to_all x1 -> x4, waiting for transfers between devices: 9.34 us -> 31.7 us  [the longest x2 18.9 us: from_everyone(): return lax.all_to_all(copies, axis, split_axis=0, concat_axis=0, tiled=True)]
    pallas_call x0 -> x2, Pallas kernels: none -> 16.7 us  [the longest x1 14 us: attention(): pl.pallas_call(attention_kernel, out_shape=jax.ShapeDtypeStruct(query.sha...]
    all_to_all x1 -> x4, starting transfers between devices: 14.8 us -> 29.4 us  [the longest x2 19.8 us: from_everyone(): return lax.all_to_all(copies, axis, split_axis=0, concat_axis=0, tiled=True)]
    ppermute x0 -> x3, starting transfers between devices: none -> 14.4 us  [partner(): return lax.ppermute(x, 'c', [(0, 1), (1, 0)])]
    all_to_all x1 -> x2, blocking collectives: 21.6 us -> 29.5 us  [exchanged(): return lax.all_to_all(chunks, axis, split_axis=0, concat_axis=0, tiled=True)]
  transfers between devices with their start and end apart: 3 -> 8, of which waited for: 3 -> 7; matrix products, arithmetic and copies ran while one was open for 16% -> 4% of each run, Pallas kernels for 0% -> 9%
where the time goes in v1:
time: 187 us; the launch traced here: 186 us
  blocking collectives  48.5 us (26%)
  starting transfers between devices  43.9 us (23%)
  waiting for transfers between devices  36.4 us (19%)
  Pallas kernels  16.7 us (9%)
  between operations  13.7 us (7%)
  matrix products  12.5 us (7%)
  local copies, waits for them, and re-layouts  10.7 us (6%)
  other arithmetic  3.93 us (2%)
    all_to_all x2, blocking collectives, exchanged(): return lax.all_to_all(chunks, axis, split_axis=0, concat_axis=0, tiled=True)  29.5 us
    all_to_all x2, starting transfers between devices, from_everyone(): return lax.all_to_all(copies, axis, split_axis=0, concat_axis=0, tiled=True)  19.8 us
    all_to_all x1, blocking collectives, from_everyone(): return lax.all_to_all(copies, axis, split_axis=0, concat_axis=0, tiled=True)  19 us
    all_to_all x2, waiting for transfers between devices, from_everyone(): return lax.all_to_all(copies, axis, split_axis=0, concat_axis=0, tiled=True)  18.9 us
    ppermute x3, starting transfers between devices, partner(): return lax.ppermute(x, 'c', [(0, 1), (1, 0)])  14.4 us
    pallas_call x1, Pallas kernels, attention(): pl.pallas_call(attention_kernel, out_shape=jax.ShapeDtypeStruct(query.sha...  14 us
    all_to_all x2, waiting for transfers between devices, exchanged(): return lax.all_to_all(chunks, axis, split_axis=0, concat_axis=0, tiled=True)  12.8 us
    all_to_all x2, starting transfers between devices, exchanged(): return lax.all_to_all(chunks, axis, split_axis=0, concat_axis=0, tiled=True)  9.63 us
  transfers between devices with their start and end apart: 8, of which 7 were waited for; matrix products, arithmetic and copies ran while one was open for 4% of the time, Pallas kernels for 9%

profile of v1, /device:TPU:1, one launch (start us, length us, event | category | flops | bytes accessed | tf_op | source)
XLA Modules:
  0.0 186.4 jit_solution(13473526776167704958)
XLA Ops:
  11.6 1.0 fusion.54
  13.8 5.0 %all-to-all-start = ((bf16[4,32,1552]{2,1,0:T(8,128)(2,1)}), bf16[4,32,1552]{2,1,0:T(8,128)(2,1)S(1)}, u32[]{:S(2)}, u32[]{:S(2)}) async-start(bf16[4,32,1552]{2,1,0:T(8,128)(2,1)} %pad_maximum_fusion), calls=%async_computation | async-start | bytes 851968 | tf_op jit(solution)/shard_map/all_to_all | solution.py:43
  21.8 3.4 %all-to-all-done = bf16[4,32,1552]{2,1,0:T(8,128)(2,1)S(1)} async-done(((bf16[4,32,1552]{2,1,0:T(8,128)(2,1)}), bf16[4,32,1552]{2,1,0:T(8,128)(2,1)S(1)}, u32[]{:S(2)}, u32[]{:S(2)}) %all-to-all-start) | async-done | bytes 397344 | tf_op jit(solution)/shard_map/all_to_all | solution.py:43
  25.9 15.8 %all-to-all-start.1 = ((bf16[16,40,128]{2,1,0:T(8,128)(2,1)}), bf16[16,40,128]{2,1,0:T(8,128)(2,1)S(1)}, u32[]{:S(2)}, u32[]{:S(2)}) async-start(bf16[16,40,128]{2,1,0:T(8,128)(2,1)} %broadcast_in_dim.6), calls=%async_computation.1 | async-start | bytes 327680 | tf_op jit(solution)/shard_map/all_to_all | solution.py:39
  42.6 11.2 %all-to-all-done.1 = bf16[16,40,128]{2,1,0:T(8,128)(2,1)S(1)} async-done(((bf16[16,40,128]{2,1,0:T(8,128)(2,1)}), bf16[16,40,128]{2,1,0:T(8,128)(2,1)S(1)}, u32[]{:S(2)}, u32[]{:S(2)}) %all-to-all-start.1) | async-done | bytes 163872 | tf_op jit(solution)/shard_map/all_to_all | solution.py:39
  53.8 0.9 broadcast_in_dim.7
  54.8 4.0 %all-to-all-start.2 = ((bf16[4,16,40,128]{3,2,1,0:T(8,128)(2,1)}), bf16[4,16,40,128]{3,2,1,0:T(8,128)(2,1)S(1)}, u32[]{:S(2)}, u32[]{:S(2)}) async-start(bf16[4,16,40,128]{3,2,1,0:T(8,128)(2,1)} %broadcast_in_dim.7), calls=%async_computation.2 | async-start | bytes 1310720 | tf_op jit(solution)/shard_map/all_to_all | solution.py:39
  58.8 7.6 %all-to-all-done.2.mine = bf16[4,16,40,128]{3,2,1,0:T(8,128)(2,1)S(1)} async-done(((bf16[4,16,40,128]{3,2,1,0:T(8,128)(2,1)}), bf16[4,16,40,128]{3,2,1,0:T(8,128)(2,1)S(1)}, u32[]{:S(2)}, u32[]{:S(2)}) %all-to-all-start.2) | async-done | bytes 655392 | tf_op jit(solution)/shard_map/all_to_all | solution.py:39
  66.4 8.3 %collective-permute-start = (bf16[4,16,40,128]{3,2,1,0:T(8,128)(2,1)S(1)}, bf16[4,16,40,128]{3,2,1,0:T(8,128)(2,1)S(1)}, u32[]{:S(2)}, u32[]{:S(2)}) collective-permute-start(bf16[4,16,40,128]{3,2,1,0:T(8,128)(2,1)S(1)} %all-to-all-done.2.mine), channel_id=1, source_target_pairs={{0,1},{1,0},{2,3},{3,2},{4,5},{5,4},{6,7},{7,6},{8,9},{9,8},{10,11... | collective-permute-start | bytes 1966088 | tf_op jit(solution)/shard_map/ppermute | solution.py:47
  74.8 1.6 collective-permute-done.other
  77.3 14.0 %attend.1 = bf16[512,256]{1,0:T(8,128)(2,1)} custom-call(s32[3]{0:T(128)} %pad_add_fusion.place, bf16[512,256]{1,0:T(8,128)(2,1)} %copy-done.4, bf16[4,16,40,128]{3,2,1,0:T(8,128)(2,1)} %copy-done.1, bf16[4,16,40,128]{3,2,1,0:T(8,128)(2,1)} %copy-done.2, bf16[256,64]{1,0:T(8,128)(2,1)} %copy.52.key_up_s, bf16[256,128]{1,0:T(8,128)(2,1)} %key_up_l.1, ...), custom_call_target="tpu_custom_call" | custom-call | tf_op jit(solution)/shard_map/attend/pallas_call | solution.py:123
  91.3 10.5 %all_to_all.35.parts = bf16[4,128,256]{2,1,0:T(8,128)(2,1)} all-to-all(bf16[4,128,256]{2,1,0:T(8,128)(2,1)} %bitcast.87), channel_id=1, replica_groups=mesh['z'=16,'y'=4,'x'=4,'c'=2] {'y'}, dimensions={0} | all-to-all | bytes 524288 | tf_op jit(solution)/shard_map/all_to_all | solution.py:43
  101.8 2.7 %merge.1 = bf16[128,2048]{1,0:T(8,128)(2,1)} custom-call(bf16[4,128,256]{2,1,0:T(8,128)(2,1)} %all_to_all.35.parts, bf16[64,2048]{1,0:T(8,128)(2,1)} %out_s.1, bf16[128,2048]{1,0:T(8,128)(2,1)} %out_l.1), custom_call_target="tpu_custom_call" | custom-call | tf_op jit(solution)/shard_map/merge/pallas_call | solution.py:169
  104.5 4.6 %all-to-all-start.4 = ((bf16[8,16,2048]{2,1,0:T(8,128)(2,1)}), bf16[8,16,2048]{2,1,0:T(8,128)(2,1)S(1)}, u32[]{:S(2)}, u32[]{:S(2)}) async-start(bf16[8,16,2048]{2,1,0:T(8,128)(2,1)} %bitcast.86), calls=%async_computation.4 | async-start | bytes 1048576 | tf_op jit(solution)/shard_map/all_to_all | solution.py:43
  109.1 9.4 %all-to-all-done.4 = bf16[8,16,2048]{2,1,0:T(8,128)(2,1)S(1)} async-done(((bf16[8,16,2048]{2,1,0:T(8,128)(2,1)}), bf16[8,16,2048]{2,1,0:T(8,128)(2,1)S(1)}, u32[]{:S(2)}, u32[]{:S(2)}) %all-to-all-start.4) | async-done | bytes 524320 | tf_op jit(solution)/shard_map/all_to_all | solution.py:43
  119.0 19.0 %all_to_all.36 = bf16[16,16,2048]{2,1,0:T(8,128)(2,1)S(1)} all-to-all(bf16[16,16,2048]{2,1,0:T(8,128)(2,1)S(1)} %broadcast_in_dim.8), channel_id=1, replica_groups=mesh['z'=16,'y'=4,'x'=4,'c'=2] {'y','x'}, dimensions={0} | all-to-all | bytes 2097152 | tf_op jit(solution)/shard_map/all_to_all | solution.py:39
  138.0 3.8 %collective-permute-start.1 = (bf16[256,2048]{1,0:T(8,128)(2,1)S(1)}, bf16[256,2048]{1,0:T(8,128)(2,1)S(1)}, u32[]{:S(2)}, u32[]{:S(2)}) collective-permute-start(bf16[256,2048]{1,0:T(8,128)(2,1)S(1)} %bitcast.83), channel_id=1, source_target_pairs={{0,1},{1,0},{2,3},{3,2},{4,5},{5,4},{6,7},{7,6},{8,9},{9,8},{10,11... | collective-permute-start | bytes 3145736 | tf_op jit(solution)/shard_map/ppermute | solution.py:47
  141.8 2.2 %collective-permute-done.1 = bf16[256,2048]{1,0:T(8,128)(2,1)S(1)} collective-permute-done((bf16[256,2048]{1,0:T(8,128)(2,1)S(1)}, bf16[256,2048]{1,0:T(8,128)(2,1)S(1)}, u32[]{:S(2)}, u32[]{:S(2)}) %collective-permute-start.1) | collective-permute-done | bytes 1048608 | tf_op jit(solution)/shard_map/ppermute | solution.py:47
  144.0 2.4 %fusion.4 = f32[256,176]{0,1:T(8,128)S(1)} fusion(bf16[256,2048]{1,0:T(8,128)(2,1)S(1)} %collective-permute-done.1, bf16[2048,528]{1,0:T(8,128)(2,1)} %all-gather.2.cloned.1.call-done), kind=kOutput, calls=%fused_computation.7 | convolution fusion | flops 184549376 | bytes 2277376 | tf_op jit(solution)/shard_map/dot_general | solution.py:275
  146.5 4.2 %convolution_convert_fusion = bf16[256,2048]{1,0:T(8,128)(2,1)} fusion(bf16[2048,528]{1,0:T(8,128)(2,1)} %all-gather.2.cloned.1.call-done, f32[256,176]{0,1:T(8,128)S(1)} %fusion.4, bf16[256,2048]{1,0:T(8,128)(2,1)S(1)} %collective-permute-done.1), kind=kOutput, calls=%fused_computation | convolution fusion | flops 369893376 | bytes 4374528 | tf_op jit(solution)/shard_map/dot_general | solution.py:277
  150.7 2.3 %collective-permute-start.2 = (bf16[256,2048]{1,0:T(8,128)(2,1)}, bf16[256,2048]{1,0:T(8,128)(2,1)}, u32[]{:S(2)}, u32[]{:S(2)}) collective-permute-start(bf16[256,2048]{1,0:T(8,128)(2,1)} %convolution_convert_fusion), channel_id=1, source_target_pairs={{0,1},{1,0},{2,3},{3,2},{4,5},{5,4},{6,7},{7,6},{8,9},{9,8},{10,11... | collective-permute-start | bytes 3145736 | tf_op jit(solution)/shard_map/ppermute | solution.py:47
  153.0 1.8 fusion.10
  155.6 4.1 %add_convert_fusion = bf16[256,2048]{1,0:T(8,128)(2,1)S(1)} fusion(bf16[256,2048]{1,0:T(8,128)(2,1)} %collective-permute-done.2, bf16[256,2048]{1,0:T(8,128)(2,1)S(1)} %bitcast.85, bf16[2048,528]{1,0:T(8,128)(2,1)} %all-gather.2.cloned.1.call-done, f32[256,176]{0,1:T(8,128)S(1)} %fusion.10), kind=kOutput, calls=%fused_computation.1 | convolution fusion | flops 370941952 | bytes 5423104 | tf_op jit(solution)/shard_map/dot_general | solution.py:277
  159.7 19.0 %all_to_all.37 = bf16[16,16,2048]{2,1,0:T(8,128)(2,1)S(1)} all-to-all(bf16[16,16,2048]{2,1,0:T(8,128)(2,1)S(1)} %bitcast.88), channel_id=1, replica_groups=mesh['z'=16,'y'=4,'x'=4,'c'=2] {'y','x'}, dimensions={0} | all-to-all | bytes 2097152 | tf_op jit(solution)/shard_map/all_to_all | solution.py:43
  (82 shorter events, 13.7 us)
Async XLA Ops:
  6.5 13.0 %copy-start = (bf16[128,256]{1,0:T(8,128)(2,1)S(1)}, bf16[128,256]{1,0:T(8,128)(2,1)}, u32[]{:S(2)}) copy-start(bf16[128,256]{1,0:T(8,128)(2,1)} %param.18) | copy-start | bytes 196612
  6.5 12.3 %copy-start.7 = (bf16[128,32]{0,1:T(8,128)(2,1)S(1)}, bf16[128,32]{0,1:T(8,128)(2,1)}, u32[]{:S(2)}) copy-start(bf16[128,32]{0,1:T(8,128)(2,1)} %param.19) | copy-start | bytes 24580
  6.5 13.2 %copy-start.5 = (bf16[256,64]{0,1:T(8,128)(2,1)S(1)}, bf16[256,64]{0,1:T(8,128)(2,1)}, u32[]{:S(2)}) copy-start(bf16[256,64]{0,1:T(8,128)(2,1)} %param.20) | copy-start | bytes 98308
  6.5 14.0 %copy-start.6 = (bf16[256,64]{0,1:T(8,128)(2,1)S(1)}, bf16[256,64]{0,1:T(8,128)(2,1)}, u32[]{:S(2)}) copy-start(bf16[256,64]{0,1:T(8,128)(2,1)} %param.21) | copy-start | bytes 98308
  13.8 11.4 %all-to-all-start = ((bf16[4,32,1552]{2,1,0:T(8,128)(2,1)}), bf16[4,32,1552]{2,1,0:T(8,128)(2,1)S(1)}, u32[]{:S(2)}, u32[]{:S(2)}) async-start(bf16[4,32,1552]{2,1,0:T(8,128)(2,1)} %pad_maximum_fusion), calls=%async_computation | async-start | bytes 851968 | tf_op jit(solution)/shard_map/all_to_all | solution.py:43
  25.9 27.9 %all-to-all-start.1 = ((bf16[16,40,128]{2,1,0:T(8,128)(2,1)}), bf16[16,40,128]{2,1,0:T(8,128)(2,1)S(1)}, u32[]{:S(2)}, u32[]{:S(2)}) async-start(bf16[16,40,128]{2,1,0:T(8,128)(2,1)} %broadcast_in_dim.6), calls=%async_computation.1 | async-start | bytes 327680 | tf_op jit(solution)/shard_map/all_to_all | solution.py:39
  41.7 100.1 %all-gather.2.cloned.1.call-start = ((), (), s32[]{:S(2)}) async-start(), calls=%async_computation.7 | async-start | bytes 2785280 | tf_op jit(solution)/shard_map/all_gather | solution.py:231
  54.8 11.6 %all-to-all-start.2 = ((bf16[4,16,40,128]{3,2,1,0:T(8,128)(2,1)}), bf16[4,16,40,128]{3,2,1,0:T(8,128)(2,1)S(1)}, u32[]{:S(2)}, u32[]{:S(2)}) async-start(bf16[4,16,40,128]{3,2,1,0:T(8,128)(2,1)} %broadcast_in_dim.7), calls=%async_computation.2 | async-start | bytes 1310720 | tf_op jit(solution)/shard_map/all_to_all | solution.py:39
  66.4 10.1 %copy-start.1 = (bf16[4,16,40,128]{3,2,1,0:T(8,128)(2,1)}, bf16[4,16,40,128]{3,2,1,0:T(8,128)(2,1)S(1)}, u32[]{:S(2)}) copy-start(bf16[4,16,40,128]{3,2,1,0:T(8,128)(2,1)S(1)} %all-to-all-done.2.mine) | copy-start | bytes 1966084
  66.4 10.1 %collective-permute-start = (bf16[4,16,40,128]{3,2,1,0:T(8,128)(2,1)S(1)}, bf16[4,16,40,128]{3,2,1,0:T(8,128)(2,1)S(1)}, u32[]{:S(2)}, u32[]{:S(2)}) collective-permute-start(bf16[4,16,40,128]{3,2,1,0:T(8,128)(2,1)S(1)} %all-to-all-done.2.mine), channel_id=1, source_target_pairs={{0,1},{1,0},{2,3},{3,2},{4,5},{5,4},{6,7},{7,6},{8,9},{9,8},{10,11... | collective-permute-start | bytes 1966088 | tf_op jit(solution)/shard_map/ppermute | solution.py:47
  74.8 1.7 copy-start.4
  74.8 34.3 %copy-start.8 = (bf16[2048]{0:T(1024)(128)(2,1)S(1)}, bf16[2048]{0:T(1024)(128)(2,1)}, u32[]{:S(2)}) copy-start(bf16[2048]{0:T(1024)(128)(2,1)} %param.26) | copy-start | bytes 12292
  74.8 43.8 %copy-start.3 = (bf16[16,2048]{1,0:T(8,128)(2,1)S(1)}, bf16[16,2048]{1,0:T(8,128)(2,1)}, u32[]{:S(2)}) copy-start(bf16[16,2048]{1,0:T(8,128)(2,1)} %param.15) | copy-start | bytes 196612
  76.5 0.8 copy-start.2
  104.5 14.0 %all-to-all-start.4 = ((bf16[8,16,2048]{2,1,0:T(8,128)(2,1)}), bf16[8,16,2048]{2,1,0:T(8,128)(2,1)S(1)}, u32[]{:S(2)}, u32[]{:S(2)}) async-start(bf16[8,16,2048]{2,1,0:T(8,128)(2,1)} %bitcast.86), calls=%async_computation.4 | async-start | bytes 1048576 | tf_op jit(solution)/shard_map/all_to_all | solution.py:43
  138.0 6.1 %collective-permute-start.1 = (bf16[256,2048]{1,0:T(8,128)(2,1)S(1)}, bf16[256,2048]{1,0:T(8,128)(2,1)S(1)}, u32[]{:S(2)}, u32[]{:S(2)}) collective-permute-start(bf16[256,2048]{1,0:T(8,128)(2,1)S(1)} %bitcast.83), channel_id=1, source_target_pairs={{0,1},{1,0},{2,3},{3,2},{4,5},{5,4},{6,7},{7,6},{8,9},{9,8},{10,11... | collective-permute-start | bytes 3145736 | tf_op jit(solution)/shard_map/ppermute | solution.py:47
  150.7 4.9 %collective-permute-start.2 = (bf16[256,2048]{1,0:T(8,128)(2,1)}, bf16[256,2048]{1,0:T(8,128)(2,1)}, u32[]{:S(2)}, u32[]{:S(2)}) collective-permute-start(bf16[256,2048]{1,0:T(8,128)(2,1)} %convolution_convert_fusion), channel_id=1, source_target_pairs={{0,1},{1,0},{2,3},{3,2},{4,5},{5,4},{6,7},{7,6},{8,9},{9,8},{10,11... | collective-permute-start | bytes 3145736 | tf_op jit(solution)/shard_map/ppermute | solution.py:47
Sparse Core Ops, SparseCore 0:
  44.6 65.7 all-gather.1

commit v2 on v1

v2 whole, which is shorter than its diff:
```python
import jax
import jax.numpy as jnp
from jax import lax
from jax.experimental import pallas as pl
from jax.experimental.pallas import tpu as pltpu
from jax.sharding import Mesh
from jax.sharding import PartitionSpec as P


HEAD_SMALL = 64
HEAD_LARGE = 128
ROPE = 32
SCALE_SMALL = (HEAD_SMALL + ROPE) ** (-0.5)
SCALE_LARGE = (HEAD_LARGE + ROPE) ** (-0.5)

big_negative = -1e30
rope_base = 500000.0
norm_eps = 1e-06

NT = (((1,), (1,)), ((), ()))
MIB = 1024 * 1024
VMEM = pl.BlockSpec(memory_space=pltpu.VMEM)
SMEM = pl.BlockSpec(memory_space=pltpu.SMEM)


def from_everyone(shard, axis):
    copies = jnp.broadcast_to(shard, (lax.axis_size(axis), *shard.shape))
    return lax.all_to_all(copies, axis, split_axis=0, concat_axis=0, tiled=True)


def exchanged(chunks, axis):
    return lax.all_to_all(chunks, axis, split_axis=0, concat_axis=0, tiled=True)


def partner(x):
    return lax.ppermute(x, "c", [(0, 1), (1, 0)])


def three_parts(v):
    high = v.astype(jnp.bfloat16).astype(jnp.float32)
    rest = v - high
    middle = rest.astype(jnp.bfloat16).astype(jnp.float32)
    low = (rest - middle).astype(jnp.bfloat16).astype(jnp.float32)
    return [high, middle, low]


def weights_kernel(gate, up, down, out):
    cut = gate.shape[1] // 2
    room = out.shape[2] // 3
    depth = gate.shape[0]
    blank = jnp.zeros((depth, room - cut), jnp.float32)
    for k, w in enumerate((gate, up, down)):
        whole = w[...].astype(jnp.float32)
        for j in range(2):
            half = jnp.concatenate([whole[:, cut * j : cut * (j + 1)], blank], axis=1)
            half = half.astype(jnp.bfloat16)
            for i in range(out.shape[0] // 2):
                out[2 * i + j, :, room * k : room * (k + 1)] = half


def pack_weights(gate, up, down, n_y):
    room = -(-(gate.shape[1] // 2) // 128) * 128
    return pl.pallas_call(
        weights_kernel,
        out_shape=jax.ShapeDtypeStruct((n_y, gate.shape[0], 3 * room), jnp.bfloat16),
        in_specs=[VMEM] * 3,
        out_specs=VMEM,
        name="pack_weights",
    )(gate, up, down)


def prepare_kernel(place, small, large, latent, rope_key, table, query, packed, tall):
    cosine = table[:, 0:ROPE]
    sine = table[:, ROPE : 2 * ROPE]

    def turn(v):
        v = v.astype(jnp.float32)
        swapped = jnp.concatenate([v[:, ROPE // 2 :], v[:, : ROPE // 2]], axis=1)
        return v * cosine + swapped * sine

    s = small[...].astype(jnp.float32)
    g = large[...].astype(jnp.float32)
    turned_s = turn(s[:, HEAD_SMALL:]) * SCALE_SMALL
    turned_l = turn(g[:, HEAD_LARGE:]) * SCALE_LARGE
    query[:, 0:128] = large[:, 0:HEAD_LARGE]
    query[:, 128:256] = jnp.concatenate([s[:, :HEAD_SMALL], turned_s, turned_l], axis=1).astype(
        jnp.bfloat16
    )
    tall[0:256, :] = latent[...].astype(jnp.float32).T
    tall[256 : 256 + ROPE, :] = turn(rope_key[...]).astype(jnp.bfloat16).astype(jnp.float32).T
    mine = tall[pl.ds(pl.multiple_of(32 * place[3], 32), 32), :]
    ours = tall[pl.ds(pl.multiple_of(256 + 8 * place[2], 8), 8), :]
    packed[...] = jnp.concatenate([mine, ours], axis=0).astype(jnp.bfloat16)


def prepare(place, small, large, latent, rope_key, table):
    rows = small.shape[0]
    return pl.pallas_call(
        prepare_kernel,
        out_shape=(
            jax.ShapeDtypeStruct((rows, 256), jnp.bfloat16),
            jax.ShapeDtypeStruct((40, rows), jnp.bfloat16),
        ),
        in_specs=[SMEM] + [VMEM] * 5,
        out_specs=(VMEM, VMEM),
        scratch_shapes=[pltpu.VMEM((256 + ROPE, rows), jnp.float32)],
        name="prepare",
    )(place, small, large, latent, rope_key, table)


def absorb_kernel(place, *refs):
    *queries, key_up_s, key_up_l, out = refs
    n_y = len(queries)
    y = place[1]
    row = lax.broadcasted_iota(jnp.int32, (128, 128), 0)
    lane = lax.broadcasted_iota(jnp.int32, (128, 128), 1)
    diagonal = jnp.where(row == lane, 1.0, 0.0)
    pick_lane = lax.broadcasted_iota(jnp.int32, (128, 96), 1)
    for k, query in enumerate(queries):
        j = lax.rem(y - k + n_y, n_y)
        q = query[...]
        own = diagonal if k == 0 else jnp.zeros((128, 128), jnp.float32)
        pick = jnp.where(pick_lane == j, 1.0, 0.0)
        heads = (
            (q[:, 0:128], q[:, 224:256], key_up_l, SCALE_LARGE),
            (q[:, 128:192], q[:, 192:224], key_up_s, SCALE_SMALL),
        )
        for h, (nope, rope, key_up, scale) in enumerate(heads):
            wide = lax.dot_general(nope, key_up[...], NT, preferred_element_type=jnp.float32)
            tail = jnp.concatenate([rope.astype(jnp.float32), pick], axis=1)
            whole = jnp.concatenate([wide * scale, tail, own], axis=1)
            out[j, h, :, :] = whole.astype(jnp.bfloat16)


def absorb(place, queries, key_up_s, key_up_l):
    n_y, rows = len(queries), queries[0].shape[0]
    return pl.pallas_call(
        absorb_kernel,
        out_shape=jax.ShapeDtypeStruct((n_y, 2, rows, 512), jnp.bfloat16),
        in_specs=[SMEM] + [VMEM] * (n_y + 2),
        out_specs=VMEM,
        name="absorb",
    )(place, *queries, key_up_s, key_up_l)


def attention_kernel(place, query, mine, other, value_up_s, value_up_l, out, keys):
    z = place[0]
    y = place[1]
    c = place[4]
    n_x, n_z = mine.shape[0], mine.shape[1]
    n_y = query.shape[0]
    row = lax.broadcasted_iota(jnp.int32, (128, 128), 0)
    lane = lax.broadcasted_iota(jnp.int32, (128, 128), 1)
    for k in range(n_z):
        lanes = pl.ds(128 * k, 128)
        for x in range(n_x):
            here = pl.multiple_of(64 * x + 32 * c, 32)
            there = pl.multiple_of(64 * x + 32 * (1 - c), 32)
            keys[pl.ds(here, 32), lanes] = mine[x, k, 0:32, :]
            keys[pl.ds(there, 32), lanes] = other[x, k, 0:32, :]
        ropes = [mine[x, k, 32:40, :].astype(jnp.float32) for x in range(n_x)]
        keys[256 : 256 + ROPE, lanes] = jnp.concatenate(ropes, axis=0).astype(jnp.bfloat16)
        hidden_from = (k > z) | ((k == z) & (y > row))
        bias = jnp.where(hidden_from & (row < n_y), big_negative, 0.0)
        keys[288:384, lanes] = bias[0:96, :].astype(jnp.bfloat16)
        later = jnp.where((lane > row) & (k == z), big_negative, 0.0)
        keys[384:512, lanes] = later.astype(jnp.bfloat16)
    stat_lane = lax.broadcasted_iota(jnp.int32, (128, 64), 1)

    def head(full, value_up):
        score = jnp.dot(full, keys[...], preferred_element_type=jnp.float32)
        top = jnp.max(score, axis=1, keepdims=True)
        weight = jnp.exp(score - top)
        total = jnp.sum(weight, axis=1, keepdims=True)
        summed = lax.dot_general(
            weight.astype(jnp.bfloat16), keys[0:256, :], NT, preferred_element_type=jnp.float32
        )
        summed = (summed / total).astype(jnp.bfloat16)
        value = jnp.dot(summed, value_up[...], preferred_element_type=jnp.float32)
        return value, top, total

    for j in range(n_y):
        value_l, top_l, total_l = head(query[j, 0], value_up_l)
        value_s, top_s, total_s = head(query[j, 1], value_up_s)
        stats = jnp.zeros((128, 64), jnp.float32)
        parts = three_parts(top_l) + three_parts(total_l) + three_parts(top_s) + three_parts(total_s)
        for i, part in enumerate(parts):
            stats = jnp.where(stat_lane == i, part, stats)
        out[j, :, 0:128] = value_l.astype(jnp.bfloat16)
        out[j, :, 128:256] = jnp.concatenate([value_s, stats], axis=1).astype(jnp.bfloat16)


def attention(place, query, mine, other, value_up_s, value_up_l):
    n_y, _, rows, depth = query.shape
    n_keys = 128 * mine.shape[1]
    return pl.pallas_call(
        attention_kernel,
        out_shape=jax.ShapeDtypeStruct((n_y, rows, 256), jnp.bfloat16),
        in_specs=[SMEM] + [VMEM] * 5,
        out_specs=VMEM,
        scratch_shapes=[pltpu.VMEM((depth, n_keys), jnp.bfloat16)],
        compiler_params=pltpu.CompilerParams(vmem_limit_bytes=24 * MIB),
        name="attend",
    )(place, query, mine, other, value_up_s, value_up_l)


def merge_kernel(parts, out_s, out_l, out):
    n = parts.shape[0]

    def merged(first, width, stat):
        def stat_of(i, k):
            at = 192 + stat + 3 * k
            return (
                parts[i, :, at : at + 1].astype(jnp.float32)
                + parts[i, :, at + 1 : at + 2].astype(jnp.float32)
            ) + parts[i, :, at + 2 : at + 3].astype(jnp.float32)

        tops = [stat_of(i, 0) for i in range(n)]
        top = tops[0]
        for t in tops[1:]:
            top = jnp.maximum(top, t)
        shares = [stat_of(i, 1) * jnp.exp(tops[i] - top) for i in range(n)]
        total = sum(shares[1:], shares[0])
        acc = 0.0
        for i in range(n):
            acc = acc + parts[i, :, first : first + width].astype(jnp.float32) * (shares[i] / total)
        return acc.astype(jnp.bfloat16)

    large = merged(0, 128, 0)
    small = merged(128, 64, 6)
    mixed = jnp.dot(small, out_s[...], preferred_element_type=jnp.float32) + jnp.dot(
        large, out_l[...], preferred_element_type=jnp.float32
    )
    out[...] = mixed.astype(jnp.bfloat16)


def merge(parts, out_s, out_l):
    return pl.pallas_call(
        merge_kernel,
        out_shape=jax.ShapeDtypeStruct((parts.shape[1], out_s.shape[1]), jnp.bfloat16),
        in_specs=[VMEM] * 3,
        out_specs=VMEM,
        name="merge",
    )(parts, out_s, out_l)


def mixer_kernel(here, there, gate_up, down, out_here, out_there, gate, up, hidden):
    step = pl.program_id(0)
    half = pl.num_programs(0) // 2
    rows = here.shape[0]
    room = down.shape[1]

    @pl.when(step == 0)
    def _():
        gate[...] = jnp.zeros_like(gate)
        up[...] = jnp.zeros_like(up)

    @pl.when(step < half)
    def _():
        x = jnp.concatenate([here[...], there[...]], axis=0)
        gate[...] += jnp.dot(x, gate_up[:, 0:room], preferred_element_type=jnp.float32)
        up[...] += jnp.dot(x, gate_up[:, room : 2 * room], preferred_element_type=jnp.float32)

    @pl.when(step == half - 1)
    def _():
        g = gate[...]
        hidden[...] = (g / (1.0 + jnp.exp(-g)) * up[...]).astype(jnp.bfloat16)

    @pl.when(step >= half)
    def _():
        part = lax.dot_general(hidden[...], down[...], NT, preferred_element_type=jnp.float32)
        out_here[...] = part[0:rows, :]
        out_there[...] = part[rows : 2 * rows, :].astype(jnp.bfloat16)


def mixer(here, there, weights):
    rows, d = here.shape
    room = weights.shape[1] // 3
    n = 4
    block = d // n
    return pl.pallas_call(
        mixer_kernel,
        grid=(2 * n,),
        out_shape=(
            jax.ShapeDtypeStruct((rows, d), jnp.float32),
            jax.ShapeDtypeStruct((rows, d), jnp.bfloat16),
        ),
        in_specs=[
            pl.BlockSpec((rows, block), lambda i: (0, jnp.minimum(i, n - 1))),
            pl.BlockSpec((rows, block), lambda i: (0, jnp.minimum(i, n - 1))),
            pl.BlockSpec((block, 2 * room), lambda i: (jnp.minimum(i, n - 1), 0)),
            pl.BlockSpec((block, room), lambda i: (jnp.maximum(i - n, 0), 2)),
        ],
        out_specs=(
            pl.BlockSpec((rows, block), lambda i: (0, jnp.maximum(i - n, 0))),
            pl.BlockSpec((rows, block), lambda i: (0, jnp.maximum(i - n, 0))),
        ),
        scratch_shapes=[
            pltpu.VMEM((2 * rows, room), jnp.float32),
            pltpu.VMEM((2 * rows, room), jnp.float32),
            pltpu.VMEM((2 * rows, room), jnp.bfloat16),
        ],
        compiler_params=pltpu.CompilerParams(vmem_limit_bytes=24 * MIB),
        name="mixer",
    )(here, there, weights, weights)


def shards(
    residual,
    query_small,
    query_large,
    latent,
    rope_key,
    key_up_small,
    value_up_small,
    key_up_large,
    value_up_large,
    out_small,
    out_large,
    norm_gain,
    gate_weight,
    up_weight,
    down_weight,
):
    n_y = lax.axis_size(("yh", "yl"))
    z = lax.axis_index("z")
    y = lax.axis_index(("yh", "yl"))
    x = lax.axis_index("x")
    c = lax.axis_index("c")
    row_count = query_small.shape[0]
    rows, d = residual.shape
    place = jnp.stack([z, y, x, x * 2 + c, c]).astype(jnp.int32)

    chunks = pack_weights(gate_weight, up_weight, down_weight, n_y)
    over_y = exchanged(chunks, ("yh", "yl"))
    weights = lax.all_gather(
        over_y.reshape(-1, over_y.shape[2]), "z", axis=0, tiled=True
    )

    positions = (z * n_y + y) * row_count + jnp.arange(row_count, dtype=jnp.int32)
    inverse = 1.0 / rope_base ** (jnp.arange(0, ROPE, 2, dtype=jnp.float32) / ROPE)
    angles = positions.astype(jnp.float32)[:, None] * inverse[None, :]
    cosine = jnp.cos(angles)
    sine = jnp.sin(angles)
    table = jnp.concatenate([cosine, cosine, -sine, sine], axis=1)
    query, packed = prepare(place, query_small, query_large, latent, rope_key, table)
    along_z = from_everyone(packed, "z")
    queries = [query] + [
        lax.ppermute(query, ("yh", "yl"), [(i, (i + k) % n_y) for i in range(n_y)])
        for k in range(1, n_y)
    ]
    full = absorb(place, queries, key_up_small, key_up_large)
    mine = from_everyone(along_z, "x")
    other = partner(mine)

    partial = attention(place, full, mine, other, value_up_small, value_up_large)
    parts = exchanged(partial, ("yh", "yl"))
    mixed_part = merge(parts, out_small, out_large)
    tiles = exchanged(mixed_part.reshape(row_count // rows, rows, d), ("x", "c"))
    mixed = jnp.sum(tiles.astype(jnp.float32), axis=0).astype(jnp.bfloat16)
    stream = (residual.astype(jnp.float32) + mixed.astype(jnp.float32)).astype(jnp.bfloat16)
    as_float = stream.astype(jnp.float32)
    normed = as_float * lax.rsqrt(jnp.mean(as_float * as_float, axis=-1, keepdims=True) + norm_eps)
    normed = (normed * norm_gain.astype(jnp.float32)[None, :]).astype(jnp.bfloat16)

    here = from_everyone(normed, ("yl", "x")).reshape(-1, d)
    there = partner(here)
    part_here, part_there = mixer(here, there, weights)
    sent = partner(part_there)
    both = (part_here + sent.astype(jnp.float32)).astype(jnp.bfloat16)
    pieces = exchanged(both.reshape(-1, rows, d), ("yl", "x"))
    channel = jnp.sum(pieces.astype(jnp.float32), axis=0).astype(jnp.bfloat16)
    return (as_float + 0.5 * channel.astype(jnp.float32)).astype(jnp.bfloat16)


def solution(mesh):
    fine = Mesh(mesh.devices.reshape(-1, 2, 2, 4, 2), ("z", "yh", "yl", "x", "c"))
    sp = ("z", "yh", "yl")
    tp = ("x", "c")
    both = sp + tp
    placed = (
        P(both, None),
        P(sp, tp),
        P(sp, tp),
        P(sp, None),
        P(sp, None),
        P(None, tp),
        P(None, tp),
        P(None, tp),
        P(None, tp),
        P(tp, None),
        P(tp, None),
        P(),
        P(sp, tp),
        P(sp, tp),
        P(sp, tp),
    )
    return jax.shard_map(
        shards, mesh=fine, in_specs=placed, out_specs=P(both, None), check_vma=False
    )
```

time: 187 us -> 181 us (0.968)
  blocking collectives: 48.5 us -> 84 us
  waiting for transfers between devices: 36.4 us -> 14.2 us
  starting transfers between devices: 43.9 us -> 29.9 us
  matrix products: 12.5 us -> 0 us
  Pallas kernels: 16.7 us -> 24.7 us
    all_to_all x1 -> x3, blocking collectives: 19 us -> 51.6 us  [from_everyone(): return lax.all_to_all(copies, axis, split_axis=0, concat_axis=0, tiled=True)]
    all_to_all x2 -> x0, starting transfers between devices: 19.8 us -> none  [from_everyone(): return lax.all_to_all(copies, axis, split_axis=0, concat_axis=0, tiled=True)]
    all_to_all x2 -> x0, waiting for transfers between devices: 18.9 us -> none  [from_everyone(): return lax.all_to_all(copies, axis, split_axis=0, concat_axis=0, tiled=True)]
    dot_general x4 -> x0, matrix products: 12.5 us -> none  [the longest x2 8.31 us: mixer(): lax.dot_general(hidden, down_full, NT, preferred_element_type=jnp.float32)]
    ppermute x0 -> x3, starting transfers between devices: none -> 9 us  [shards(): lax.ppermute(query, ('yh', 'yl'), [(i, (i + k) % n_y) for i in range(n_y)])]
    pallas_call x1 -> x5, Pallas kernels: 14 us -> 22 us  [the longest x1 11.9 us: attention(): pl.pallas_call(attention_kernel, out_shape=jax.ShapeDtypeStruct((n_y, row...]
    unnamed x38 -> x27, local copies, waits for them, and re-layouts: 2.73 us -> 9.45 us
    slice x13 -> x0, local copies, waits for them, and re-layouts: 5.39 us -> none  [the longest x2 1.86 us: shards(): w[:, cut * j:cut * (j + 1)]]
  transfers between devices with their start and end apart: 8 -> 8, of which waited for: 7 -> 4; matrix products, arithmetic and copies ran while one was open for 4% -> 4% of each run, Pallas kernels for 9% -> 10%
where the time goes in v2:
time: 181 us; the launch traced here: 180 us
  blocking collectives  84 us (46%)
  starting transfers between devices  29.9 us (17%)
  Pallas kernels  24.7 us (14%)
  waiting for transfers between devices  14.2 us (8%)
  between operations  13.6 us (8%)
  local copies, waits for them, and re-layouts  10.9 us (6%)
  other arithmetic  2.23 us (1%)
    all_to_all x3, blocking collectives, from_everyone(): return lax.all_to_all(copies, axis, split_axis=0, concat_axis=0, tiled=True)  51.6 us
    all_to_all x3, blocking collectives, exchanged(): return lax.all_to_all(chunks, axis, split_axis=0, concat_axis=0, tiled=True)  32.3 us
    ppermute x3, starting transfers between devices, partner(): return lax.ppermute(x, 'c', [(0, 1), (1, 0)])  14.8 us
    pallas_call x1, Pallas kernels, attention(): pl.pallas_call(attention_kernel, out_shape=jax.ShapeDtypeStruct((n_y, row...  11.9 us
    unnamed x27, local copies, waits for them, and re-layouts  9.45 us
    all_to_all x1, waiting for transfers between devices, exchanged(): return lax.all_to_all(chunks, axis, split_axis=0, concat_axis=0, tiled=True)  9.37 us
    ppermute x3, starting transfers between devices, shards(): lax.ppermute(query, ('yh', 'yl'), [(i, (i + k) % n_y) for i in range(n_y)])  9 us
    all_to_all x1, starting transfers between devices, exchanged(): return lax.all_to_all(chunks, axis, split_axis=0, concat_axis=0, tiled=True)  6.14 us
  transfers between devices with their start and end apart: 8, of which 4 were waited for; matrix products, arithmetic and copies ran while one was open for 4% of the time, Pallas kernels for 10%

profile of v2, /device:TPU:1, one launch (start us, length us, event | category | flops | bytes accessed | tf_op | source)
XLA Modules:
  0.0 179.6 jit_solution(4439758687789953186)
XLA Ops:
  6.5 1.7 pack_weights.1
  8.2 10.8 %all_to_all.35 = bf16[4,32,1152]{2,1,0:T(8,128)(2,1)} all-to-all(bf16[4,32,1152]{2,1,0:T(8,128)(2,1)} %pack_weights.1), channel_id=1, replica_groups=mesh['z'=16,'yh'=2,'yl'=2,'x'=4,'c'=2] {'yh','yl'}, dimensions={0} | all-to-all | bytes 589824 | tf_op jit(solution)/shard_map/all_to_all | solution.py:32
  25.2 1.9 %prepare.1 = (bf16[128,256]{1,0:T(8,128)(2,1)}, bf16[40,128]{1,0:T(8,128)(2,1)}) custom-call(s32[5]{0:T(128)} %stack.23.place, bf16[128,96]{1,0:T(8,128)(2,1)} %copy.22.small, bf16[128,160]{1,0:T(8,128)(2,1)} %copy.23.large, bf16[128,256]{1,0:T(8,128)(2,1)} %latent.1, bf16[128,32]{1,0:T(8,128)(2,1)} %copy.24.rope_key, f32[128,64]{1,0:T(8,128)} %pad_maximum_fusion.table), custom_call_target="tpu_custom_call" | custom-call | tf_op jit(solution)/shard_map/prepare/pallas_call | solution.py:98
  27.8 28.3 %all_to_all.36 = bf16[16,40,128]{2,1,0:T(8,128)(2,1)S(1)} all-to-all(bf16[16,40,128]{2,1,0:T(8,128)(2,1)S(1)} %broadcast_in_dim.6), channel_id=1, replica_groups=mesh['z'=16,'yh'=2,'yl'=2,'x'=4,'c'=2] {'z'}, dimensions={0} | all-to-all | bytes 327680 | tf_op jit(solution)/shard_map/all_to_all | solution.py:28
  56.2 11.7 %all_to_all.37.mine = bf16[4,16,40,128]{3,2,1,0:T(8,128)(2,1)S(1)} all-to-all(bf16[4,16,40,128]{3,2,1,0:T(8,128)(2,1)S(1)} %broadcast_in_dim.14), channel_id=1, replica_groups=mesh['z'=16,'yh'=2,'yl'=2,'x'=4,'c'=2] {'x'}, dimensions={0} | all-to-all | bytes 1310720 | tf_op jit(solution)/shard_map/all_to_all | solution.py:28
  67.9 8.8 %collective-permute-start.3 = (bf16[4,16,40,128]{3,2,1,0:T(8,128)(2,1)S(1)}, bf16[4,16,40,128]{3,2,1,0:T(8,128)(2,1)S(1)}, u32[]{:S(2)}, u32[]{:S(2)}) collective-permute-start(bf16[4,16,40,128]{3,2,1,0:T(8,128)(2,1)S(1)} %all_to_all.37.mine), channel_id=1, source_target_pairs={{0,1},{1,0},{2,3},{3,2},{4,5},{5,4},{6,7},{7,6},{8,9},{9,8},{10,11... | collective-permute-start | bytes 1966088 | tf_op jit(solution)/shard_map/ppermute | solution.py:36
  76.6 2.5 %collective-permute-start = (bf16[128,256]{1,0:T(8,128)(2,1)}, bf16[128,256]{1,0:T(8,128)(2,1)S(1)}, u32[]{:S(2)}, u32[]{:S(2)}) collective-permute-start(bf16[128,256]{1,0:T(8,128)(2,1)} %get-tuple-element.9.refs_0_), channel_id=1, source_target_pairs={{0,8},{8,16},{16,24},{24,0},{1,9},{9,17},{17,25},{25,1},{2,10},{10... | collective-permute-start | bytes 196616 | tf_op jit(solution)/shard_map/ppermute | solution.py:349
  79.2 3.6 %collective-permute-start.1 = (bf16[128,256]{1,0:T(8,128)(2,1)}, bf16[128,256]{1,0:T(8,128)(2,1)S(1)}, u32[]{:S(2)}, u32[]{:S(2)}) collective-permute-start(bf16[128,256]{1,0:T(8,128)(2,1)} %get-tuple-element.9.refs_0_), channel_id=1, source_target_pairs={{0,16},{8,24},{16,0},{24,8},{1,17},{9,25},{17,1},{25,9},{2,18},{10... | collective-permute-start | bytes 196616 | tf_op jit(solution)/shard_map/ppermute | solution.py:349
  82.8 2.9 %collective-permute-start.2 = (bf16[128,256]{1,0:T(8,128)(2,1)}, bf16[128,256]{1,0:T(8,128)(2,1)S(1)}, u32[]{:S(2)}, u32[]{:S(2)}) collective-permute-start(bf16[128,256]{1,0:T(8,128)(2,1)} %get-tuple-element.9.refs_0_), channel_id=1, source_target_pairs={{0,24},{8,0},{16,8},{24,16},{1,25},{9,1},{17,9},{25,17},{2,26},{10... | collective-permute-start | bytes 196616 | tf_op jit(solution)/shard_map/ppermute | solution.py:349
  86.6 1.8 %collective-permute-done.2.refs_3_ = bf16[128,256]{1,0:T(8,128)(2,1)S(1)} collective-permute-done((bf16[128,256]{1,0:T(8,128)(2,1)}, bf16[128,256]{1,0:T(8,128)(2,1)S(1)}, u32[]{:S(2)}, u32[]{:S(2)}) %collective-permute-start.2) | collective-permute-done | bytes 65568 | tf_op jit(solution)/shard_map/ppermute | solution.py:349
  89.0 2.3 %absorb.1.query = bf16[4,2,128,512]{3,2,1,0:T(8,128)(2,1)} custom-call(s32[5]{0:T(128)} %stack.23.place, bf16[128,256]{1,0:T(8,128)(2,1)} %get-tuple-element.9.refs_0_, bf16[128,256]{1,0:T(8,128)(2,1)} %copy-done.5, bf16[128,256]{1,0:T(8,128)(2,1)} %copy-done.6, bf16[128,256]{1,0:T(8,128)(2,1)} %copy-done.7, bf16[256,64]{1,0:T(8,128)(2,1)} %copy.25.refs_4_, ...), custom_call_target="tpu_custom_call" | custom-call | tf_op jit(solution)/shard_map/absorb/pallas_call | solution.py:137
  92.6 11.9 %attend.1 = bf16[4,128,256]{2,1,0:T(8,128)(2,1)S(1)} custom-call(s32[5]{0:T(128)S(1)} %copy-done.3, bf16[4,2,128,512]{3,2,1,0:T(8,128)(2,1)S(1)} %copy-done.1, bf16[4,16,40,128]{3,2,1,0:T(8,128)(2,1)S(1)} %all_to_all.37.mine, bf16[4,16,40,128]{3,2,1,0:T(8,128)(2,1)S(1)} %collective-permute-done.3.other, bf16[256,64]{1,0:T(8,128)(2,1)S(1)} %copy.26.value_up_s, ...), custom_call_target="tpu_custom_call" | custom-call | tf_op jit(solution)/shard_map/attend/pallas_call | solution.py:196
  104.5 8.9 %all_to_all.38.parts = bf16[4,128,256]{2,1,0:T(8,128)(2,1)} all-to-all(bf16[4,128,256]{2,1,0:T(8,128)(2,1)S(1)} %attend.1), channel_id=1, replica_groups=mesh['z'=16,'yh'=2,'yl'=2,'x'=4,'c'=2] {'yh','yl'}, dimensions={0} | all-to-all | bytes 524288 | tf_op jit(solution)/shard_map/all_to_all | solution.py:32
  113.4 2.7 %merge.1 = bf16[128,2048]{1,0:T(8,128)(2,1)} custom-call(bf16[4,128,256]{2,1,0:T(8,128)(2,1)} %all_to_all.38.parts, bf16[64,2048]{1,0:T(8,128)(2,1)} %out_s.1, bf16[128,2048]{1,0:T(8,128)(2,1)} %out_l.1), custom_call_target="tpu_custom_call" | custom-call | tf_op jit(solution)/shard_map/merge/pallas_call | solution.py:238
  116.1 6.1 %all-to-all-start.3 = ((bf16[8,16,2048]{2,1,0:T(8,128)(2,1)}), bf16[8,16,2048]{2,1,0:T(8,128)(2,1)S(1)}, u32[]{:S(2)}, u32[]{:S(2)}) async-start(bf16[8,16,2048]{2,1,0:T(8,128)(2,1)} %bitcast.11), calls=%async_computation.3 | async-start | bytes 1048576 | tf_op jit(solution)/shard_map/all_to_all | solution.py:32
  122.3 9.4 %all-to-all-done.3 = bf16[8,16,2048]{2,1,0:T(8,128)(2,1)S(1)} async-done(((bf16[8,16,2048]{2,1,0:T(8,128)(2,1)}), bf16[8,16,2048]{2,1,0:T(8,128)(2,1)S(1)}, u32[]{:S(2)}, u32[]{:S(2)}) %all-to-all-start.3) | async-done | bytes 524320 | tf_op jit(solution)/shard_map/all_to_all | solution.py:32
  132.0 11.6 %all_to_all.39 = bf16[8,16,2048]{2,1,0:T(8,128)(2,1)S(1)} all-to-all(bf16[8,16,2048]{2,1,0:T(8,128)(2,1)S(1)} %broadcast_in_dim.15), channel_id=1, replica_groups=mesh['z'=16,'yh'=2,'yl'=2,'x'=4,'c'=2] {'yl','x'}, dimensions={0} | all-to-all | bytes 1048576 | tf_op jit(solution)/shard_map/all_to_all | solution.py:28
  143.7 3.7 %collective-permute-start.4 = (bf16[128,2048]{1,0:T(8,128)(2,1)S(1)}, bf16[128,2048]{1,0:T(8,128)(2,1)S(1)}, u32[]{:S(2)}, u32[]{:S(2)}) collective-permute-start(bf16[128,2048]{1,0:T(8,128)(2,1)S(1)} %bitcast.9), channel_id=1, source_target_pairs={{0,1},{1,0},{2,3},{3,2},{4,5},{5,4},{6,7},{7,6},{8,9},{9,8},{10,11... | collective-permute-start | bytes 1572872 | tf_op jit(solution)/shard_map/ppermute | solution.py:36
  147.4 1.5 collective-permute-done.4.there
  148.9 2.3 %copy-done = bf16[2048,1152]{1,0:T(8,128)(2,1)S(1)} copy-done((bf16[2048,1152]{1,0:T(8,128)(2,1)S(1)}, bf16[2048,1152]{1,0:T(8,128)(2,1)}, u32[]{:S(2)}) %copy-start) | copy-done | bytes 4718616
  151.2 4.2 %mixer.1 = (f32[128,2048]{1,0:T(8,128)S(1)}, bf16[128,2048]{1,0:T(8,128)(2,1)S(1)}) custom-call(bf16[128,2048]{1,0:T(8,128)(2,1)S(1)} %bitcast.10, bf16[128,2048]{1,0:T(8,128)(2,1)S(1)} %collective-permute-done.4.there, bf16[2048,1152]{1,0:T(8,128)(2,1)S(1)} %copy-done, bf16[2048,1152]{1,0:T(8,128)(2,1)S(1)} %copy-done), custom_call_target="tpu_custom_call" | custom-call | tf_op jit(solution)/shard_map/mixer/pallas_call | solution.py:281
  155.4 2.3 %collective-permute-start.5 = (bf16[128,2048]{1,0:T(8,128)(2,1)S(1)}, bf16[128,2048]{1,0:T(8,128)(2,1)S(1)}, u32[]{:S(2)}, u32[]{:S(2)}) collective-permute-start(bf16[128,2048]{1,0:T(8,128)(2,1)S(1)} %get-tuple-element.12), channel_id=1, source_target_pairs={{0,1},{1,0},{2,3},{3,2},{4,5},{5,4},{6,7},{7,6},{8,9},{9,8},{10,11... | collective-permute-start | bytes 1572872 | tf_op jit(solution)/shard_map/ppermute | solution.py:36
  157.7 1.5 collective-permute-done.5
  159.3 12.6 %all_to_all.40 = bf16[8,16,2048]{2,1,0:T(8,128)(2,1)S(1)} all-to-all(bf16[8,16,2048]{2,1,0:T(8,128)(2,1)S(1)} %bitcast.12), channel_id=1, replica_groups=mesh['z'=16,'yh'=2,'yl'=2,'x'=4,'c'=2] {'yl','x'}, dimensions={0} | all-to-all | bytes 1048576 | tf_op jit(solution)/shard_map/all_to_all | solution.py:32
  (48 shorter events, 10.8 us)
Async XLA Ops:
  6.5 79.1 %copy-start.8 = (bf16[256,64]{0,1:T(8,128)(2,1)S(1)}, bf16[256,64]{0,1:T(8,128)(2,1)}, u32[]{:S(2)}) copy-start(bf16[256,64]{0,1:T(8,128)(2,1)} %param.20) | copy-start | bytes 98308
  6.5 79.9 %copy-start.9 = (bf16[256,64]{0,1:T(8,128)(2,1)S(1)}, bf16[256,64]{0,1:T(8,128)(2,1)}, u32[]{:S(2)}) copy-start(bf16[256,64]{0,1:T(8,128)(2,1)} %param.21) | copy-start | bytes 98308
  6.5 84.8 %copy-start.2 = (bf16[256,128]{1,0:T(8,128)(2,1)S(1)}, bf16[256,128]{1,0:T(8,128)(2,1)}, u32[]{:S(2)}) copy-start(bf16[256,128]{1,0:T(8,128)(2,1)} %value_up_l.1) | copy-start | bytes 196612
  6.5 142.4 %all-gather.2.cloned.1.call-start = ((), (), s32[]{:S(2)}) async-start(), calls=%async_computation.7 | async-start | bytes 5013504 | tf_op jit(solution)/shard_map/all_gather | solution.py:336
  24.1 67.3 %copy-start.3 = (s32[5]{0:T(128)S(1)}, s32[5]{0:T(128)}, u32[]{:S(2)}) copy-start(s32[5]{0:T(128)} %stack.23.place) | copy-start | bytes 64
  56.1 66.1 %copy-start.10 = (bf16[2048]{0:T(1024)(128)(2,1)S(1)}, bf16[2048]{0:T(1024)(128)(2,1)}, u32[]{:S(2)}) copy-start(bf16[2048]{0:T(1024)(128)(2,1)} %param.26) | copy-start | bytes 12292
  56.2 75.5 %copy-start.4 = (bf16[16,2048]{1,0:T(8,128)(2,1)S(1)}, bf16[16,2048]{1,0:T(8,128)(2,1)}, u32[]{:S(2)}) copy-start(bf16[16,2048]{1,0:T(8,128)(2,1)} %param.15) | copy-start | bytes 196612
  67.9 23.5 %collective-permute-start.3 = (bf16[4,16,40,128]{3,2,1,0:T(8,128)(2,1)S(1)}, bf16[4,16,40,128]{3,2,1,0:T(8,128)(2,1)S(1)}, u32[]{:S(2)}, u32[]{:S(2)}) collective-permute-start(bf16[4,16,40,128]{3,2,1,0:T(8,128)(2,1)S(1)} %all_to_all.37.mine), channel_id=1, source_target_pairs={{0,1},{1,0},{2,3},{3,2},{4,5},{5,4},{6,7},{7,6},{8,9},{9,8},{10,11... | collective-permute-start | bytes 1966088 | tf_op jit(solution)/shard_map/ppermute | solution.py:36
  76.6 9.9 %collective-permute-start = (bf16[128,256]{1,0:T(8,128)(2,1)}, bf16[128,256]{1,0:T(8,128)(2,1)S(1)}, u32[]{:S(2)}, u32[]{:S(2)}) collective-permute-start(bf16[128,256]{1,0:T(8,128)(2,1)} %get-tuple-element.9.refs_0_), channel_id=1, source_target_pairs={{0,8},{8,16},{16,24},{24,0},{1,9},{9,17},{17,25},{25,1},{2,10},{10... | collective-permute-start | bytes 196616 | tf_op jit(solution)/shard_map/ppermute | solution.py:349
  79.2 7.4 %collective-permute-start.1 = (bf16[128,256]{1,0:T(8,128)(2,1)}, bf16[128,256]{1,0:T(8,128)(2,1)S(1)}, u32[]{:S(2)}, u32[]{:S(2)}) collective-permute-start(bf16[128,256]{1,0:T(8,128)(2,1)} %get-tuple-element.9.refs_0_), channel_id=1, source_target_pairs={{0,16},{8,24},{16,0},{24,8},{1,17},{9,25},{17,1},{25,9},{2,18},{10... | collective-permute-start | bytes 196616 | tf_op jit(solution)/shard_map/ppermute | solution.py:349
  82.8 5.6 %collective-permute-start.2 = (bf16[128,256]{1,0:T(8,128)(2,1)}, bf16[128,256]{1,0:T(8,128)(2,1)S(1)}, u32[]{:S(2)}, u32[]{:S(2)}) collective-permute-start(bf16[128,256]{1,0:T(8,128)(2,1)} %get-tuple-element.9.refs_0_), channel_id=1, source_target_pairs={{0,24},{8,0},{16,8},{24,16},{1,25},{9,1},{17,9},{25,17},{2,26},{10... | collective-permute-start | bytes 196616 | tf_op jit(solution)/shard_map/ppermute | solution.py:349
  86.5 1.8 %copy-start.5 = (bf16[128,256]{1,0:T(8,128)(2,1)}, bf16[128,256]{1,0:T(8,128)(2,1)S(1)}, u32[]{:S(2)}) copy-start(bf16[128,256]{1,0:T(8,128)(2,1)S(1)} %collective-permute-done.refs_1_) | copy-start | bytes 196612
  86.6 1.8 %copy-start.6 = (bf16[128,256]{1,0:T(8,128)(2,1)}, bf16[128,256]{1,0:T(8,128)(2,1)S(1)}, u32[]{:S(2)}) copy-start(bf16[128,256]{1,0:T(8,128)(2,1)S(1)} %collective-permute-done.1.refs_2_) | copy-start | bytes 196612
  88.4 0.6 copy-start.7
  91.4 1.2 copy-start.1
  116.1 15.5 %all-to-all-start.3 = ((bf16[8,16,2048]{2,1,0:T(8,128)(2,1)}), bf16[8,16,2048]{2,1,0:T(8,128)(2,1)S(1)}, u32[]{:S(2)}, u32[]{:S(2)}) async-start(bf16[8,16,2048]{2,1,0:T(8,128)(2,1)} %bitcast.11), calls=%async_computation.3 | async-start | bytes 1048576 | tf_op jit(solution)/shard_map/all_to_all | solution.py:32
  143.7 5.2 %collective-permute-start.4 = (bf16[128,2048]{1,0:T(8,128)(2,1)S(1)}, bf16[128,2048]{1,0:T(8,128)(2,1)S(1)}, u32[]{:S(2)}, u32[]{:S(2)}) collective-permute-start(bf16[128,2048]{1,0:T(8,128)(2,1)S(1)} %bitcast.9), channel_id=1, source_target_pairs={{0,1},{1,0},{2,3},{3,2},{4,5},{5,4},{6,7},{7,6},{8,9},{9,8},{10,11... | collective-permute-start | bytes 1572872 | tf_op jit(solution)/shard_map/ppermute | solution.py:36
  148.9 2.3 %copy-start = (bf16[2048,1152]{1,0:T(8,128)(2,1)S(1)}, bf16[2048,1152]{1,0:T(8,128)(2,1)}, u32[]{:S(2)}) copy-start(bf16[2048,1152]{1,0:T(8,128)(2,1)} %all-gather.2.cloned.1.call-done.gate_up.down) | copy-start | bytes 14155780
  155.4 3.8 %collective-permute-start.5 = (bf16[128,2048]{1,0:T(8,128)(2,1)S(1)}, bf16[128,2048]{1,0:T(8,128)(2,1)S(1)}, u32[]{:S(2)}, u32[]{:S(2)}) collective-permute-start(bf16[128,2048]{1,0:T(8,128)(2,1)S(1)} %get-tuple-element.12), channel_id=1, source_target_pairs={{0,1},{1,0},{2,3},{3,2},{4,5},{5,4},{6,7},{7,6},{8,9},{9,8},{10,11... | collective-permute-start | bytes 1572872 | tf_op jit(solution)/shard_map/ppermute | solution.py:36
Sparse Core Ops, SparseCore 0:
  19.2 81.6 all-gather.1

commit v3 on v2

--- a/solution.py
+++ b/solution.py
@@ -21,6 +21,13 @@
 MIB = 1024 * 1024
 VMEM = pl.BlockSpec(memory_space=pltpu.VMEM)
 SMEM = pl.BlockSpec(memory_space=pltpu.SMEM)
+
+
+def where_in(place):
+    core = lax.rem(place, 2)
+    x = lax.rem(lax.div(place, 2), 4)
+    y = lax.rem(lax.div(place, 8), 4)
+    return lax.div(place, 32), y, x, core
 
 
 def from_everyone(shard, axis):
@@ -69,49 +76,58 @@
     )(gate, up, down)
 
 
-def prepare_kernel(place, small, large, latent, rope_key, table, query, packed, tall):
-    cosine = table[:, 0:ROPE]
-    sine = table[:, ROPE : 2 * ROPE]
+def prepare_kernel(place, small, large, latent, rope_key, cosine_of, sine_of, query, packed, tall):
+    _, _, x, core = where_in(place[0])
+    half = ROPE // 2
+    cosine = cosine_of[...]
+    sine = sine_of[...]
 
     def turn(v):
         v = v.astype(jnp.float32)
-        swapped = jnp.concatenate([v[:, ROPE // 2 :], v[:, : ROPE // 2]], axis=1)
-        return v * cosine + swapped * sine
-
-    s = small[...].astype(jnp.float32)
-    g = large[...].astype(jnp.float32)
-    turned_s = turn(s[:, HEAD_SMALL:]) * SCALE_SMALL
-    turned_l = turn(g[:, HEAD_LARGE:]) * SCALE_LARGE
-    query[:, 0:128] = large[:, 0:HEAD_LARGE]
-    query[:, 128:256] = jnp.concatenate([s[:, :HEAD_SMALL], turned_s, turned_l], axis=1).astype(
-        jnp.bfloat16
-    )
+        leading = v[0:half, :]
+        trailing = v[half:, :]
+        return jnp.concatenate(
+            [leading * cosine - trailing * sine, trailing * cosine + leading * sine], axis=0
+        )
+
     tall[0:256, :] = latent[...].astype(jnp.float32).T
-    tall[256 : 256 + ROPE, :] = turn(rope_key[...]).astype(jnp.bfloat16).astype(jnp.float32).T
-    mine = tall[pl.ds(pl.multiple_of(32 * place[3], 32), 32), :]
-    ours = tall[pl.ds(pl.multiple_of(256 + 8 * place[2], 8), 8), :]
-    packed[...] = jnp.concatenate([mine, ours], axis=0).astype(jnp.bfloat16)
-
-
-def prepare(place, small, large, latent, rope_key, table):
-    rows = small.shape[0]
+    tall[256 : 256 + ROPE, :] = turn(rope_key[...])
+    mine = tall[pl.ds(pl.multiple_of(64 * x + 32 * core, 32), 32), :]
+    ours = tall[pl.ds(pl.multiple_of(256 + 8 * x, 8), 8), :]
+    piece = jnp.concatenate([mine, ours], axis=0).astype(jnp.bfloat16)
+    for k in range(packed.shape[0]):
+        packed[k] = piece
+    upright = jnp.concatenate(
+        [
+            large[0:HEAD_LARGE, :].astype(jnp.float32),
+            small[0:HEAD_SMALL, :].astype(jnp.float32),
+            turn(small[HEAD_SMALL:, :]) * SCALE_SMALL,
+            turn(large[HEAD_LARGE:, :]) * SCALE_LARGE,
+        ],
+        axis=0,
+    )
+    query[...] = upright.T.astype(jnp.bfloat16)
+
+
+def prepare(place, small, large, latent, rope_key, cosine, sine, n_z):
+    rows = latent.shape[0]
     return pl.pallas_call(
         prepare_kernel,
         out_shape=(
             jax.ShapeDtypeStruct((rows, 256), jnp.bfloat16),
-            jax.ShapeDtypeStruct((40, rows), jnp.bfloat16),
+            jax.ShapeDtypeStruct((n_z, 40, rows), jnp.bfloat16),
         ),
-        in_specs=[SMEM] + [VMEM] * 5,
+        in_specs=[SMEM] + [VMEM] * 6,
         out_specs=(VMEM, VMEM),
         scratch_shapes=[pltpu.VMEM((256 + ROPE, rows), jnp.float32)],
         name="prepare",
-    )(place, small, large, latent, rope_key, table)
+    )(place, small, large, latent, rope_key, cosine, sine)
 
 
 def absorb_kernel(place, *refs):
     *queries, key_up_s, key_up_l, out = refs
     n_y = len(queries)
-    y = place[1]
+    _, y, _, _ = where_in(place[0])
     row = lax.broadcasted_iota(jnp.int32, (128, 128), 0)
     lane = lax.broadcasted_iota(jnp.int32, (128, 128), 1)
     diagonal = jnp.where(row == lane, 1.0, 0.0)
@@ -122,11 +138,11 @@
         own = diagonal if k == 0 else jnp.zeros((128, 128), jnp.float32)
         pick = jnp.where(pick_lane == j, 1.0, 0.0)
         heads = (
-            (q[:, 0:128], q[:, 224:256], key_up_l, SCALE_LARGE),
-            (q[:, 128:192], q[:, 192:224], key_up_s, SCALE_SMALL),
+            (q[:, 0:128], q[:, 224:256], key_up_l[...].T, SCALE_LARGE),
+            (q[:, 128:192], q[:, 192:224], key_up_s[...], SCALE_SMALL),
         )
         for h, (nope, rope, key_up, scale) in enumerate(heads):
-            wide = lax.dot_general(nope, key_up[...], NT, preferred_element_type=jnp.float32)
+            wide = jnp.dot(nope, key_up, preferred_element_type=jnp.float32)
             tail = jnp.concatenate([rope.astype(jnp.float32), pick], axis=1)
             whole = jnp.concatenate([wide * scale, tail, own], axis=1)
             out[j, h, :, :] = whole.astype(jnp.bfloat16)
@@ -144,9 +160,7 @@
 
 
 def attention_kernel(place, query, mine, other, value_up_s, value_up_l, out, keys):
-    z = place[0]
-    y = place[1]
-    c = place[4]
+    z, y, _, c = where_in(place[0])
     n_x, n_z = mine.shape[0], mine.shape[1]
     n_y = query.shape[0]
     row = lax.broadcasted_iota(jnp.int32, (128, 128), 0)
@@ -167,23 +181,26 @@
         keys[384:512, lanes] = later.astype(jnp.bfloat16)
     stat_lane = lax.broadcasted_iota(jnp.int32, (128, 64), 1)
 
-    def head(full, value_up):
-        score = jnp.dot(full, keys[...], preferred_element_type=jnp.float32)
-        top = jnp.max(score, axis=1, keepdims=True)
-        weight = jnp.exp(score - top)
-        total = jnp.sum(weight, axis=1, keepdims=True)
-        summed = lax.dot_general(
-            weight.astype(jnp.bfloat16), keys[0:256, :], NT, preferred_element_type=jnp.float32
+    full = query[...].reshape(n_y * 256, query.shape[3])
+    score = jnp.dot(full, keys[...], preferred_element_type=jnp.float32)
+    tops = jnp.max(score, axis=1, keepdims=True)
+    weight = jnp.exp(score - tops)
+    totals = jnp.sum(weight, axis=1, keepdims=True)
+    summed = lax.dot_general(
+        weight.astype(jnp.bfloat16), keys[0:256, :], NT, preferred_element_type=jnp.float32
+    )
+    summed = (summed / totals).astype(jnp.bfloat16)
+    for j in range(n_y):
+        large = slice(256 * j, 256 * j + 128)
+        small = slice(256 * j + 128, 256 * j + 256)
+        value_l = jnp.dot(summed[large], value_up_l[...], preferred_element_type=jnp.float32)
+        value_s = lax.dot_general(
+            summed[small], value_up_s[...], NT, preferred_element_type=jnp.float32
         )
-        summed = (summed / total).astype(jnp.bfloat16)
-        value = jnp.dot(summed, value_up[...], preferred_element_type=jnp.float32)
-        return value, top, total
-
-    for j in range(n_y):
-        value_l, top_l, total_l = head(query[j, 0], value_up_l)
-        value_s, top_s, total_s = head(query[j, 1], value_up_s)
         stats = jnp.zeros((128, 64), jnp.float32)
-        parts = three_parts(top_l) + three_parts(total_l) + three_parts(top_s) + three_parts(total_s)
+        parts = [
+            p for v in (tops[large], totals[large], tops[small], totals[small]) for p in three_parts(v)
+        ]
         for i, part in enumerate(parts):
             stats = jnp.where(stat_lane == i, part, stats)
         out[j, :, 0:128] = value_l.astype(jnp.bfloat16)
@@ -199,7 +216,7 @@
         in_specs=[SMEM] + [VMEM] * 5,
         out_specs=VMEM,
         scratch_shapes=[pltpu.VMEM((depth, n_keys), jnp.bfloat16)],
-        compiler_params=pltpu.CompilerParams(vmem_limit_bytes=24 * MIB),
+        compiler_params=pltpu.CompilerParams(vmem_limit_bytes=36 * MIB),
         name="attend",
     )(place, query, mine, other, value_up_s, value_up_l)
 
@@ -244,65 +261,30 @@
     )(parts, out_s, out_l)
 
 
-def mixer_kernel(here, there, gate_up, down, out_here, out_there, gate, up, hidden):
-    step = pl.program_id(0)
-    half = pl.num_programs(0) // 2
+def mixer_kernel(here, there, weights, out_here, out_there):
     rows = here.shape[0]
-    room = down.shape[1]
-
-    @pl.when(step == 0)
-    def _():
-        gate[...] = jnp.zeros_like(gate)
-        up[...] = jnp.zeros_like(up)
-
-    @pl.when(step < half)
-    def _():
-        x = jnp.concatenate([here[...], there[...]], axis=0)
-        gate[...] += jnp.dot(x, gate_up[:, 0:room], preferred_element_type=jnp.float32)
-        up[...] += jnp.dot(x, gate_up[:, room : 2 * room], preferred_element_type=jnp.float32)
-
-    @pl.when(step == half - 1)
-    def _():
-        g = gate[...]
-        hidden[...] = (g / (1.0 + jnp.exp(-g)) * up[...]).astype(jnp.bfloat16)
-
-    @pl.when(step >= half)
-    def _():
-        part = lax.dot_general(hidden[...], down[...], NT, preferred_element_type=jnp.float32)
-        out_here[...] = part[0:rows, :]
-        out_there[...] = part[rows : 2 * rows, :].astype(jnp.bfloat16)
+    room = weights.shape[1] // 3
+    x = jnp.concatenate([here[...], there[...]], axis=0)
+    both = jnp.dot(x, weights[:, 0 : 2 * room], preferred_element_type=jnp.float32)
+    gate = both[:, :room]
+    hidden = (gate / (1.0 + jnp.exp(-gate)) * both[:, room:]).astype(jnp.bfloat16)
+    part = lax.dot_general(hidden, weights[:, 2 * room :], NT, preferred_element_type=jnp.float32)
+    out_here[...] = part[0:rows, :]
+    out_there[...] = part[rows : 2 * rows, :].astype(jnp.bfloat16)
 
 
 def mixer(here, there, weights):
-    rows, d = here.shape
-    room = weights.shape[1] // 3
-    n = 4
-    block = d // n
     return pl.pallas_call(
         mixer_kernel,
-        grid=(2 * n,),
         out_shape=(
-            jax.ShapeDtypeStruct((rows, d), jnp.float32),
-            jax.ShapeDtypeStruct((rows, d), jnp.bfloat16),
+            jax.ShapeDtypeStruct(here.shape, jnp.float32),
+            jax.ShapeDtypeStruct(here.shape, jnp.bfloat16),
         ),
-        in_specs=[
-            pl.BlockSpec((rows, block), lambda i: (0, jnp.minimum(i, n - 1))),
-            pl.BlockSpec((rows, block), lambda i: (0, jnp.minimum(i, n - 1))),
-            pl.BlockSpec((block, 2 * room), lambda i: (jnp.minimum(i, n - 1), 0)),
-            pl.BlockSpec((block, room), lambda i: (jnp.maximum(i - n, 0), 2)),
-        ],
-        out_specs=(
-            pl.BlockSpec((rows, block), lambda i: (0, jnp.maximum(i - n, 0))),
-            pl.BlockSpec((rows, block), lambda i: (0, jnp.maximum(i - n, 0))),
-        ),
-        scratch_shapes=[
-            pltpu.VMEM((2 * rows, room), jnp.float32),
-            pltpu.VMEM((2 * rows, room), jnp.float32),
-            pltpu.VMEM((2 * rows, room), jnp.bfloat16),
-        ],
+        in_specs=[VMEM] * 3,
+        out_specs=(VMEM, VMEM),
         compiler_params=pltpu.CompilerParams(vmem_limit_bytes=24 * MIB),
         name="mixer",
-    )(here, there, weights, weights)
+    )(here, there, weights)
 
 
 def shards(
@@ -329,7 +311,7 @@
     c = lax.axis_index("c")
     row_count = query_small.shape[0]
     rows, d = residual.shape
-    place = jnp.stack([z, y, x, x * 2 + c, c]).astype(jnp.int32)
+    place = (((z * n_y + y) * lax.axis_size("x") + x) * 2 + c).astype(jnp.int32).reshape(1)
 
     chunks = pack_weights(gate_weight, up_weight, down_weight, n_y)
     over_y = exchanged(chunks, ("yh", "yl"))
@@ -339,21 +321,27 @@
 
     positions = (z * n_y + y) * row_count + jnp.arange(row_count, dtype=jnp.int32)
     inverse = 1.0 / rope_base ** (jnp.arange(0, ROPE, 2, dtype=jnp.float32) / ROPE)
-    angles = positions.astype(jnp.float32)[:, None] * inverse[None, :]
-    cosine = jnp.cos(angles)
-    sine = jnp.sin(angles)
-    table = jnp.concatenate([cosine, cosine, -sine, sine], axis=1)
-    query, packed = prepare(place, query_small, query_large, latent, rope_key, table)
-    along_z = from_everyone(packed, "z")
+    angles = positions.astype(jnp.float32)[None, :] * inverse[:, None]
+    query, packed = prepare(
+        place,
+        query_small.T,
+        query_large.T,
+        latent,
+        rope_key.T,
+        jnp.cos(angles),
+        jnp.sin(angles),
+        lax.axis_size("z"),
+    )
+    along_z = exchanged(packed, "z")
     queries = [query] + [
         lax.ppermute(query, ("yh", "yl"), [(i, (i + k) % n_y) for i in range(n_y)])
         for k in range(1, n_y)
     ]
-    full = absorb(place, queries, key_up_small, key_up_large)
+    full = absorb(place, queries, key_up_small.T, key_up_large)
     mine = from_everyone(along_z, "x")
     other = partner(mine)
 
-    partial = attention(place, full, mine, other, value_up_small, value_up_large)
+    partial = attention(place, full, mine, other, value_up_small.T, value_up_large)
     parts = exchanged(partial, ("yh", "yl"))
     mixed_part = merge(parts, out_small, out_large)
     tiles = exchanged(mixed_part.reshape(row_count // rows, rows, d), ("x", "c"))
@@ -364,6 +352,7 @@
     normed = (normed * norm_gain.astype(jnp.float32)[None, :]).astype(jnp.bfloat16)
 
     here = from_everyone(normed, ("yl", "x")).reshape(-1, d)
+    here, weights = lax.optimization_barrier((here, weights))
     there = partner(here)
     part_here, part_there = mixer(here, there, weights)
     sent = partner(part_there)

time: 181 us -> 167 us (0.923)
  Pallas kernels: 24.7 us -> 17.4 us
  local copies, waits for them, and re-layouts: 10.9 us -> 4.34 us
  waiting for transfers between devices: 14.2 us -> 17 us
    all_to_all x3 -> x2, blocking collectives: 51.6 us -> 23.2 us  [from_everyone(): return lax.all_to_all(copies, axis, split_axis=0, concat_axis=0, tiled=True)]
    all_to_all x3 -> x4, blocking collectives: 32.3 us -> 59.2 us  [exchanged(): return lax.all_to_all(chunks, axis, split_axis=0, concat_axis=0, tiled=True)]
    unnamed x27 -> x18, local copies, waits for them, and re-layouts: 9.45 us -> 4.21 us
    pallas_call x1, Pallas kernels: 11.9 us -> 6.94 us  [attention(): pl.pallas_call(attention_kernel, out_shape=jax.ShapeDtypeStruct((n_y, row...]
    ppermute x3, waiting for transfers between devices: 1.81 us -> 4.61 us  [shards(): lax.ppermute(query, ('yh', 'yl'), [(i, (i + k) % n_y) for i in range(n_y)])]
    pallas_call x1, Pallas kernels: 4.17 us -> 2.14 us  [mixer(): pl.pallas_call(mixer_kernel, out_shape=(jax.ShapeDtypeStruct(here.shape,...]
  transfers between devices with their start and end apart: 8 -> 8, of which waited for: 4 -> 5; matrix products, arithmetic and copies ran while one was open for 4% -> 1% of each run, Pallas kernels for 10% -> 8%
where the time goes in v3:
time: 167 us; the launch traced here: 166 us
  blocking collectives  82.5 us (49%)
  starting transfers between devices  29.2 us (17%)
  Pallas kernels  17.4 us (10%)
  waiting for transfers between devices  17 us (10%)
  between operations  13.6 us (8%)
  local copies, waits for them, and re-layouts  4.34 us (3%)
  other arithmetic  1.9 us (1%)
    all_to_all x4, blocking collectives, exchanged(): return lax.all_to_all(chunks, axis, split_axis=0, concat_axis=0, tiled=True)  59.2 us
    all_to_all x2, blocking collectives, from_everyone(): return lax.all_to_all(copies, axis, split_axis=0, concat_axis=0, tiled=True)  23.2 us
    ppermute x3, starting transfers between devices, partner(): return lax.ppermute(x, 'c', [(0, 1), (1, 0)])  16.2 us
    all_to_all x1, waiting for transfers between devices, exchanged(): return lax.all_to_all(chunks, axis, split_axis=0, concat_axis=0, tiled=True)  9.37 us
    ppermute x3, starting transfers between devices, shards(): lax.ppermute(query, ('yh', 'yl'), [(i, (i + k) % n_y) for i in range(n_y)])  7.2 us
    pallas_call x1, Pallas kernels, attention(): pl.pallas_call(attention_kernel, out_shape=jax.ShapeDtypeStruct((n_y, row...  6.94 us
    all_to_all x1, starting transfers between devices, exchanged(): return lax.all_to_all(chunks, axis, split_axis=0, concat_axis=0, tiled=True)  5.78 us
    ppermute x3, waiting for transfers between devices, shards(): lax.ppermute(query, ('yh', 'yl'), [(i, (i + k) % n_y) for i in range(n_y)])  4.61 us
  transfers between devices with their start and end apart: 8, of which 5 were waited for; matrix products, arithmetic and copies ran while one was open for 1% of the time, Pallas kernels for 8%

profile of v3, /device:TPU:1, one launch (start us, length us, event | category | flops | bytes accessed | tf_op | source)
XLA Modules:
  0.0 165.9 jit_solution(14922800294918553869)
XLA Ops:
  6.5 1.7 %pack_weights.1 = bf16[4,32,1152]{2,1,0:T(8,128)(2,1)} custom-call(bf16[32,704]{1,0:T(8,128)(2,1)} %gate.1, bf16[32,704]{1,0:T(8,128)(2,1)} %up.1, bf16[32,704]{1,0:T(8,128)(2,1)} %down.1), custom_call_target="tpu_custom_call" | custom-call | tf_op jit(solution)/shard_map/pack_weights/pallas_call | solution.py:70
  8.2 10.8 %all_to_all.35 = bf16[4,32,1152]{2,1,0:T(8,128)(2,1)} all-to-all(bf16[4,32,1152]{2,1,0:T(8,128)(2,1)} %pack_weights.1), channel_id=1, replica_groups=mesh['z'=16,'yh'=2,'yl'=2,'x'=4,'c'=2] {'yh','yl'}, dimensions={0} | all-to-all | bytes 589824 | tf_op jit(solution)/shard_map/all_to_all | solution.py:39
  19.8 1.7 %prepare.1 = (bf16[128,256]{1,0:T(8,128)(2,1)}, bf16[16,40,128]{2,1,0:T(8,128)(2,1)}) custom-call(s32[1]{0:T(128)} %bitcast.place, bf16[96,128]{1,0:T(8,128)(2,1)} %bitcast.18, bf16[160,128]{1,0:T(8,128)(2,1)} %bitcast.16, bf16[128,256]{1,0:T(8,128)(2,1)} %latent.1, bf16[32,128]{1,0:T(8,128)(2,1)} %bitcast.19, f32[16,128]{1,0:T(8,128)} %get-tuple-element.18.cosine_of, ...), custom_call_target="tpu_custom_call" | custom-call | tf_op jit(solution)/shard_map/prepare/pallas_call | solution.py:114
  21.5 27.2 %all_to_all.36 = bf16[16,40,128]{2,1,0:T(8,128)(2,1)S(1)} all-to-all(bf16[16,40,128]{2,1,0:T(8,128)(2,1)} %get-tuple-element.12), channel_id=1, replica_groups=mesh['z'=16,'yh'=2,'yl'=2,'x'=4,'c'=2] {'z'}, dimensions={0} | all-to-all | bytes 327680 | tf_op jit(solution)/shard_map/all_to_all | solution.py:39
  48.8 11.6 %all_to_all.37.mine = bf16[4,16,40,128]{3,2,1,0:T(8,128)(2,1)S(1)} all-to-all(bf16[4,16,40,128]{3,2,1,0:T(8,128)(2,1)S(1)} %broadcast_in_dim.4), channel_id=1, replica_groups=mesh['z'=16,'yh'=2,'yl'=2,'x'=4,'c'=2] {'x'}, dimensions={0} | all-to-all | bytes 1310720 | tf_op jit(solution)/shard_map/all_to_all | solution.py:35
  60.4 10.2 %collective-permute-start.3 = (bf16[4,16,40,128]{3,2,1,0:T(8,128)(2,1)S(1)}, bf16[4,16,40,128]{3,2,1,0:T(8,128)(2,1)S(1)}, u32[]{:S(2)}, u32[]{:S(2)}) collective-permute-start(bf16[4,16,40,128]{3,2,1,0:T(8,128)(2,1)S(1)} %all_to_all.37.mine), channel_id=1, source_target_pairs={{0,1},{1,0},{2,3},{3,2},{4,5},{5,4},{6,7},{7,6},{8,9},{9,8},{10,11... | collective-permute-start | bytes 1966088 | tf_op jit(solution)/shard_map/ppermute | solution.py:43
  70.6 1.9 %collective-permute-start.2 = (bf16[128,256]{1,0:T(8,128)(2,1)}, bf16[128,256]{1,0:T(8,128)(2,1)S(1)}, u32[]{:S(2)}, u32[]{:S(2)}) collective-permute-start(bf16[128,256]{1,0:T(8,128)(2,1)} %get-tuple-element.11.refs_0_), channel_id=1, source_target_pairs={{0,24},{8,0},{16,8},{24,16},{1,25},{9,1},{17,9},{25,17},{2,26},{10... | collective-permute-start | bytes 196616 | tf_op jit(solution)/shard_map/ppermute | solution.py:337
  72.5 3.1 %collective-permute-start.1 = (bf16[128,256]{1,0:T(8,128)(2,1)}, bf16[128,256]{1,0:T(8,128)(2,1)S(1)}, u32[]{:S(2)}, u32[]{:S(2)}) collective-permute-start(bf16[128,256]{1,0:T(8,128)(2,1)} %get-tuple-element.11.refs_0_), channel_id=1, source_target_pairs={{0,16},{8,24},{16,0},{24,8},{1,17},{9,25},{17,1},{25,9},{2,18},{10... | collective-permute-start | bytes 196616 | tf_op jit(solution)/shard_map/ppermute | solution.py:337
  75.6 2.2 %collective-permute-start = (bf16[128,256]{1,0:T(8,128)(2,1)}, bf16[128,256]{1,0:T(8,128)(2,1)S(1)}, u32[]{:S(2)}, u32[]{:S(2)}) collective-permute-start(bf16[128,256]{1,0:T(8,128)(2,1)} %get-tuple-element.11.refs_0_), channel_id=1, source_target_pairs={{0,8},{8,16},{16,24},{24,0},{1,9},{9,17},{17,25},{25,1},{2,10},{10... | collective-permute-start | bytes 196616 | tf_op jit(solution)/shard_map/ppermute | solution.py:337
  77.9 1.9 %collective-permute-done.1.refs_2_ = bf16[128,256]{1,0:T(8,128)(2,1)S(1)} collective-permute-done((bf16[128,256]{1,0:T(8,128)(2,1)}, bf16[128,256]{1,0:T(8,128)(2,1)S(1)}, u32[]{:S(2)}, u32[]{:S(2)}) %collective-permute-start.1) | collective-permute-done | bytes 65568 | tf_op jit(solution)/shard_map/ppermute | solution.py:337
  79.8 2.7 %collective-permute-done.refs_1_ = bf16[128,256]{1,0:T(8,128)(2,1)S(1)} collective-permute-done((bf16[128,256]{1,0:T(8,128)(2,1)}, bf16[128,256]{1,0:T(8,128)(2,1)S(1)}, u32[]{:S(2)}, u32[]{:S(2)}) %collective-permute-start) | collective-permute-done | bytes 65568 | tf_op jit(solution)/shard_map/ppermute | solution.py:337
  83.1 2.3 %absorb.1.query = bf16[4,2,128,512]{3,2,1,0:T(8,128)(2,1)} custom-call(s32[1]{0:T(128)} %bitcast.place, bf16[128,256]{1,0:T(8,128)(2,1)} %get-tuple-element.11.refs_0_, bf16[128,256]{1,0:T(8,128)(2,1)} %copy-done.7, bf16[128,256]{1,0:T(8,128)(2,1)} %copy-done.6, bf16[128,256]{1,0:T(8,128)(2,1)} %copy-done.5, bf16[64,256]{1,0:T(8,128)(2,1)} %bitcast.17, ...), custom_call_target="tpu_custom_call" | custom-call | tf_op jit(solution)/shard_map/absorb/pallas_call | solution.py:153
  86.6 6.9 %attend.1 = bf16[4,128,256]{2,1,0:T(8,128)(2,1)S(1)} custom-call(s32[1]{0:T(128)} %bitcast.place, bf16[4,2,128,512]{3,2,1,0:T(8,128)(2,1)S(1)} %copy-done.1, bf16[4,16,40,128]{3,2,1,0:T(8,128)(2,1)S(1)} %all_to_all.37.mine, bf16[4,16,40,128]{3,2,1,0:T(8,128)(2,1)S(1)} %collective-permute-done.3.other, bf16[64,256]{1,0:T(8,128)(2,1)S(1)} %bitcast.12, ...), custom_call_target="tpu_custom_call" | custom-call | tf_op jit(solution)/shard_map/attend/pallas_call | solution.py:213
  93.6 8.6 %all_to_all.38.parts = bf16[4,128,256]{2,1,0:T(8,128)(2,1)} all-to-all(bf16[4,128,256]{2,1,0:T(8,128)(2,1)S(1)} %attend.1), channel_id=1, replica_groups=mesh['z'=16,'yh'=2,'yl'=2,'x'=4,'c'=2] {'yh','yl'}, dimensions={0} | all-to-all | bytes 524288 | tf_op jit(solution)/shard_map/all_to_all | solution.py:39
  102.2 2.7 %merge.1 = bf16[128,2048]{1,0:T(8,128)(2,1)} custom-call(bf16[4,128,256]{2,1,0:T(8,128)(2,1)} %all_to_all.38.parts, bf16[64,2048]{1,0:T(8,128)(2,1)} %out_s.1, bf16[128,2048]{1,0:T(8,128)(2,1)} %out_l.1), custom_call_target="tpu_custom_call" | custom-call | tf_op jit(solution)/shard_map/merge/pallas_call | solution.py:255
  104.8 5.8 %all-to-all-start.3 = ((bf16[8,16,2048]{2,1,0:T(8,128)(2,1)}), bf16[8,16,2048]{2,1,0:T(8,128)(2,1)S(1)}, u32[]{:S(2)}, u32[]{:S(2)}) async-start(bf16[8,16,2048]{2,1,0:T(8,128)(2,1)} %bitcast.13), calls=%async_computation.3 | async-start | bytes 1048576 | tf_op jit(solution)/shard_map/all_to_all | solution.py:39
  110.6 9.4 %all-to-all-done.3 = bf16[8,16,2048]{2,1,0:T(8,128)(2,1)S(1)} async-done(((bf16[8,16,2048]{2,1,0:T(8,128)(2,1)}), bf16[8,16,2048]{2,1,0:T(8,128)(2,1)S(1)}, u32[]{:S(2)}, u32[]{:S(2)}) %all-to-all-start.3) | async-done | bytes 524320 | tf_op jit(solution)/shard_map/all_to_all | solution.py:39
  120.4 11.6 %all_to_all.39 = bf16[8,16,2048]{2,1,0:T(8,128)(2,1)S(1)} all-to-all(bf16[8,16,2048]{2,1,0:T(8,128)(2,1)S(1)} %broadcast_in_dim.5), channel_id=1, replica_groups=mesh['z'=16,'yh'=2,'yl'=2,'x'=4,'c'=2] {'yl','x'}, dimensions={0} | all-to-all | bytes 1048576 | tf_op jit(solution)/shard_map/all_to_all | solution.py:35
  132.0 3.7 %collective-permute-start.4 = (bf16[128,2048]{1,0:T(8,128)(2,1)S(1)}, bf16[128,2048]{1,0:T(8,128)(2,1)S(1)}, u32[]{:S(2)}, u32[]{:S(2)}) collective-permute-start(bf16[128,2048]{1,0:T(8,128)(2,1)S(1)} %bitcast.10), channel_id=1, source_target_pairs={{0,1},{1,0},{2,3},{3,2},{4,5},{5,4},{6,7},{7,6},{8,9},{9,8},{10,11... | collective-permute-start | bytes 1572872 | tf_op jit(solution)/shard_map/ppermute | solution.py:43
  135.8 1.5 collective-permute-done.4.there
  137.3 2.3 %copy-done = bf16[2048,1152]{1,0:T(8,128)(2,1)S(1)} copy-done((bf16[2048,1152]{1,0:T(8,128)(2,1)S(1)}, bf16[2048,1152]{1,0:T(8,128)(2,1)}, u32[]{:S(2)}) %copy-start) | copy-done | bytes 4718616
  139.6 2.1 %mixer.1 = (f32[128,2048]{1,0:T(8,128)S(1)}, bf16[128,2048]{1,0:T(8,128)(2,1)S(1)}) custom-call(bf16[128,2048]{1,0:T(8,128)(2,1)S(1)} %bitcast.11, bf16[128,2048]{1,0:T(8,128)(2,1)S(1)} %collective-permute-done.4.there, bf16[2048,1152]{1,0:T(8,128)(2,1)S(1)} %copy-done), custom_call_target="tpu_custom_call" | custom-call | tf_op jit(solution)/shard_map/mixer/pallas_call | solution.py:277
  141.8 2.3 %collective-permute-start.5 = (bf16[128,2048]{1,0:T(8,128)(2,1)S(1)}, bf16[128,2048]{1,0:T(8,128)(2,1)S(1)}, u32[]{:S(2)}, u32[]{:S(2)}) collective-permute-start(bf16[128,2048]{1,0:T(8,128)(2,1)S(1)} %get-tuple-element.16), channel_id=1, source_target_pairs={{0,1},{1,0},{2,3},{3,2},{4,5},{5,4},{6,7},{7,6},{8,9},{9,8},{10,11... | collective-permute-start | bytes 1572872 | tf_op jit(solution)/shard_map/ppermute | solution.py:43
  145.7 12.6 %all_to_all.40 = bf16[8,16,2048]{2,1,0:T(8,128)(2,1)S(1)} all-to-all(bf16[8,16,2048]{2,1,0:T(8,128)(2,1)S(1)} %bitcast.14), channel_id=1, replica_groups=mesh['z'=16,'yh'=2,'yl'=2,'x'=4,'c'=2] {'yl','x'}, dimensions={0} | all-to-all | bytes 1048576 | tf_op jit(solution)/shard_map/all_to_all | solution.py:39
  (36 shorter events, 5.4 us)
Async XLA Ops:
  6.5 78.8 %copy-start.2 = (bf16[256,128]{1,0:T(8,128)(2,1)S(1)}, bf16[256,128]{1,0:T(8,128)(2,1)}, u32[]{:S(2)}) copy-start(bf16[256,128]{1,0:T(8,128)(2,1)} %value_up_l.1) | copy-start | bytes 196612
  6.5 78.8 %copy-start.3 = (bf16[256,64]{0,1:T(8,128)(2,1)S(1)}, bf16[256,64]{0,1:T(8,128)(2,1)}, u32[]{:S(2)}) copy-start(bf16[256,64]{0,1:T(8,128)(2,1)} %param.21) | copy-start | bytes 98308
  6.5 125.5 %all-gather.2.cloned.1.call-start = ((), (), s32[]{:S(2)}) async-start(), calls=%async_computation.7 | async-start | bytes 5013504 | tf_op jit(solution)/shard_map/all_gather | solution.py:318
  48.7 61.9 %copy-start.8 = (bf16[2048]{0:T(1024)(128)(2,1)S(1)}, bf16[2048]{0:T(1024)(128)(2,1)}, u32[]{:S(2)}) copy-start(bf16[2048]{0:T(1024)(128)(2,1)} %param.26) | copy-start | bytes 12292
  48.8 71.3 %copy-start.4 = (bf16[16,2048]{1,0:T(8,128)(2,1)S(1)}, bf16[16,2048]{1,0:T(8,128)(2,1)}, u32[]{:S(2)}) copy-start(bf16[16,2048]{1,0:T(8,128)(2,1)} %param.15) | copy-start | bytes 196612
  60.4 25.0 %collective-permute-start.3 = (bf16[4,16,40,128]{3,2,1,0:T(8,128)(2,1)S(1)}, bf16[4,16,40,128]{3,2,1,0:T(8,128)(2,1)S(1)}, u32[]{:S(2)}, u32[]{:S(2)}) collective-permute-start(bf16[4,16,40,128]{3,2,1,0:T(8,128)(2,1)S(1)} %all_to_all.37.mine), channel_id=1, source_target_pairs={{0,1},{1,0},{2,3},{3,2},{4,5},{5,4},{6,7},{7,6},{8,9},{9,8},{10,11... | collective-permute-start | bytes 1966088 | tf_op jit(solution)/shard_map/ppermute | solution.py:43
  70.6 7.2 %collective-permute-start.2 = (bf16[128,256]{1,0:T(8,128)(2,1)}, bf16[128,256]{1,0:T(8,128)(2,1)S(1)}, u32[]{:S(2)}, u32[]{:S(2)}) collective-permute-start(bf16[128,256]{1,0:T(8,128)(2,1)} %get-tuple-element.11.refs_0_), channel_id=1, source_target_pairs={{0,24},{8,0},{16,8},{24,16},{1,25},{9,1},{17,9},{25,17},{2,26},{10... | collective-permute-start | bytes 196616 | tf_op jit(solution)/shard_map/ppermute | solution.py:337
  72.5 7.2 %collective-permute-start.1 = (bf16[128,256]{1,0:T(8,128)(2,1)}, bf16[128,256]{1,0:T(8,128)(2,1)S(1)}, u32[]{:S(2)}, u32[]{:S(2)}) collective-permute-start(bf16[128,256]{1,0:T(8,128)(2,1)} %get-tuple-element.11.refs_0_), channel_id=1, source_target_pairs={{0,16},{8,24},{16,0},{24,8},{1,17},{9,25},{17,1},{25,9},{2,18},{10... | collective-permute-start | bytes 196616 | tf_op jit(solution)/shard_map/ppermute | solution.py:337
  75.6 6.9 %collective-permute-start = (bf16[128,256]{1,0:T(8,128)(2,1)}, bf16[128,256]{1,0:T(8,128)(2,1)S(1)}, u32[]{:S(2)}, u32[]{:S(2)}) collective-permute-start(bf16[128,256]{1,0:T(8,128)(2,1)} %get-tuple-element.11.refs_0_), channel_id=1, source_target_pairs={{0,8},{8,16},{16,24},{24,0},{1,9},{9,17},{17,25},{25,1},{2,10},{10... | collective-permute-start | bytes 196616 | tf_op jit(solution)/shard_map/ppermute | solution.py:337
  77.9 4.6 %copy-start.5 = (bf16[128,256]{1,0:T(8,128)(2,1)}, bf16[128,256]{1,0:T(8,128)(2,1)S(1)}, u32[]{:S(2)}) copy-start(bf16[128,256]{1,0:T(8,128)(2,1)S(1)} %collective-permute-done.2.refs_3_) | copy-start | bytes 196612
  79.8 2.7 %copy-start.6 = (bf16[128,256]{1,0:T(8,128)(2,1)}, bf16[128,256]{1,0:T(8,128)(2,1)S(1)}, u32[]{:S(2)}) copy-start(bf16[128,256]{1,0:T(8,128)(2,1)S(1)} %collective-permute-done.1.refs_2_) | copy-start | bytes 196612
  82.5 0.6 copy-start.7
  85.4 1.2 copy-start.1
  104.8 15.2 %all-to-all-start.3 = ((bf16[8,16,2048]{2,1,0:T(8,128)(2,1)}), bf16[8,16,2048]{2,1,0:T(8,128)(2,1)S(1)}, u32[]{:S(2)}, u32[]{:S(2)}) async-start(bf16[8,16,2048]{2,1,0:T(8,128)(2,1)} %bitcast.13), calls=%async_computation.3 | async-start | bytes 1048576 | tf_op jit(solution)/shard_map/all_to_all | solution.py:39
  132.0 5.2 %collective-permute-start.4 = (bf16[128,2048]{1,0:T(8,128)(2,1)S(1)}, bf16[128,2048]{1,0:T(8,128)(2,1)S(1)}, u32[]{:S(2)}, u32[]{:S(2)}) collective-permute-start(bf16[128,2048]{1,0:T(8,128)(2,1)S(1)} %bitcast.10), channel_id=1, source_target_pairs={{0,1},{1,0},{2,3},{3,2},{4,5},{5,4},{6,7},{7,6},{8,9},{9,8},{10,11... | collective-permute-start | bytes 1572872 | tf_op jit(solution)/shard_map/ppermute | solution.py:43
  137.3 2.3 %copy-start = (bf16[2048,1152]{1,0:T(8,128)(2,1)S(1)}, bf16[2048,1152]{1,0:T(8,128)(2,1)}, u32[]{:S(2)}) copy-start(bf16[2048,1152]{1,0:T(8,128)(2,1)} %all-gather.2.cloned.1.call-done.weights) | copy-start | bytes 14155780
  141.8 3.8 %collective-permute-start.5 = (bf16[128,2048]{1,0:T(8,128)(2,1)S(1)}, bf16[128,2048]{1,0:T(8,128)(2,1)S(1)}, u32[]{:S(2)}, u32[]{:S(2)}) collective-permute-start(bf16[128,2048]{1,0:T(8,128)(2,1)S(1)} %get-tuple-element.16), channel_id=1, source_target_pairs={{0,1},{1,0},{2,3},{3,2},{4,5},{5,4},{6,7},{7,6},{8,9},{9,8},{10,11... | collective-permute-start | bytes 1572872 | tf_op jit(solution)/shard_map/ppermute | solution.py:43
Sparse Core Ops, SparseCore 0:
  19.2 79.1 all-gather.1

commit v4 on v3

--- a/solution.py
+++ b/solution.py
@@ -72,6 +72,7 @@
         out_shape=jax.ShapeDtypeStruct((n_y, gate.shape[0], 3 * room), jnp.bfloat16),
         in_specs=[VMEM] * 3,
         out_specs=VMEM,
+        compiler_params=pltpu.CompilerParams(vmem_limit_bytes=4 * MIB),
         name="pack_weights",
     )(gate, up, down)
 
@@ -120,25 +121,44 @@
         in_specs=[SMEM] + [VMEM] * 6,
         out_specs=(VMEM, VMEM),
         scratch_shapes=[pltpu.VMEM((256 + ROPE, rows), jnp.float32)],
+        compiler_params=pltpu.CompilerParams(vmem_limit_bytes=4 * MIB),
         name="prepare",
     )(place, small, large, latent, rope_key, cosine, sine)
 
 
-def absorb_kernel(place, *refs):
-    *queries, key_up_s, key_up_l, out = refs
+def join_kernel(place, *refs):
+    *queries, out = refs
     n_y = len(queries)
+    _, y, _, _ = where_in(place[0])
+    for k, query in enumerate(queries):
+        out[lax.rem(y - k + n_y, n_y)] = query[...]
+
+
+def join(place, queries):
+    return pl.pallas_call(
+        join_kernel,
+        out_shape=jax.ShapeDtypeStruct((len(queries), *queries[0].shape), jnp.bfloat16),
+        in_specs=[SMEM] + [VMEM] * len(queries),
+        out_specs=VMEM,
+        compiler_params=pltpu.CompilerParams(vmem_limit_bytes=4 * MIB),
+        name="join",
+    )(place, *queries)
+
+
+def absorb_kernel(place, query, key_up_s, key_up_l, out):
+    n_y = query.shape[0]
     _, y, _, _ = where_in(place[0])
     row = lax.broadcasted_iota(jnp.int32, (128, 128), 0)
     lane = lax.broadcasted_iota(jnp.int32, (128, 128), 1)
     diagonal = jnp.where(row == lane, 1.0, 0.0)
     pick_lane = lax.broadcasted_iota(jnp.int32, (128, 96), 1)
-    for k, query in enumerate(queries):
-        j = lax.rem(y - k + n_y, n_y)
-        q = query[...]
-        own = diagonal if k == 0 else jnp.zeros((128, 128), jnp.float32)
+    key_up_large = key_up_l[...].T
+    for j in range(n_y):
+        q = query[j]
+        own = jnp.where(y == j, diagonal, 0.0)
         pick = jnp.where(pick_lane == j, 1.0, 0.0)
         heads = (
-            (q[:, 0:128], q[:, 224:256], key_up_l[...].T, SCALE_LARGE),
+            (q[:, 0:128], q[:, 224:256], key_up_large, SCALE_LARGE),
             (q[:, 128:192], q[:, 192:224], key_up_s[...], SCALE_SMALL),
         )
         for h, (nope, rope, key_up, scale) in enumerate(heads):
@@ -148,15 +168,16 @@
             out[j, h, :, :] = whole.astype(jnp.bfloat16)
 
 
-def absorb(place, queries, key_up_s, key_up_l):
-    n_y, rows = len(queries), queries[0].shape[0]
+def absorb(place, query, key_up_s, key_up_l):
+    n_y, rows = query.shape[:2]
     return pl.pallas_call(
         absorb_kernel,
         out_shape=jax.ShapeDtypeStruct((n_y, 2, rows, 512), jnp.bfloat16),
-        in_specs=[SMEM] + [VMEM] * (n_y + 2),
+        in_specs=[SMEM] + [VMEM] * 3,
         out_specs=VMEM,
+        compiler_params=pltpu.CompilerParams(vmem_limit_bytes=8 * MIB),
         name="absorb",
-    )(place, *queries, key_up_s, key_up_l)
+    )(place, query, key_up_s, key_up_l)
 
 
 def attention_kernel(place, query, mine, other, value_up_s, value_up_l, out, keys):
@@ -257,32 +278,65 @@
         out_shape=jax.ShapeDtypeStruct((parts.shape[1], out_s.shape[1]), jnp.bfloat16),
         in_specs=[VMEM] * 3,
         out_specs=VMEM,
+        compiler_params=pltpu.CompilerParams(vmem_limit_bytes=8 * MIB),
         name="merge",
     )(parts, out_s, out_l)
 
 
-def mixer_kernel(here, there, weights, out_here, out_there):
+def mixer_kernel(here, there, weights, out_here, out_there, gate_up, down, arrived):
     rows = here.shape[0]
+    d = weights.shape[0]
     room = weights.shape[1] // 3
+    pieces = arrived.shape[0] - 1
+    block = d // pieces
+    copies = [
+        pltpu.make_async_copy(
+            weights.at[pl.ds(block * i, block), pl.ds(0, 2 * room)],
+            gate_up.at[pl.ds(block * i, block), :],
+            arrived.at[i],
+        )
+        for i in range(pieces)
+    ]
+    copies.append(
+        pltpu.make_async_copy(weights.at[:, pl.ds(2 * room, room)], down, arrived.at[pieces])
+    )
+    for copy in copies:
+        copy.start()
     x = jnp.concatenate([here[...], there[...]], axis=0)
-    both = jnp.dot(x, weights[:, 0 : 2 * room], preferred_element_type=jnp.float32)
+    both = None
+    for i in range(pieces):
+        copies[i].wait()
+        term = jnp.dot(
+            x[:, block * i : block * (i + 1)],
+            gate_up[block * i : block * (i + 1), :],
+            preferred_element_type=jnp.float32,
+        )
+        both = term if both is None else both + term
     gate = both[:, :room]
     hidden = (gate / (1.0 + jnp.exp(-gate)) * both[:, room:]).astype(jnp.bfloat16)
-    part = lax.dot_general(hidden, weights[:, 2 * room :], NT, preferred_element_type=jnp.float32)
+    copies[pieces].wait()
+    part = lax.dot_general(hidden, down[...], NT, preferred_element_type=jnp.float32)
     out_here[...] = part[0:rows, :]
     out_there[...] = part[rows : 2 * rows, :].astype(jnp.bfloat16)
 
 
 def mixer(here, there, weights):
+    d = weights.shape[0]
+    room = weights.shape[1] // 3
     return pl.pallas_call(
         mixer_kernel,
         out_shape=(
             jax.ShapeDtypeStruct(here.shape, jnp.float32),
             jax.ShapeDtypeStruct(here.shape, jnp.bfloat16),
         ),
-        in_specs=[VMEM] * 3,
+        in_specs=[VMEM] * 2 + [pl.BlockSpec(memory_space=pltpu.HBM)],
         out_specs=(VMEM, VMEM),
-        compiler_params=pltpu.CompilerParams(vmem_limit_bytes=24 * MIB),
+        scratch_shapes=[
+            pltpu.VMEM((d, 2 * room), jnp.bfloat16),
+            pltpu.VMEM((d, room), jnp.bfloat16),
+            pltpu.SemaphoreType.DMA((5,)),
+        ],
+        compiler_params=pltpu.CompilerParams(vmem_limit_bytes=52 * MIB),
         name="mixer",
     )(here, there, weights)
 
@@ -337,7 +391,7 @@
         lax.ppermute(query, ("yh", "yl"), [(i, (i + k) % n_y) for i in range(n_y)])
         for k in range(1, n_y)
     ]
-    full = absorb(place, queries, key_up_small.T, key_up_large)
+    full = absorb(place, join(place, queries), key_up_small.T, key_up_large)
     mine = from_everyone(along_z, "x")
     other = partner(mine)
 

time: 167 us -> 167 us (level)
  Pallas kernels: 17.4 us -> 13.8 us
  local copies, waits for them, and re-layouts: 4.34 us -> 7.26 us
    unnamed x18 -> x30, local copies, waits for them, and re-layouts: 4.21 us -> 7.14 us
    pallas_call x1, Pallas kernels: 2.14 us -> 4.72 us  [mixer(): pl.pallas_call(mixer_kernel, out_shape=(jax.ShapeDtypeStruct(here.shape,...]
    pallas_call x1, Pallas kernels: 2.28 us -> 0.28 us  [absorb(): pl.pallas_call(absorb_kernel, out_shape=jax.ShapeDtypeStruct((n_y, 2, row...]
  transfers between devices with their start and end apart: 8 -> 8, of which waited for: 5 -> 5; matrix products, arithmetic and copies ran while one was open for 1% -> 0% of each run, Pallas kernels for 8% -> 5%
where the time goes in v4:
time: 167 us; the launch traced here: 166 us
  blocking collectives  81.6 us (49%)
  starting transfers between devices  29.7 us (18%)
  waiting for transfers between devices  17.1 us (10%)
  Pallas kernels  13.8 us (8%)
  between operations  13.6 us (8%)
  local copies, waits for them, and re-layouts  7.26 us (4%)
  other arithmetic  2.51 us (2%)
    all_to_all x4, blocking collectives, exchanged(): return lax.all_to_all(chunks, axis, split_axis=0, concat_axis=0, tiled=True)  58.3 us
    all_to_all x2, blocking collectives, from_everyone(): return lax.all_to_all(copies, axis, split_axis=0, concat_axis=0, tiled=True)  23.2 us
    ppermute x3, starting transfers between devices, partner(): return lax.ppermute(x, 'c', [(0, 1), (1, 0)])  15.8 us
    all_to_all x1, waiting for transfers between devices, exchanged(): return lax.all_to_all(chunks, axis, split_axis=0, concat_axis=0, tiled=True)  9.37 us
    ppermute x3, starting transfers between devices, shards(): lax.ppermute(query, ('yh', 'yl'), [(i, (i + k) % n_y) for i in range(n_y)])  8.15 us
    unnamed x30, local copies, waits for them, and re-layouts  7.14 us
    pallas_call x1, Pallas kernels, attention(): pl.pallas_call(attention_kernel, out_shape=jax.ShapeDtypeStruct((n_y, row...  7.06 us
    all_to_all x1, starting transfers between devices, exchanged(): return lax.all_to_all(chunks, axis, split_axis=0, concat_axis=0, tiled=True)  5.79 us
  transfers between devices with their start and end apart: 8, of which 5 were waited for; matrix products, arithmetic and copies ran while one was open for 0% of the time, Pallas kernels for 5%

profile of v4, /device:TPU:1, one launch (start us, length us, event | category | flops | bytes accessed | tf_op | source)
XLA Modules:
  0.0 165.6 jit_solution(7079470906303297170)
XLA Ops:
  6.5 0.9 copy-done.5
  9.1 10.6 %all_to_all.35 = bf16[4,32,1152]{2,1,0:T(8,128)(2,1)} all-to-all(bf16[4,32,1152]{2,1,0:T(8,128)(2,1)S(1)} %pack_weights.1), channel_id=1, replica_groups=mesh['z'=16,'yh'=2,'yl'=2,'x'=4,'c'=2] {'yh','yl'}, dimensions={0} | all-to-all | bytes 589824 | tf_op jit(solution)/shard_map/all_to_all | solution.py:39
  19.9 0.8 copy-done.4
  23.1 27.1 %all_to_all.36 = bf16[16,40,128]{2,1,0:T(8,128)(2,1)S(1)} all-to-all(bf16[16,40,128]{2,1,0:T(8,128)(2,1)S(1)} %get-tuple-element.12), channel_id=1, replica_groups=mesh['z'=16,'yh'=2,'yl'=2,'x'=4,'c'=2] {'z'}, dimensions={0} | all-to-all | bytes 327680 | tf_op jit(solution)/shard_map/all_to_all | solution.py:39
  50.3 11.6 %all_to_all.37.mine = bf16[4,16,40,128]{3,2,1,0:T(8,128)(2,1)S(1)} all-to-all(bf16[4,16,40,128]{3,2,1,0:T(8,128)(2,1)S(1)} %broadcast_in_dim.4), channel_id=1, replica_groups=mesh['z'=16,'yh'=2,'yl'=2,'x'=4,'c'=2] {'x'}, dimensions={0} | all-to-all | bytes 1310720 | tf_op jit(solution)/shard_map/all_to_all | solution.py:35
  61.9 9.8 %collective-permute-start.3 = (bf16[4,16,40,128]{3,2,1,0:T(8,128)(2,1)S(1)}, bf16[4,16,40,128]{3,2,1,0:T(8,128)(2,1)S(1)}, u32[]{:S(2)}, u32[]{:S(2)}) collective-permute-start(bf16[4,16,40,128]{3,2,1,0:T(8,128)(2,1)S(1)} %all_to_all.37.mine), channel_id=1, source_target_pairs={{0,1},{1,0},{2,3},{3,2},{4,5},{5,4},{6,7},{7,6},{8,9},{9,8},{10,11... | collective-permute-start | bytes 1966088 | tf_op jit(solution)/shard_map/ppermute | solution.py:43
  71.7 2.2 %collective-permute-start.2 = (bf16[128,256]{1,0:T(8,128)(2,1)S(1)}, bf16[128,256]{1,0:T(8,128)(2,1)S(1)}, u32[]{:S(2)}, u32[]{:S(2)}) collective-permute-start(bf16[128,256]{1,0:T(8,128)(2,1)S(1)} %get-tuple-element.11.refs_0_), channel_id=1, source_target_pairs={{0,24},{8,0},{16,8},{24,16},{1,25},{9,1},{17,9},{25,17},{2,26},{10... | collective-permute-start | bytes 196616 | tf_op jit(solution)/shard_map/ppermute | solution.py:391
  73.9 4.0 %collective-permute-start.1 = (bf16[128,256]{1,0:T(8,128)(2,1)S(1)}, bf16[128,256]{1,0:T(8,128)(2,1)S(1)}, u32[]{:S(2)}, u32[]{:S(2)}) collective-permute-start(bf16[128,256]{1,0:T(8,128)(2,1)S(1)} %get-tuple-element.11.refs_0_), channel_id=1, source_target_pairs={{0,16},{8,24},{16,0},{24,8},{1,17},{9,25},{17,1},{25,9},{2,18},{10... | collective-permute-start | bytes 196616 | tf_op jit(solution)/shard_map/ppermute | solution.py:391
  77.9 1.9 %collective-permute-start = (bf16[128,256]{1,0:T(8,128)(2,1)S(1)}, bf16[128,256]{1,0:T(8,128)(2,1)S(1)}, u32[]{:S(2)}, u32[]{:S(2)}) collective-permute-start(bf16[128,256]{1,0:T(8,128)(2,1)S(1)} %get-tuple-element.11.refs_0_), channel_id=1, source_target_pairs={{0,8},{8,16},{16,24},{24,0},{1,9},{9,17},{17,25},{25,1},{2,10},{10... | collective-permute-start | bytes 196616 | tf_op jit(solution)/shard_map/ppermute | solution.py:391
  80.4 4.1 %collective-permute-done.refs_1_ = bf16[128,256]{1,0:T(8,128)(2,1)S(1)} collective-permute-done((bf16[128,256]{1,0:T(8,128)(2,1)S(1)}, bf16[128,256]{1,0:T(8,128)(2,1)S(1)}, u32[]{:S(2)}, u32[]{:S(2)}) %collective-permute-start) | collective-permute-done | bytes 65568 | tf_op jit(solution)/shard_map/ppermute | solution.py:391
  84.6 0.8 copy-done.2
  86.5 7.1 %attend.1 = bf16[4,128,256]{2,1,0:T(8,128)(2,1)S(1)} custom-call(s32[1]{0:T(128)} %bitcast.place, bf16[4,2,128,512]{3,2,1,0:T(8,128)(2,1)S(1)} %absorb.1.query, bf16[4,16,40,128]{3,2,1,0:T(8,128)(2,1)S(1)} %all_to_all.37.mine, bf16[4,16,40,128]{3,2,1,0:T(8,128)(2,1)S(1)} %collective-permute-done.3.other, bf16[64,256]{1,0:T(8,128)(2,1)S(1)} %bitcast.13, ...), custom_call_target="tpu_custom_call" | custom-call | tf_op jit(solution)/shard_map/attend/pallas_call | solution.py:234
  93.6 8.0 %all_to_all.38.parts = bf16[4,128,256]{2,1,0:T(8,128)(2,1)S(1)} all-to-all(bf16[4,128,256]{2,1,0:T(8,128)(2,1)S(1)} %attend.1), channel_id=1, replica_groups=mesh['z'=16,'yh'=2,'yl'=2,'x'=4,'c'=2] {'yh','yl'}, dimensions={0} | all-to-all | bytes 524288 | tf_op jit(solution)/shard_map/all_to_all | solution.py:39
  101.6 1.5 merge.1
  103.0 5.8 %all-to-all-start.3 = ((bf16[8,16,2048]{2,1,0:T(8,128)(2,1)}), bf16[8,16,2048]{2,1,0:T(8,128)(2,1)S(1)}, u32[]{:S(2)}, u32[]{:S(2)}) async-start(bf16[8,16,2048]{2,1,0:T(8,128)(2,1)} %bitcast.6), calls=%async_computation.3 | async-start | bytes 1048576 | tf_op jit(solution)/shard_map/all_to_all | solution.py:39
  108.8 9.4 %all-to-all-done.3 = bf16[8,16,2048]{2,1,0:T(8,128)(2,1)S(1)} async-done(((bf16[8,16,2048]{2,1,0:T(8,128)(2,1)}), bf16[8,16,2048]{2,1,0:T(8,128)(2,1)S(1)}, u32[]{:S(2)}, u32[]{:S(2)}) %all-to-all-start.3) | async-done | bytes 524320 | tf_op jit(solution)/shard_map/all_to_all | solution.py:39
  118.6 11.6 %all_to_all.39 = bf16[8,16,2048]{2,1,0:T(8,128)(2,1)S(1)} all-to-all(bf16[8,16,2048]{2,1,0:T(8,128)(2,1)S(1)} %broadcast_in_dim.5), channel_id=1, replica_groups=mesh['z'=16,'yh'=2,'yl'=2,'x'=4,'c'=2] {'yl','x'}, dimensions={0} | all-to-all | bytes 1048576 | tf_op jit(solution)/shard_map/all_to_all | solution.py:35
  130.2 3.7 %collective-permute-start.4 = (bf16[128,2048]{1,0:T(8,128)(2,1)S(1)}, bf16[128,2048]{1,0:T(8,128)(2,1)S(1)}, u32[]{:S(2)}, u32[]{:S(2)}) collective-permute-start(bf16[128,2048]{1,0:T(8,128)(2,1)S(1)} %bitcast.10), channel_id=1, source_target_pairs={{0,1},{1,0},{2,3},{3,2},{4,5},{5,4},{6,7},{7,6},{8,9},{9,8},{10,11... | collective-permute-start | bytes 1572872 | tf_op jit(solution)/shard_map/ppermute | solution.py:43
  134.0 1.5 collective-permute-done.4.there
  135.5 4.7 %mixer.1 = (f32[128,2048]{1,0:T(8,128)}, bf16[128,2048]{1,0:T(8,128)(2,1)S(1)}) custom-call(bf16[128,2048]{1,0:T(8,128)(2,1)S(1)} %bitcast.11, bf16[128,2048]{1,0:T(8,128)(2,1)S(1)} %collective-permute-done.4.there, bf16[2048,1152]{1,0:T(8,128)(2,1)} %all-gather.2.cloned.1.call-done.weights), custom_call_target="tpu_custom_call" | custom-call | tf_op jit(solution)/shard_map/mixer/pallas_call | solution.py:326
  140.2 2.3 %collective-permute-start.5 = (bf16[128,2048]{1,0:T(8,128)(2,1)S(1)}, bf16[128,2048]{1,0:T(8,128)(2,1)S(1)}, u32[]{:S(2)}, u32[]{:S(2)}) collective-permute-start(bf16[128,2048]{1,0:T(8,128)(2,1)S(1)} %get-tuple-element.16), channel_id=1, source_target_pairs={{0,1},{1,0},{2,3},{3,2},{4,5},{5,4},{6,7},{7,6},{8,9},{9,8},{10,11... | collective-permute-start | bytes 1572872 | tf_op jit(solution)/shard_map/ppermute | solution.py:43
  142.5 1.5 collective-permute-done.5
  144.0 1.3 add_convert_fusion
  145.3 12.6 %all_to_all.40 = bf16[8,16,2048]{2,1,0:T(8,128)(2,1)S(1)} all-to-all(bf16[8,16,2048]{2,1,0:T(8,128)(2,1)S(1)} %bitcast.17), channel_id=1, replica_groups=mesh['z'=16,'yh'=2,'yl'=2,'x'=4,'c'=2] {'yl','x'}, dimensions={0} | all-to-all | bytes 1048576 | tf_op jit(solution)/shard_map/all_to_all | solution.py:39
  (49 shorter events, 7.0 us)
Async XLA Ops:
  6.5 80.0 %copy-start.3 = (bf16[256,128]{1,0:T(8,128)(2,1)S(1)}, bf16[256,128]{1,0:T(8,128)(2,1)}, u32[]{:S(2)}) copy-start(bf16[256,128]{1,0:T(8,128)(2,1)} %value_up_l.1) | copy-start | bytes 196612
  6.5 95.0 %copy-start = (bf16[128,2048]{1,0:T(8,128)(2,1)S(1)}, bf16[128,2048]{1,0:T(8,128)(2,1)}, u32[]{:S(2)}) copy-start(bf16[128,2048]{1,0:T(8,128)(2,1)} %out_l.1) | copy-start | bytes 1572868
  6.5 95.0 %copy-start.1 = (bf16[64,2048]{1,0:T(8,128)(2,1)S(1)}, bf16[64,2048]{1,0:T(8,128)(2,1)}, u32[]{:S(2)}) copy-start(bf16[64,2048]{1,0:T(8,128)(2,1)} %out_s.1) | copy-start | bytes 786436
  6.5 123.7 %all-gather.2.cloned.1.call-start = ((), (), s32[]{:S(2)}) async-start(), calls=%async_computation.7 | async-start | bytes 5013504 | tf_op jit(solution)/shard_map/all_gather | solution.py:372
  6.5 0.9 copy-start.5
  7.4 0.8 copy-start.6
  8.2 0.8 copy-start.7
  9.0 77.5 %copy-start.9 = (bf16[256,64]{0,1:T(8,128)(2,1)S(1)}, bf16[256,64]{0,1:T(8,128)(2,1)}, u32[]{:S(2)}) copy-start(bf16[256,64]{0,1:T(8,128)(2,1)} %param.21) | copy-start | bytes 98308
  19.9 0.8 copy-start.4
  20.8 0.8 copy-start.8
  21.5 0.7 copy-start.11
  22.3 0.7 copy-start.12
  50.3 58.5 %copy-start.14 = (bf16[2048]{0:T(1024)(128)(2,1)S(1)}, bf16[2048]{0:T(1024)(128)(2,1)}, u32[]{:S(2)}) copy-start(bf16[2048]{0:T(1024)(128)(2,1)} %param.26) | copy-start | bytes 12292
  50.3 68.0 %copy-start.13 = (bf16[16,2048]{1,0:T(8,128)(2,1)S(1)}, bf16[16,2048]{1,0:T(8,128)(2,1)}, u32[]{:S(2)}) copy-start(bf16[16,2048]{1,0:T(8,128)(2,1)} %param.15) | copy-start | bytes 196612
  61.9 24.6 %collective-permute-start.3 = (bf16[4,16,40,128]{3,2,1,0:T(8,128)(2,1)S(1)}, bf16[4,16,40,128]{3,2,1,0:T(8,128)(2,1)S(1)}, u32[]{:S(2)}, u32[]{:S(2)}) collective-permute-start(bf16[4,16,40,128]{3,2,1,0:T(8,128)(2,1)S(1)} %all_to_all.37.mine), channel_id=1, source_target_pairs={{0,1},{1,0},{2,3},{3,2},{4,5},{5,4},{6,7},{7,6},{8,9},{9,8},{10,11... | collective-permute-start | bytes 1966088 | tf_op jit(solution)/shard_map/ppermute | solution.py:43
  71.7 8.2 %collective-permute-start.2 = (bf16[128,256]{1,0:T(8,128)(2,1)S(1)}, bf16[128,256]{1,0:T(8,128)(2,1)S(1)}, u32[]{:S(2)}, u32[]{:S(2)}) collective-permute-start(bf16[128,256]{1,0:T(8,128)(2,1)S(1)} %get-tuple-element.11.refs_0_), channel_id=1, source_target_pairs={{0,24},{8,0},{16,8},{24,16},{1,25},{9,1},{17,9},{25,17},{2,26},{10... | collective-permute-start | bytes 196616 | tf_op jit(solution)/shard_map/ppermute | solution.py:391
  73.9 6.5 %collective-permute-start.1 = (bf16[128,256]{1,0:T(8,128)(2,1)S(1)}, bf16[128,256]{1,0:T(8,128)(2,1)S(1)}, u32[]{:S(2)}, u32[]{:S(2)}) collective-permute-start(bf16[128,256]{1,0:T(8,128)(2,1)S(1)} %get-tuple-element.11.refs_0_), channel_id=1, source_target_pairs={{0,16},{8,24},{16,0},{24,8},{1,17},{9,25},{17,1},{25,9},{2,18},{10... | collective-permute-start | bytes 196616 | tf_op jit(solution)/shard_map/ppermute | solution.py:391
  77.9 6.6 %collective-permute-start = (bf16[128,256]{1,0:T(8,128)(2,1)S(1)}, bf16[128,256]{1,0:T(8,128)(2,1)S(1)}, u32[]{:S(2)}, u32[]{:S(2)}) collective-permute-start(bf16[128,256]{1,0:T(8,128)(2,1)S(1)} %get-tuple-element.11.refs_0_), channel_id=1, source_target_pairs={{0,8},{8,16},{16,24},{24,0},{1,9},{9,17},{17,25},{25,1},{2,10},{10... | collective-permute-start | bytes 196616 | tf_op jit(solution)/shard_map/ppermute | solution.py:391
  84.6 0.8 copy-start.2
  85.4 0.8 copy-start.10
  103.0 15.2 %all-to-all-start.3 = ((bf16[8,16,2048]{2,1,0:T(8,128)(2,1)}), bf16[8,16,2048]{2,1,0:T(8,128)(2,1)S(1)}, u32[]{:S(2)}, u32[]{:S(2)}) async-start(bf16[8,16,2048]{2,1,0:T(8,128)(2,1)} %bitcast.6), calls=%async_computation.3 | async-start | bytes 1048576 | tf_op jit(solution)/shard_map/all_to_all | solution.py:39
  130.2 5.2 %collective-permute-start.4 = (bf16[128,2048]{1,0:T(8,128)(2,1)S(1)}, bf16[128,2048]{1,0:T(8,128)(2,1)S(1)}, u32[]{:S(2)}, u32[]{:S(2)}) collective-permute-start(bf16[128,2048]{1,0:T(8,128)(2,1)S(1)} %bitcast.10), channel_id=1, source_target_pairs={{0,1},{1,0},{2,3},{3,2},{4,5},{5,4},{6,7},{7,6},{8,9},{9,8},{10,11... | collective-permute-start | bytes 1572872 | tf_op jit(solution)/shard_map/ppermute | solution.py:43
  140.2 3.8 %collective-permute-start.5 = (bf16[128,2048]{1,0:T(8,128)(2,1)S(1)}, bf16[128,2048]{1,0:T(8,128)(2,1)S(1)}, u32[]{:S(2)}, u32[]{:S(2)}) collective-permute-start(bf16[128,2048]{1,0:T(8,128)(2,1)S(1)} %get-tuple-element.16), channel_id=1, source_target_pairs={{0,1},{1,0},{2,3},{3,2},{4,5},{5,4},{6,7},{7,6},{8,9},{9,8},{10,11... | collective-permute-start | bytes 1572872 | tf_op jit(solution)/shard_map/ppermute | solution.py:43
Sparse Core Ops, SparseCore 0:
  19.9 79.7 all-gather.1

commit v5 on v4

--- a/solution.py
+++ b/solution.py
@@ -72,7 +72,6 @@
         out_shape=jax.ShapeDtypeStruct((n_y, gate.shape[0], 3 * room), jnp.bfloat16),
         in_specs=[VMEM] * 3,
         out_specs=VMEM,
-        compiler_params=pltpu.CompilerParams(vmem_limit_bytes=4 * MIB),
         name="pack_weights",
     )(gate, up, down)
 
@@ -283,62 +282,41 @@
     )(parts, out_s, out_l)
 
 
-def mixer_kernel(here, there, weights, out_here, out_there, gate_up, down, arrived):
-    rows = here.shape[0]
-    d = weights.shape[0]
+def fetch_kernel(weights, out, arrived):
+    copy = pltpu.make_async_copy(weights, out, arrived)
+    copy.start()
+    copy.wait()
+
+
+def fetch(weights):
+    return pl.pallas_call(
+        fetch_kernel,
+        out_shape=jax.ShapeDtypeStruct(weights.shape, weights.dtype),
+        in_specs=[pl.BlockSpec(memory_space=pltpu.HBM)],
+        out_specs=VMEM,
+        scratch_shapes=[pltpu.SemaphoreType.DMA],
+        compiler_params=pltpu.CompilerParams(vmem_limit_bytes=46 * MIB),
+        name="fetch",
+    )(weights)
+
+
+def mixer_kernel(rows, weights, out):
     room = weights.shape[1] // 3
-    pieces = arrived.shape[0] - 1
-    block = d // pieces
-    copies = [
-        pltpu.make_async_copy(
-            weights.at[pl.ds(block * i, block), pl.ds(0, 2 * room)],
-            gate_up.at[pl.ds(block * i, block), :],
-            arrived.at[i],
-        )
-        for i in range(pieces)
-    ]
-    copies.append(
-        pltpu.make_async_copy(weights.at[:, pl.ds(2 * room, room)], down, arrived.at[pieces])
-    )
-    for copy in copies:
-        copy.start()
-    x = jnp.concatenate([here[...], there[...]], axis=0)
-    both = None
-    for i in range(pieces):
-        copies[i].wait()
-        term = jnp.dot(
-            x[:, block * i : block * (i + 1)],
-            gate_up[block * i : block * (i + 1), :],
-            preferred_element_type=jnp.float32,
-        )
-        both = term if both is None else both + term
+    both = jnp.dot(rows[...], weights[:, 0 : 2 * room], preferred_element_type=jnp.float32)
     gate = both[:, :room]
     hidden = (gate / (1.0 + jnp.exp(-gate)) * both[:, room:]).astype(jnp.bfloat16)
-    copies[pieces].wait()
-    part = lax.dot_general(hidden, down[...], NT, preferred_element_type=jnp.float32)
-    out_here[...] = part[0:rows, :]
-    out_there[...] = part[rows : 2 * rows, :].astype(jnp.bfloat16)
-
-
-def mixer(here, there, weights):
-    d = weights.shape[0]
-    room = weights.shape[1] // 3
+    part = lax.dot_general(hidden, weights[:, 2 * room :], NT, preferred_element_type=jnp.float32)
+    out[...] = part.astype(out.dtype)
+
+
+def mixer(rows, weights, dtype):
     return pl.pallas_call(
         mixer_kernel,
-        out_shape=(
-            jax.ShapeDtypeStruct(here.shape, jnp.float32),
-            jax.ShapeDtypeStruct(here.shape, jnp.bfloat16),
-        ),
-        in_specs=[VMEM] * 2 + [pl.BlockSpec(memory_space=pltpu.HBM)],
-        out_specs=(VMEM, VMEM),
-        scratch_shapes=[
-            pltpu.VMEM((d, 2 * room), jnp.bfloat16),
-            pltpu.VMEM((d, room), jnp.bfloat16),
-            pltpu.SemaphoreType.DMA((5,)),
-        ],
-        compiler_params=pltpu.CompilerParams(vmem_limit_bytes=52 * MIB),
-        name="mixer",
-    )(here, there, weights)
+        out_shape=jax.ShapeDtypeStruct(rows.shape, dtype),
+        in_specs=[VMEM] * 2,
+        out_specs=VMEM,
+        compiler_params=pltpu.CompilerParams(vmem_limit_bytes=16 * MIB),
+    )(rows, weights)
 
 
 def shards(
@@ -408,8 +386,10 @@
     here = from_everyone(normed, ("yl", "x")).reshape(-1, d)
     here, weights = lax.optimization_barrier((here, weights))
     there = partner(here)
-    part_here, part_there = mixer(here, there, weights)
+    held = fetch(weights)
+    part_there = mixer(there, held, jnp.bfloat16)
     sent = partner(part_there)
+    part_here = mixer(here, held, jnp.float32)
     both = (part_here + sent.astype(jnp.float32)).astype(jnp.bfloat16)
     pieces = exchanged(both.reshape(-1, rows, d), ("yl", "x"))
     channel = jnp.sum(pieces.astype(jnp.float32), axis=0).astype(jnp.bfloat16)

time: 167 us -> 162 us (0.970)
  local copies, waits for them, and re-layouts: 7.26 us -> 4.8 us
  waiting for transfers between devices: 17.1 us -> 14.7 us
  Pallas kernels: 13.8 us -> 15.5 us
    unnamed x30 -> x24, local copies, waits for them, and re-layouts: 7.14 us -> 4.67 us
    ppermute x3, waiting for transfers between devices: 3.03 us -> 0.58 us  [partner(): return lax.ppermute(x, 'c', [(0, 1), (1, 0)])]
    pallas_call x1 -> x3, Pallas kernels: 4.72 us -> 4.93 us  [the longest x2 2.59 us: mixer(): pl.pallas_call(mixer_kernel, out_shape=jax.ShapeDtypeStruct(rows.shape, d...]
  transfers between devices with their start and end apart: 8 -> 8, of which waited for: 5 -> 4; matrix products, arithmetic and copies ran while one was open for 0% -> 0% of each run, Pallas kernels for 5% -> 8%
where the time goes in v5:
time: 162 us; the launch traced here: 161 us
  blocking collectives  81.7 us (50%)
  starting transfers between devices  29.4 us (18%)
  Pallas kernels  15.5 us (10%)
  waiting for transfers between devices  14.7 us (9%)
  between operations  13.6 us (8%)
  local copies, waits for them, and re-layouts  4.8 us (3%)
    all_to_all x4, blocking collectives, exchanged(): return lax.all_to_all(chunks, axis, split_axis=0, concat_axis=0, tiled=True)  58.5 us
    all_to_all x2, blocking collectives, from_everyone(): return lax.all_to_all(copies, axis, split_axis=0, concat_axis=0, tiled=True)  23.2 us
    ppermute x3, starting transfers between devices, partner(): return lax.ppermute(x, 'c', [(0, 1), (1, 0)])  15.4 us
    all_to_all x1, waiting for transfers between devices, exchanged(): return lax.all_to_all(chunks, axis, split_axis=0, concat_axis=0, tiled=True)  9.37 us
    ppermute x3, starting transfers between devices, shards(): lax.ppermute(query, ('yh', 'yl'), [(i, (i + k) % n_y) for i in range(n_y)])  8.15 us
    pallas_call x1, Pallas kernels, attention(): pl.pallas_call(attention_kernel, out_shape=jax.ShapeDtypeStruct((n_y, row...  6.95 us
    all_to_all x1, starting transfers between devices, exchanged(): return lax.all_to_all(chunks, axis, split_axis=0, concat_axis=0, tiled=True)  5.84 us
    ppermute x3, waiting for transfers between devices, shards(): lax.ppermute(query, ('yh', 'yl'), [(i, (i + k) % n_y) for i in range(n_y)])  4.68 us
  transfers between devices with their start and end apart: 8, of which 4 were waited for; matrix products, arithmetic and copies ran while one was open for 0% of the time, Pallas kernels for 8%

profile of v5, /device:TPU:1, one launch (start us, length us, event | category | flops | bytes accessed | tf_op | source)
XLA Modules:
  0.0 161.0 jit_solution(2602344011501260785)
XLA Ops:
  6.6 1.7 %pack_weights.1 = bf16[4,32,1152]{2,1,0:T(8,128)(2,1)} custom-call(bf16[32,704]{1,0:T(8,128)(2,1)} %gate.1, bf16[32,704]{1,0:T(8,128)(2,1)} %up.1, bf16[32,704]{1,0:T(8,128)(2,1)} %down.1), custom_call_target="tpu_custom_call" | custom-call | tf_op jit(solution)/shard_map/pack_weights/pallas_call | solution.py:70
  8.3 10.8 %all_to_all.35 = bf16[4,32,1152]{2,1,0:T(8,128)(2,1)} all-to-all(bf16[4,32,1152]{2,1,0:T(8,128)(2,1)} %pack_weights.1), channel_id=1, replica_groups=mesh['z'=16,'yh'=2,'yl'=2,'x'=4,'c'=2] {'yh','yl'}, dimensions={0} | all-to-all | bytes 589824 | tf_op jit(solution)/shard_map/all_to_all | solution.py:39
  19.3 0.8 copy-done.4
  20.2 0.8 copy-done.5
  22.5 27.1 %all_to_all.36 = bf16[16,40,128]{2,1,0:T(8,128)(2,1)S(1)} all-to-all(bf16[16,40,128]{2,1,0:T(8,128)(2,1)S(1)} %get-tuple-element.10), channel_id=1, replica_groups=mesh['z'=16,'yh'=2,'yl'=2,'x'=4,'c'=2] {'z'}, dimensions={0} | all-to-all | bytes 327680 | tf_op jit(solution)/shard_map/all_to_all | solution.py:39
  49.7 11.6 %all_to_all.37.mine = bf16[4,16,40,128]{3,2,1,0:T(8,128)(2,1)S(1)} all-to-all(bf16[4,16,40,128]{3,2,1,0:T(8,128)(2,1)S(1)} %broadcast_in_dim.4), channel_id=1, replica_groups=mesh['z'=16,'yh'=2,'yl'=2,'x'=4,'c'=2] {'x'}, dimensions={0} | all-to-all | bytes 1310720 | tf_op jit(solution)/shard_map/all_to_all | solution.py:35
  61.3 9.8 %collective-permute-start.3 = (bf16[4,16,40,128]{3,2,1,0:T(8,128)(2,1)S(1)}, bf16[4,16,40,128]{3,2,1,0:T(8,128)(2,1)S(1)}, u32[]{:S(2)}, u32[]{:S(2)}) collective-permute-start(bf16[4,16,40,128]{3,2,1,0:T(8,128)(2,1)S(1)} %all_to_all.37.mine), channel_id=1, source_target_pairs={{0,1},{1,0},{2,3},{3,2},{4,5},{5,4},{6,7},{7,6},{8,9},{9,8},{10,11... | collective-permute-start | bytes 1966088 | tf_op jit(solution)/shard_map/ppermute | solution.py:43
  71.1 2.2 %collective-permute-start.2 = (bf16[128,256]{1,0:T(8,128)(2,1)S(1)}, bf16[128,256]{1,0:T(8,128)(2,1)S(1)}, u32[]{:S(2)}, u32[]{:S(2)}) collective-permute-start(bf16[128,256]{1,0:T(8,128)(2,1)S(1)} %get-tuple-element.9.refs_0_), channel_id=1, source_target_pairs={{0,24},{8,0},{16,8},{24,16},{1,25},{9,1},{17,9},{25,17},{2,26},{10... | collective-permute-start | bytes 196616 | tf_op jit(solution)/shard_map/ppermute | solution.py:369
  73.3 4.0 %collective-permute-start.1 = (bf16[128,256]{1,0:T(8,128)(2,1)S(1)}, bf16[128,256]{1,0:T(8,128)(2,1)S(1)}, u32[]{:S(2)}, u32[]{:S(2)}) collective-permute-start(bf16[128,256]{1,0:T(8,128)(2,1)S(1)} %get-tuple-element.9.refs_0_), channel_id=1, source_target_pairs={{0,16},{8,24},{16,0},{24,8},{1,17},{9,25},{17,1},{25,9},{2,18},{10... | collective-permute-start | bytes 196616 | tf_op jit(solution)/shard_map/ppermute | solution.py:369
  77.3 1.9 %collective-permute-start = (bf16[128,256]{1,0:T(8,128)(2,1)S(1)}, bf16[128,256]{1,0:T(8,128)(2,1)S(1)}, u32[]{:S(2)}, u32[]{:S(2)}) collective-permute-start(bf16[128,256]{1,0:T(8,128)(2,1)S(1)} %get-tuple-element.9.refs_0_), channel_id=1, source_target_pairs={{0,8},{8,16},{16,24},{24,0},{1,9},{9,17},{17,25},{25,1},{2,10},{10... | collective-permute-start | bytes 196616 | tf_op jit(solution)/shard_map/ppermute | solution.py:369
  79.8 4.1 %collective-permute-done.refs_1_ = bf16[128,256]{1,0:T(8,128)(2,1)S(1)} collective-permute-done((bf16[128,256]{1,0:T(8,128)(2,1)S(1)}, bf16[128,256]{1,0:T(8,128)(2,1)S(1)}, u32[]{:S(2)}, u32[]{:S(2)}) %collective-permute-start) | collective-permute-done | bytes 65568 | tf_op jit(solution)/shard_map/ppermute | solution.py:369
  84.0 0.8 copy-done.2
  85.9 7.0 %attend.1 = bf16[4,128,256]{2,1,0:T(8,128)(2,1)S(1)} custom-call(s32[1]{0:T(128)} %bitcast.place, bf16[4,2,128,512]{3,2,1,0:T(8,128)(2,1)S(1)} %absorb.1.query, bf16[4,16,40,128]{3,2,1,0:T(8,128)(2,1)S(1)} %all_to_all.37.mine, bf16[4,16,40,128]{3,2,1,0:T(8,128)(2,1)S(1)} %collective-permute-done.3.other, bf16[64,256]{1,0:T(8,128)(2,1)S(1)} %bitcast.13, ...), custom_call_target="tpu_custom_call" | custom-call | tf_op jit(solution)/shard_map/attend/pallas_call | solution.py:233
  92.9 7.9 %all_to_all.38.parts = bf16[4,128,256]{2,1,0:T(8,128)(2,1)S(1)} all-to-all(bf16[4,128,256]{2,1,0:T(8,128)(2,1)S(1)} %attend.1), channel_id=1, replica_groups=mesh['z'=16,'yh'=2,'yl'=2,'x'=4,'c'=2] {'yh','yl'}, dimensions={0} | all-to-all | bytes 524288 | tf_op jit(solution)/shard_map/all_to_all | solution.py:39
  100.8 1.5 merge.1
  102.3 5.8 %all-to-all-start.3 = ((bf16[8,16,2048]{2,1,0:T(8,128)(2,1)}), bf16[8,16,2048]{2,1,0:T(8,128)(2,1)S(1)}, u32[]{:S(2)}, u32[]{:S(2)}) async-start(bf16[8,16,2048]{2,1,0:T(8,128)(2,1)} %bitcast.6), calls=%async_computation.3 | async-start | bytes 1048576 | tf_op jit(solution)/shard_map/all_to_all | solution.py:39
  108.1 9.4 %all-to-all-done.3 = bf16[8,16,2048]{2,1,0:T(8,128)(2,1)S(1)} async-done(((bf16[8,16,2048]{2,1,0:T(8,128)(2,1)}), bf16[8,16,2048]{2,1,0:T(8,128)(2,1)S(1)}, u32[]{:S(2)}, u32[]{:S(2)}) %all-to-all-start.3) | async-done | bytes 524320 | tf_op jit(solution)/shard_map/all_to_all | solution.py:39
  117.9 11.6 %all_to_all.39 = bf16[8,16,2048]{2,1,0:T(8,128)(2,1)S(1)} all-to-all(bf16[8,16,2048]{2,1,0:T(8,128)(2,1)S(1)} %broadcast_in_dim.5), channel_id=1, replica_groups=mesh['z'=16,'yh'=2,'yl'=2,'x'=4,'c'=2] {'yl','x'}, dimensions={0} | all-to-all | bytes 1048576 | tf_op jit(solution)/shard_map/all_to_all | solution.py:35
  129.5 3.7 %collective-permute-start.4 = (bf16[128,2048]{1,0:T(8,128)(2,1)S(1)}, bf16[128,2048]{1,0:T(8,128)(2,1)S(1)}, u32[]{:S(2)}, u32[]{:S(2)}) collective-permute-start(bf16[128,2048]{1,0:T(8,128)(2,1)S(1)} %bitcast.10), channel_id=1, source_target_pairs={{0,1},{1,0},{2,3},{3,2},{4,5},{5,4},{6,7},{7,6},{8,9},{9,8},{10,11... | collective-permute-start | bytes 1572872 | tf_op jit(solution)/shard_map/ppermute | solution.py:43
  133.2 2.3 %fetch.1.weights = bf16[2048,1152]{1,0:T(8,128)(2,1)S(1)} custom-call(bf16[2048,1152]{1,0:T(8,128)(2,1)} %all-gather.2.cloned.1.call-done.weights), custom_call_target="tpu_custom_call" | custom-call | tf_op jit(solution)/shard_map/fetch/pallas_call | solution.py:292
  135.6 1.3 shard_map.146
  136.9 1.9 %collective-permute-start.5 = (bf16[128,2048]{1,0:T(8,128)(2,1)S(1)}, bf16[128,2048]{1,0:T(8,128)(2,1)S(1)}, u32[]{:S(2)}, u32[]{:S(2)}) collective-permute-start(bf16[128,2048]{1,0:T(8,128)(2,1)S(1)} %shard_map.146), channel_id=1, source_target_pairs={{0,1},{1,0},{2,3},{3,2},{4,5},{5,4},{6,7},{7,6},{8,9},{9,8},{10,11... | collective-permute-start | bytes 1572872 | tf_op jit(solution)/shard_map/ppermute | solution.py:43
  138.8 1.3 shard_map.145
  140.8 12.6 %all_to_all.40 = bf16[8,16,2048]{2,1,0:T(8,128)(2,1)S(1)} all-to-all(bf16[8,16,2048]{2,1,0:T(8,128)(2,1)S(1)} %bitcast.17), channel_id=1, replica_groups=mesh['z'=16,'yh'=2,'yl'=2,'x'=4,'c'=2] {'yl','x'}, dimensions={0} | all-to-all | bytes 1048576 | tf_op jit(solution)/shard_map/all_to_all | solution.py:39
  (45 shorter events, 5.3 us)
Async XLA Ops:
  6.5 79.4 %copy-start.3 = (bf16[256,128]{1,0:T(8,128)(2,1)S(1)}, bf16[256,128]{1,0:T(8,128)(2,1)}, u32[]{:S(2)}) copy-start(bf16[256,128]{1,0:T(8,128)(2,1)} %value_up_l.1) | copy-start | bytes 196612
  6.5 79.4 %copy-start.6 = (bf16[256,64]{0,1:T(8,128)(2,1)S(1)}, bf16[256,64]{0,1:T(8,128)(2,1)}, u32[]{:S(2)}) copy-start(bf16[256,64]{0,1:T(8,128)(2,1)} %param.21) | copy-start | bytes 98308
  6.5 94.2 %copy-start = (bf16[128,2048]{1,0:T(8,128)(2,1)S(1)}, bf16[128,2048]{1,0:T(8,128)(2,1)}, u32[]{:S(2)}) copy-start(bf16[128,2048]{1,0:T(8,128)(2,1)} %out_l.1) | copy-start | bytes 1572868
  6.5 94.2 %copy-start.1 = (bf16[64,2048]{1,0:T(8,128)(2,1)S(1)}, bf16[64,2048]{1,0:T(8,128)(2,1)}, u32[]{:S(2)}) copy-start(bf16[64,2048]{1,0:T(8,128)(2,1)} %out_s.1) | copy-start | bytes 786436
  6.5 123.0 %all-gather.2.cloned.1.call-start = ((), (), s32[]{:S(2)}) async-start(), calls=%async_computation.7 | async-start | bytes 5013504 | tf_op jit(solution)/shard_map/all_gather | solution.py:350
  19.3 0.8 copy-start.4
  20.2 0.8 copy-start.5
  20.9 0.7 copy-start.8
  21.7 0.7 copy-start.9
  49.7 58.4 %copy-start.11 = (bf16[2048]{0:T(1024)(128)(2,1)S(1)}, bf16[2048]{0:T(1024)(128)(2,1)}, u32[]{:S(2)}) copy-start(bf16[2048]{0:T(1024)(128)(2,1)} %param.26) | copy-start | bytes 12292
  49.7 67.9 %copy-start.10 = (bf16[16,2048]{1,0:T(8,128)(2,1)S(1)}, bf16[16,2048]{1,0:T(8,128)(2,1)}, u32[]{:S(2)}) copy-start(bf16[16,2048]{1,0:T(8,128)(2,1)} %param.15) | copy-start | bytes 196612
  61.3 24.6 %collective-permute-start.3 = (bf16[4,16,40,128]{3,2,1,0:T(8,128)(2,1)S(1)}, bf16[4,16,40,128]{3,2,1,0:T(8,128)(2,1)S(1)}, u32[]{:S(2)}, u32[]{:S(2)}) collective-permute-start(bf16[4,16,40,128]{3,2,1,0:T(8,128)(2,1)S(1)} %all_to_all.37.mine), channel_id=1, source_target_pairs={{0,1},{1,0},{2,3},{3,2},{4,5},{5,4},{6,7},{7,6},{8,9},{9,8},{10,11... | collective-permute-start | bytes 1966088 | tf_op jit(solution)/shard_map/ppermute | solution.py:43
  71.1 8.2 %collective-permute-start.2 = (bf16[128,256]{1,0:T(8,128)(2,1)S(1)}, bf16[128,256]{1,0:T(8,128)(2,1)S(1)}, u32[]{:S(2)}, u32[]{:S(2)}) collective-permute-start(bf16[128,256]{1,0:T(8,128)(2,1)S(1)} %get-tuple-element.9.refs_0_), channel_id=1, source_target_pairs={{0,24},{8,0},{16,8},{24,16},{1,25},{9,1},{17,9},{25,17},{2,26},{10... | collective-permute-start | bytes 196616 | tf_op jit(solution)/shard_map/ppermute | solution.py:369
  73.3 6.5 %collective-permute-start.1 = (bf16[128,256]{1,0:T(8,128)(2,1)S(1)}, bf16[128,256]{1,0:T(8,128)(2,1)S(1)}, u32[]{:S(2)}, u32[]{:S(2)}) collective-permute-start(bf16[128,256]{1,0:T(8,128)(2,1)S(1)} %get-tuple-element.9.refs_0_), channel_id=1, source_target_pairs={{0,16},{8,24},{16,0},{24,8},{1,17},{9,25},{17,1},{25,9},{2,18},{10... | collective-permute-start | bytes 196616 | tf_op jit(solution)/shard_map/ppermute | solution.py:369
  77.3 6.6 %collective-permute-start = (bf16[128,256]{1,0:T(8,128)(2,1)S(1)}, bf16[128,256]{1,0:T(8,128)(2,1)S(1)}, u32[]{:S(2)}, u32[]{:S(2)}) collective-permute-start(bf16[128,256]{1,0:T(8,128)(2,1)S(1)} %get-tuple-element.9.refs_0_), channel_id=1, source_target_pairs={{0,8},{8,16},{16,24},{24,0},{1,9},{9,17},{17,25},{25,1},{2,10},{10... | collective-permute-start | bytes 196616 | tf_op jit(solution)/shard_map/ppermute | solution.py:369
  84.0 0.8 copy-start.2
  84.8 0.8 copy-start.7
  102.3 15.2 %all-to-all-start.3 = ((bf16[8,16,2048]{2,1,0:T(8,128)(2,1)}), bf16[8,16,2048]{2,1,0:T(8,128)(2,1)S(1)}, u32[]{:S(2)}, u32[]{:S(2)}) async-start(bf16[8,16,2048]{2,1,0:T(8,128)(2,1)} %bitcast.6), calls=%async_computation.3 | async-start | bytes 1048576 | tf_op jit(solution)/shard_map/all_to_all | solution.py:39
  129.5 6.1 %collective-permute-start.4 = (bf16[128,2048]{1,0:T(8,128)(2,1)S(1)}, bf16[128,2048]{1,0:T(8,128)(2,1)S(1)}, u32[]{:S(2)}, u32[]{:S(2)}) collective-permute-start(bf16[128,2048]{1,0:T(8,128)(2,1)S(1)} %bitcast.10), channel_id=1, source_target_pairs={{0,1},{1,0},{2,3},{3,2},{4,5},{5,4},{6,7},{7,6},{8,9},{9,8},{10,11... | collective-permute-start | bytes 1572872 | tf_op jit(solution)/shard_map/ppermute | solution.py:43
  136.9 3.8 %collective-permute-start.5 = (bf16[128,2048]{1,0:T(8,128)(2,1)S(1)}, bf16[128,2048]{1,0:T(8,128)(2,1)S(1)}, u32[]{:S(2)}, u32[]{:S(2)}) collective-permute-start(bf16[128,2048]{1,0:T(8,128)(2,1)S(1)} %shard_map.146), channel_id=1, source_target_pairs={{0,1},{1,0},{2,3},{3,2},{4,5},{5,4},{6,7},{7,6},{8,9},{9,8},{10,11... | collective-permute-start | bytes 1572872 | tf_op jit(solution)/shard_map/ppermute | solution.py:43
Sparse Core Ops, SparseCore 0:
  19.3 79.8 all-gather.1

commit v6 on v5

--- a/solution.py
+++ b/solution.py
@@ -120,7 +120,6 @@
         in_specs=[SMEM] + [VMEM] * 6,
         out_specs=(VMEM, VMEM),
         scratch_shapes=[pltpu.VMEM((256 + ROPE, rows), jnp.float32)],
-        compiler_params=pltpu.CompilerParams(vmem_limit_bytes=4 * MIB),
         name="prepare",
     )(place, small, large, latent, rope_key, cosine, sine)
 
@@ -241,45 +240,128 @@
     )(place, query, mine, other, value_up_s, value_up_l)
 
 
-def merge_kernel(parts, out_s, out_l, out):
-    n = parts.shape[0]
-
-    def merged(first, width, stat):
-        def stat_of(i, k):
-            at = 192 + stat + 3 * k
-            return (
-                parts[i, :, at : at + 1].astype(jnp.float32)
-                + parts[i, :, at + 1 : at + 2].astype(jnp.float32)
-            ) + parts[i, :, at + 2 : at + 3].astype(jnp.float32)
-
-        tops = [stat_of(i, 0) for i in range(n)]
-        top = tops[0]
-        for t in tops[1:]:
-            top = jnp.maximum(top, t)
-        shares = [stat_of(i, 1) * jnp.exp(tops[i] - top) for i in range(n)]
-        total = sum(shares[1:], shares[0])
-        acc = 0.0
-        for i in range(n):
-            acc = acc + parts[i, :, first : first + width].astype(jnp.float32) * (shares[i] / total)
-        return acc.astype(jnp.bfloat16)
-
-    large = merged(0, 128, 0)
-    small = merged(128, 64, 6)
-    mixed = jnp.dot(small, out_s[...], preferred_element_type=jnp.float32) + jnp.dot(
-        large, out_l[...], preferred_element_type=jnp.float32
-    )
-    out[...] = mixed.astype(jnp.bfloat16)
-
-
-def merge(parts, out_s, out_l):
+def stack_kernel(out_l, out_s, out):
+    rows = out_l.shape[0]
+    out[0:rows, :] = out_l[...]
+    out[rows:, :] = out_s[...]
+
+
+def stack(out_l, out_s):
+    rows = out_l.shape[0] + out_s.shape[0]
+    return pl.pallas_call(
+        stack_kernel,
+        out_shape=jax.ShapeDtypeStruct((rows, out_l.shape[1]), jnp.bfloat16),
+        in_specs=[VMEM] * 2,
+        out_specs=VMEM,
+        name="stack_out",
+    )(out_l, out_s)
+
+
+def halves_kernel(before, after, large, small):
+    large[...] = before[0:HEAD_LARGE, :]
+    small[...] = after[HEAD_LARGE:, :]
+
+
+def halves(before, after):
+    d = before.shape[1]
+    return pl.pallas_call(
+        halves_kernel,
+        out_shape=(
+            jax.ShapeDtypeStruct((HEAD_LARGE, d), jnp.bfloat16),
+            jax.ShapeDtypeStruct((HEAD_SMALL, d), jnp.bfloat16),
+        ),
+        in_specs=[VMEM] * 2,
+        out_specs=(VMEM, VMEM),
+        compiler_params=pltpu.CompilerParams(vmem_limit_bytes=8 * MIB),
+        name="halves",
+    )(before, after)
+
+
+def merge_kernel(place, parts, own, before, after, far_l, far_s, mine, theirs):
+    _, _, x, core = where_in(place[0])
+    n_x = 4
+    n_y = parts.shape[0] // n_x
+    rows = mine.shape[0]
+
+    def attended(k):
+        column = lax.rem(x - k + n_x, n_x)
+        pieces = [parts[n_x * i + column].astype(jnp.float32) for i in range(n_y)]
+
+        def merged(first, width, stat):
+            def stat_of(piece, which):
+                at = 192 + stat + 3 * which
+                return (piece[:, at : at + 1] + piece[:, at + 1 : at + 2]) + piece[:, at + 2 : at + 3]
+
+            tops = [stat_of(piece, 0) for piece in pieces]
+            top = tops[0]
+            for t in tops[1:]:
+                top = jnp.maximum(top, t)
+            shares = [stat_of(p, 1) * jnp.exp(t - top) for p, t in zip(pieces, tops)]
+            total = sum(shares[1:], shares[0])
+            acc = 0.0
+            for piece, share in zip(pieces, shares):
+                acc = acc + piece[:, first : first + width] * (share / total)
+            return acc.astype(jnp.bfloat16)
+
+        return merged(0, HEAD_LARGE, 0), merged(HEAD_LARGE, HEAD_SMALL, 6)
+
+    total = None
+    for k, (large_w, small_w) in enumerate(
+        (
+            (own[0:HEAD_LARGE, :], own[HEAD_LARGE:, :]),
+            (before[0:HEAD_LARGE, :], before[HEAD_LARGE:, :]),
+            (far_l[...], far_s[...]),
+            (after[0:HEAD_LARGE, :], after[HEAD_LARGE:, :]),
+        )
+    ):
+        large, small = attended(k)
+        term = jnp.dot(large, large_w, preferred_element_type=jnp.float32) + jnp.dot(
+            small, small_w, preferred_element_type=jnp.float32
+        )
+        total = term if total is None else total + term
+    top, bottom = total[0:rows, :], total[rows : 2 * rows, :]
+    mine[...] = jnp.where(core == 0, top, bottom)
+    theirs[...] = jnp.where(core == 0, bottom, top).astype(jnp.bfloat16)
+
+
+def merge(place, parts, own, before, after, far_l, far_s):
+    rows, d = parts.shape[1] // 2, own.shape[1]
     return pl.pallas_call(
         merge_kernel,
-        out_shape=jax.ShapeDtypeStruct((parts.shape[1], out_s.shape[1]), jnp.bfloat16),
-        in_specs=[VMEM] * 3,
-        out_specs=VMEM,
+        out_shape=(
+            jax.ShapeDtypeStruct((rows, d), jnp.float32),
+            jax.ShapeDtypeStruct((rows, d), jnp.bfloat16),
+        ),
+        in_specs=[SMEM] + [VMEM] * 6,
+        out_specs=(VMEM, VMEM),
+        compiler_params=pltpu.CompilerParams(vmem_limit_bytes=16 * MIB),
+        name="merge",
+    )(place, parts, own, before, after, far_l, far_s)
+
+
+def norm_kernel(mine, sent, residual, gain, copies, stream):
+    mixed = (mine[...] + sent[...].astype(jnp.float32)).astype(jnp.bfloat16).astype(jnp.float32)
+    total = (residual[...].astype(jnp.float32) + mixed).astype(jnp.bfloat16)
+    stream[...] = total
+    wide = total.astype(jnp.float32)
+    normed = wide * lax.rsqrt(jnp.mean(wide * wide, axis=-1, keepdims=True) + norm_eps)
+    normed = (normed * gain[...].astype(jnp.float32)).astype(jnp.bfloat16)
+    for k in range(copies.shape[0]):
+        copies[k] = normed
+
+
+def norm(mine, sent, residual, gain, count):
+    return pl.pallas_call(
+        norm_kernel,
+        out_shape=(
+            jax.ShapeDtypeStruct((count, *residual.shape), jnp.bfloat16),
+            jax.ShapeDtypeStruct(residual.shape, jnp.bfloat16),
+        ),
+        in_specs=[VMEM] * 4,
+        out_specs=(VMEM, VMEM),
         compiler_params=pltpu.CompilerParams(vmem_limit_bytes=8 * MIB),
-        name="merge",
-    )(parts, out_s, out_l)
+        name="norm",
+    )(mine, sent, residual, gain)
 
 
 def fetch_kernel(weights, out, arrived):
@@ -337,6 +419,7 @@
     down_weight,
 ):
     n_y = lax.axis_size(("yh", "yl"))
+    n_x = lax.axis_size("x")
     z = lax.axis_index("z")
     y = lax.axis_index(("yh", "yl"))
     x = lax.axis_index("x")
@@ -350,6 +433,13 @@
     weights = lax.all_gather(
         over_y.reshape(-1, over_y.shape[2]), "z", axis=0, tiled=True
     )
+
+    own_out = stack(out_large, out_small)
+    before = lax.ppermute(own_out, "x", [(i, (i + 1) % n_x) for i in range(n_x)])
+    after = lax.ppermute(own_out, "x", [(i, (i - 1) % n_x) for i in range(n_x)])
+    pass_l, pass_s = halves(before, after)
+    far_l = lax.ppermute(pass_l, "x", [(i, (i + 1) % n_x) for i in range(n_x)])
+    far_s = lax.ppermute(pass_s, "x", [(i, (i - 1) % n_x) for i in range(n_x)])
 
     positions = (z * n_y + y) * row_count + jnp.arange(row_count, dtype=jnp.int32)
     inverse = 1.0 / rope_base ** (jnp.arange(0, ROPE, 2, dtype=jnp.float32) / ROPE)
@@ -374,16 +464,16 @@
     other = partner(mine)
 
     partial = attention(place, full, mine, other, value_up_small.T, value_up_large)
-    parts = exchanged(partial, ("yh", "yl"))
-    mixed_part = merge(parts, out_small, out_large)
-    tiles = exchanged(mixed_part.reshape(row_count // rows, rows, d), ("x", "c"))
-    mixed = jnp.sum(tiles.astype(jnp.float32), axis=0).astype(jnp.bfloat16)
-    stream = (residual.astype(jnp.float32) + mixed.astype(jnp.float32)).astype(jnp.bfloat16)
+    parts = exchanged(
+        partial.reshape(n_y * n_x, row_count // n_x, partial.shape[2]), ("yh", "yl", "x")
+    )
+    mine_part, theirs_part = merge(place, parts, own_out, before, after, far_l, far_s)
+    sent_part = partner(theirs_part)
+    copies, stream = norm(
+        mine_part, sent_part, residual, norm_gain.reshape(1, d), lax.axis_size(("yl", "x"))
+    )
     as_float = stream.astype(jnp.float32)
-    normed = as_float * lax.rsqrt(jnp.mean(as_float * as_float, axis=-1, keepdims=True) + norm_eps)
-    normed = (normed * norm_gain.astype(jnp.float32)[None, :]).astype(jnp.bfloat16)
-
-    here = from_everyone(normed, ("yl", "x")).reshape(-1, d)
+    here = exchanged(copies, ("yl", "x")).reshape(-1, d)
     here, weights = lax.optimization_barrier((here, weights))
     there = partner(here)
     held = fetch(weights)

time: 162 us -> 179 us (1.10)
  starting transfers between devices: 29.4 us -> 57.8 us
  blocking collectives: 81.7 us -> 63.3 us
  Pallas kernels: 15.5 us -> 21.5 us
    all_to_all x2 -> x0, blocking collectives: 23.2 us -> none  [from_everyone(): return lax.all_to_all(copies, axis, split_axis=0, concat_axis=0, tiled=True)]
    ppermute x0 -> x4, starting transfers between devices: none -> 13.1 us  [the longest x1 4.69 us: shards(): after = lax.ppermute(own_out, 'x', [(i, (i - 1) % n_x) for i in range(n_x)])]
    ppermute x3 -> x4, starting transfers between devices: 15.4 us -> 28.1 us  [partner(): return lax.ppermute(x, 'c', [(0, 1), (1, 0)])]
    ppermute x0 -> x4, waiting for transfers between devices: none -> 4.99 us  [the longest x1 3.28 us: shards(): lax.ppermute(own_out, 'x', [(i, (i + 1) % n_x) for i in range(n_x)])]
    all_to_all x4, blocking collectives: 58.5 us -> 63.3 us  [exchanged(): return lax.all_to_all(chunks, axis, split_axis=0, concat_axis=0, tiled=True)]
    ppermute x3, waiting for transfers between devices: 4.68 us -> 0.03 us  [shards(): lax.ppermute(query, ('yh', 'yl'), [(i, (i + k) % n_y) for i in range(n_y)])]
    all_to_all x0 -> x1, starting transfers between devices: none -> 4.01 us  [from_everyone(): return lax.all_to_all(copies, axis, split_axis=0, concat_axis=0, tiled=True)]
    pallas_call x1 -> x4, Pallas kernels: 1.49 us -> 5.29 us  [the longest x1 2.1 us: stack(): pl.pallas_call(stack_kernel, out_shape=jax.ShapeDtypeStruct((rows, out_l....]
  transfers between devices with their start and end apart: 8 -> 14, of which waited for: 4 -> 5; matrix products, arithmetic and copies ran while one was open for 0% -> 1% of each run, Pallas kernels for 8% -> 10%
where the time goes in v6:
time: 179 us; the launch traced here: 178 us
  blocking collectives  63.3 us (35%)
  starting transfers between devices  57.8 us (32%)
  Pallas kernels  21.5 us (12%)
  waiting for transfers between devices  14 us (8%)
  between operations  13.7 us (8%)
  local copies, waits for them, and re-layouts  5.82 us (3%)
    all_to_all x4, blocking collectives, exchanged(): return lax.all_to_all(chunks, axis, split_axis=0, concat_axis=0, tiled=True)  63.3 us
    ppermute x4, starting transfers between devices, partner(): return lax.ppermute(x, 'c', [(0, 1), (1, 0)])  28.1 us
    ppermute x3, starting transfers between devices, shards(): lax.ppermute(query, ('yh', 'yl'), [(i, (i + k) % n_y) for i in range(n_y)])  7.73 us
    pallas_call x1, Pallas kernels, attention(): pl.pallas_call(attention_kernel, out_shape=jax.ShapeDtypeStruct((n_y, row...  7.62 us
    all_to_all x1, waiting for transfers between devices, exchanged(): return lax.all_to_all(chunks, axis, split_axis=0, concat_axis=0, tiled=True)  7.52 us
    all_to_all x1, starting transfers between devices, exchanged(): return lax.all_to_all(chunks, axis, split_axis=0, concat_axis=0, tiled=True)  4.88 us
    unnamed x16, local copies, waits for them, and re-layouts  4.87 us
    ppermute x1, starting transfers between devices, shards(): after = lax.ppermute(own_out, 'x', [(i, (i - 1) % n_x) for i in range(n_x)])  4.69 us
  transfers between devices with their start and end apart: 14, of which 5 were waited for; matrix products, arithmetic and copies ran while one was open for 1% of the time, Pallas kernels for 10%

profile of v6, /device:TPU:1, one launch (start us, length us, event | category | flops | bytes accessed | tf_op | source)
XLA Modules:
  0.0 177.7 jit_solution(16879231017024895379)
XLA Ops:
  8.2 10.8 %all_to_all.30 = bf16[4,32,1152]{2,1,0:T(8,128)(2,1)} all-to-all(bf16[4,32,1152]{2,1,0:T(8,128)(2,1)} %pack_weights.1), channel_id=1, replica_groups=mesh['z'=16,'yh'=2,'yl'=2,'x'=4,'c'=2] {'yh','yl'}, dimensions={0} | all-to-all | bytes 589824 | tf_op jit(solution)/shard_map/all_to_all | solution.py:39
  19.8 1.7 prepare.1
  21.5 27.2 %all_to_all.31 = bf16[16,40,128]{2,1,0:T(8,128)(2,1)S(1)} all-to-all(bf16[16,40,128]{2,1,0:T(8,128)(2,1)} %get-tuple-element.16), channel_id=1, replica_groups=mesh['z'=16,'yh'=2,'yl'=2,'x'=4,'c'=2] {'z'}, dimensions={0} | all-to-all | bytes 327680 | tf_op jit(solution)/shard_map/all_to_all | solution.py:39
  49.6 4.0 %all-to-all-start.1 = ((bf16[4,16,40,128]{3,2,1,0:T(8,128)(2,1)}), bf16[4,16,40,128]{3,2,1,0:T(8,128)(2,1)S(1)}, u32[]{:S(2)}, u32[]{:S(2)}) async-start(bf16[4,16,40,128]{3,2,1,0:T(8,128)(2,1)} %broadcast_in_dim.2), calls=%async_computation.1 | async-start | bytes 1310720 | tf_op jit(solution)/shard_map/all_to_all | solution.py:35
  53.7 2.1 %stack_out.1.own = bf16[192,2048]{1,0:T(8,128)(2,1)} custom-call(bf16[128,2048]{1,0:T(8,128)(2,1)} %out_l.1, bf16[64,2048]{1,0:T(8,128)(2,1)} %out_s.1), custom_call_target="tpu_custom_call" | custom-call | tf_op jit(solution)/shard_map/stack_out/pallas_call | solution.py:251
  55.8 4.7 %collective-permute-start.5 = (bf16[192,2048]{1,0:T(8,128)(2,1)}, bf16[192,2048]{1,0:T(8,128)(2,1)S(1)}, u32[]{:S(2)}, u32[]{:S(2)}) collective-permute-start(bf16[192,2048]{1,0:T(8,128)(2,1)} %stack_out.1.own), channel_id=1, source_target_pairs={{0,6},{2,0},{4,2},{6,4},{1,7},{3,1},{5,3},{7,5},{8,14},{10,8},{12,... | collective-permute-start | bytes 2359304 | tf_op jit(solution)/shard_map/ppermute | solution.py:439
  60.5 1.9 %collective-permute-start.4 = (bf16[192,2048]{1,0:T(8,128)(2,1)}, bf16[192,2048]{1,0:T(8,128)(2,1)S(1)}, u32[]{:S(2)}, u32[]{:S(2)}) collective-permute-start(bf16[192,2048]{1,0:T(8,128)(2,1)} %stack_out.1.own), channel_id=1, source_target_pairs={{0,2},{2,4},{4,6},{6,0},{1,3},{3,5},{5,7},{7,1},{8,10},{10,12},{12... | collective-permute-start | bytes 2359304 | tf_op jit(solution)/shard_map/ppermute | solution.py:438
  62.4 12.6 %collective-permute-start.3 = (bf16[4,16,40,128]{3,2,1,0:T(8,128)(2,1)S(1)}, bf16[4,16,40,128]{3,2,1,0:T(8,128)(2,1)S(1)}, u32[]{:S(2)}, u32[]{:S(2)}) collective-permute-start(bf16[4,16,40,128]{3,2,1,0:T(8,128)(2,1)S(1)} %all-to-all-done.1.mine), channel_id=1, source_target_pairs={{0,1},{1,0},{2,3},{3,2},{4,5},{5,4},{6,7},{7,6},{8,9},{9,8},{10,11... | collective-permute-start | bytes 1966088 | tf_op jit(solution)/shard_map/ppermute | solution.py:43
  76.7 3.3 %collective-permute-done.4.before = bf16[192,2048]{1,0:T(8,128)(2,1)S(1)} collective-permute-done((bf16[192,2048]{1,0:T(8,128)(2,1)}, bf16[192,2048]{1,0:T(8,128)(2,1)S(1)}, u32[]{:S(2)}, u32[]{:S(2)}) %collective-permute-start.4) | collective-permute-done | bytes 786464 | tf_op jit(solution)/shard_map/ppermute | solution.py:438
  80.9 1.9 %collective-permute-start.6 = (bf16[128,2048]{1,0:T(8,128)(2,1)}, bf16[128,2048]{1,0:T(8,128)(2,1)S(1)}, u32[]{:S(2)}, u32[]{:S(2)}) collective-permute-start(bf16[128,2048]{1,0:T(8,128)(2,1)} %get-tuple-element.17), channel_id=1, source_target_pairs={{0,2},{2,4},{4,6},{6,0},{1,3},{3,5},{5,7},{7,1},{8,10},{10,12},{12... | collective-permute-start | bytes 1572872 | tf_op jit(solution)/shard_map/ppermute | solution.py:441
  82.8 2.8 %collective-permute-start.2 = (bf16[128,256]{1,0:T(8,128)(2,1)}, bf16[128,256]{1,0:T(8,128)(2,1)S(1)}, u32[]{:S(2)}, u32[]{:S(2)}) collective-permute-start(bf16[128,256]{1,0:T(8,128)(2,1)} %get-tuple-element.15.refs_0_), channel_id=1, source_target_pairs={{0,24},{8,0},{16,8},{24,16},{1,25},{9,1},{17,9},{25,17},{2,26},{10... | collective-permute-start | bytes 196616 | tf_op jit(solution)/shard_map/ppermute | solution.py:459
  85.7 2.8 %collective-permute-start.1 = (bf16[128,256]{1,0:T(8,128)(2,1)}, bf16[128,256]{1,0:T(8,128)(2,1)S(1)}, u32[]{:S(2)}, u32[]{:S(2)}) collective-permute-start(bf16[128,256]{1,0:T(8,128)(2,1)} %get-tuple-element.15.refs_0_), channel_id=1, source_target_pairs={{0,16},{8,24},{16,0},{24,8},{1,17},{9,25},{17,1},{25,9},{2,18},{10... | collective-permute-start | bytes 196616 | tf_op jit(solution)/shard_map/ppermute | solution.py:459
  88.5 2.1 %collective-permute-start = (bf16[128,256]{1,0:T(8,128)(2,1)}, bf16[128,256]{1,0:T(8,128)(2,1)S(1)}, u32[]{:S(2)}, u32[]{:S(2)}) collective-permute-start(bf16[128,256]{1,0:T(8,128)(2,1)} %get-tuple-element.15.refs_0_), channel_id=1, source_target_pairs={{0,8},{8,16},{16,24},{24,0},{1,9},{9,17},{17,25},{25,1},{2,10},{10... | collective-permute-start | bytes 196616 | tf_op jit(solution)/shard_map/ppermute | solution.py:459
  90.6 4.6 %collective-permute-start.7 = (bf16[64,2048]{1,0:T(8,128)(2,1)}, bf16[64,2048]{1,0:T(8,128)(2,1)}, u32[]{:S(2)}, u32[]{:S(2)}) collective-permute-start(bf16[64,2048]{1,0:T(8,128)(2,1)} %get-tuple-element.18), channel_id=1, source_target_pairs={{0,6},{2,0},{4,2},{6,4},{1,7},{3,1},{5,3},{7,5},{8,14},{10,8},{12,... | collective-permute-start | bytes 786440 | tf_op jit(solution)/shard_map/ppermute | solution.py:442
  99.6 7.6 %attend.1 = bf16[4,128,256]{2,1,0:T(8,128)(2,1)} custom-call(s32[1]{0:T(128)} %bitcast.place, bf16[4,2,128,512]{3,2,1,0:T(8,128)(2,1)S(1)} %absorb.1.query, bf16[4,16,40,128]{3,2,1,0:T(8,128)(2,1)S(1)} %all-to-all-done.1.mine, bf16[4,16,40,128]{3,2,1,0:T(8,128)(2,1)S(1)} %collective-permute-done.3.other, bf16[64,256]{1,0:T(8,128)(2,1)S(1)} %bitcast.12, ...), custom_call_target="tpu_custom_call" | custom-call | tf_op jit(solution)/shard_map/attend/pallas_call | solution.py:232
  107.2 4.9 %all-to-all-start.2 = ((bf16[16,32,256]{2,1,0:T(8,128)(2,1)}), bf16[16,32,256]{2,1,0:T(8,128)(2,1)S(1)}, u32[]{:S(2)}, u32[]{:S(2)}) async-start(bf16[16,32,256]{2,1,0:T(8,128)(2,1)} %bitcast.6), calls=%async_computation.2 | async-start | bytes 524288 | tf_op jit(solution)/shard_map/all_to_all | solution.py:39
  112.1 7.5 %all-to-all-done.2.parts = bf16[16,32,256]{2,1,0:T(8,128)(2,1)S(1)} async-done(((bf16[16,32,256]{2,1,0:T(8,128)(2,1)}), bf16[16,32,256]{2,1,0:T(8,128)(2,1)S(1)}, u32[]{:S(2)}, u32[]{:S(2)}) %all-to-all-start.2) | async-done | bytes 262176 | tf_op jit(solution)/shard_map/all_to_all | solution.py:39
  119.7 2.1 %merge.1 = (f32[16,2048]{1,0:T(8,128)S(1)}, bf16[16,2048]{1,0:T(8,128)(2,1)S(1)}) custom-call(s32[1]{0:T(128)} %bitcast.place, bf16[16,32,256]{2,1,0:T(8,128)(2,1)S(1)} %all-to-all-done.2.parts, bf16[192,2048]{1,0:T(8,128)(2,1)S(1)} %copy-done, bf16[192,2048]{1,0:T(8,128)(2,1)S(1)} %collective-permute-done.4.before, ...), custom_call_target="tpu_custom_call" | custom-call | tf_op jit(solution)/shard_map/merge/pallas_call | solution.py:329
  121.7 10.9 %collective-permute-start.8 = (bf16[16,2048]{1,0:T(8,128)(2,1)S(1)}, bf16[16,2048]{1,0:T(8,128)(2,1)S(1)}, u32[]{:S(2)}, u32[]{:S(2)}) collective-permute-start(bf16[16,2048]{1,0:T(8,128)(2,1)S(1)} %get-tuple-element.20), channel_id=1, source_target_pairs={{0,1},{1,0},{2,3},{3,2},{4,5},{5,4},{6,7},{7,6},{8,9},{9,8},{10,11... | collective-permute-start | bytes 196616 | tf_op jit(solution)/shard_map/ppermute | solution.py:43
  134.5 12.6 %all_to_all.32 = bf16[8,16,2048]{2,1,0:T(8,128)(2,1)S(1)} all-to-all(bf16[8,16,2048]{2,1,0:T(8,128)(2,1)S(1)} %get-tuple-element.22), channel_id=1, replica_groups=mesh['z'=16,'yh'=2,'yl'=2,'x'=4,'c'=2] {'yl','x'}, dimensions={0} | all-to-all | bytes 1048576 | tf_op jit(solution)/shard_map/all_to_all | solution.py:39
  147.1 2.7 %collective-permute-start.9 = (bf16[128,2048]{1,0:T(8,128)(2,1)S(1)}, bf16[128,2048]{1,0:T(8,128)(2,1)S(1)}, u32[]{:S(2)}, u32[]{:S(2)}) collective-permute-start(bf16[128,2048]{1,0:T(8,128)(2,1)S(1)} %bitcast.10), channel_id=1, source_target_pairs={{0,1},{1,0},{2,3},{3,2},{4,5},{5,4},{6,7},{7,6},{8,9},{9,8},{10,11... | collective-permute-start | bytes 1572872 | tf_op jit(solution)/shard_map/ppermute | solution.py:43
  149.9 2.3 %fetch.1.weights = bf16[2048,1152]{1,0:T(8,128)(2,1)S(1)} custom-call(bf16[2048,1152]{1,0:T(8,128)(2,1)} %all-gather.2.cloned.1.call-done.weights), custom_call_target="tpu_custom_call" | custom-call | tf_op jit(solution)/shard_map/fetch/pallas_call | solution.py:374
  153.5 1.9 %collective-permute-start.10 = (bf16[128,2048]{1,0:T(8,128)(2,1)S(1)}, bf16[128,2048]{1,0:T(8,128)(2,1)S(1)}, u32[]{:S(2)}, u32[]{:S(2)}) collective-permute-start(bf16[128,2048]{1,0:T(8,128)(2,1)S(1)} %shard_map.146), channel_id=1, source_target_pairs={{0,1},{1,0},{2,3},{3,2},{4,5},{5,4},{6,7},{7,6},{8,9},{9,8},{10,11... | collective-permute-start | bytes 1572872 | tf_op jit(solution)/shard_map/ppermute | solution.py:43
  157.4 12.6 %all_to_all.33 = bf16[8,16,2048]{2,1,0:T(8,128)(2,1)S(1)} all-to-all(bf16[8,16,2048]{2,1,0:T(8,128)(2,1)S(1)} %bitcast.14), channel_id=1, replica_groups=mesh['z'=16,'yh'=2,'yl'=2,'x'=4,'c'=2] {'yl','x'}, dimensions={0} | all-to-all | bytes 1048576 | tf_op jit(solution)/shard_map/all_to_all | solution.py:39
  (45 shorter events, 16.2 us)
Async XLA Ops:
  6.5 140.6 %all-gather.2.cloned.1.call-start = ((), (), s32[]{:S(2)}) async-start(), calls=%async_computation.6 | async-start | bytes 5013504 | tf_op jit(solution)/shard_map/all_gather | solution.py:433
  49.6 12.8 %all-to-all-start.1 = ((bf16[4,16,40,128]{3,2,1,0:T(8,128)(2,1)}), bf16[4,16,40,128]{3,2,1,0:T(8,128)(2,1)S(1)}, u32[]{:S(2)}, u32[]{:S(2)}) async-start(bf16[4,16,40,128]{3,2,1,0:T(8,128)(2,1)} %broadcast_in_dim.2), calls=%async_computation.1 | async-start | bytes 1310720 | tf_op jit(solution)/shard_map/all_to_all | solution.py:35
  55.8 63.9 %copy-start = (bf16[192,2048]{1,0:T(8,128)(2,1)S(1)}, bf16[192,2048]{1,0:T(8,128)(2,1)}, u32[]{:S(2)}) copy-start(bf16[192,2048]{1,0:T(8,128)(2,1)} %stack_out.1.own) | copy-start | bytes 2359300
  55.8 76.9 %copy-start.7 = (bf16[2048]{0:T(1024)(128)(2,1)S(1)}, bf16[2048]{0:T(1024)(128)(2,1)}, u32[]{:S(2)}) copy-start(bf16[2048]{0:T(1024)(128)(2,1)} %param.26) | copy-start | bytes 12292
  55.8 20.9 %collective-permute-start.5 = (bf16[192,2048]{1,0:T(8,128)(2,1)}, bf16[192,2048]{1,0:T(8,128)(2,1)S(1)}, u32[]{:S(2)}, u32[]{:S(2)}) collective-permute-start(bf16[192,2048]{1,0:T(8,128)(2,1)} %stack_out.1.own), channel_id=1, source_target_pairs={{0,6},{2,0},{4,2},{6,4},{1,7},{3,1},{5,3},{7,5},{8,14},{10,8},{12,... | collective-permute-start | bytes 2359304 | tf_op jit(solution)/shard_map/ppermute | solution.py:439
  60.5 19.5 %collective-permute-start.4 = (bf16[192,2048]{1,0:T(8,128)(2,1)}, bf16[192,2048]{1,0:T(8,128)(2,1)S(1)}, u32[]{:S(2)}, u32[]{:S(2)}) collective-permute-start(bf16[192,2048]{1,0:T(8,128)(2,1)} %stack_out.1.own), channel_id=1, source_target_pairs={{0,2},{2,4},{4,6},{6,0},{1,3},{3,5},{5,7},{7,1},{8,10},{10,12},{12... | collective-permute-start | bytes 2359304 | tf_op jit(solution)/shard_map/ppermute | solution.py:438
  62.4 35.6 %collective-permute-start.3 = (bf16[4,16,40,128]{3,2,1,0:T(8,128)(2,1)S(1)}, bf16[4,16,40,128]{3,2,1,0:T(8,128)(2,1)S(1)}, u32[]{:S(2)}, u32[]{:S(2)}) collective-permute-start(bf16[4,16,40,128]{3,2,1,0:T(8,128)(2,1)S(1)} %all-to-all-done.1.mine), channel_id=1, source_target_pairs={{0,1},{1,0},{2,3},{3,2},{4,5},{5,4},{6,7},{7,6},{8,9},{9,8},{10,11... | collective-permute-start | bytes 1966088 | tf_op jit(solution)/shard_map/ppermute | solution.py:43
  80.9 31.2 %collective-permute-start.6 = (bf16[128,2048]{1,0:T(8,128)(2,1)}, bf16[128,2048]{1,0:T(8,128)(2,1)S(1)}, u32[]{:S(2)}, u32[]{:S(2)}) collective-permute-start(bf16[128,2048]{1,0:T(8,128)(2,1)} %get-tuple-element.17), channel_id=1, source_target_pairs={{0,2},{2,4},{4,6},{6,0},{1,3},{3,5},{5,7},{7,1},{8,10},{10,12},{12... | collective-permute-start | bytes 1572872 | tf_op jit(solution)/shard_map/ppermute | solution.py:441
  82.8 7.8 %collective-permute-start.2 = (bf16[128,256]{1,0:T(8,128)(2,1)}, bf16[128,256]{1,0:T(8,128)(2,1)S(1)}, u32[]{:S(2)}, u32[]{:S(2)}) collective-permute-start(bf16[128,256]{1,0:T(8,128)(2,1)} %get-tuple-element.15.refs_0_), channel_id=1, source_target_pairs={{0,24},{8,0},{16,8},{24,16},{1,25},{9,1},{17,9},{25,17},{2,26},{10... | collective-permute-start | bytes 196616 | tf_op jit(solution)/shard_map/ppermute | solution.py:459
  85.7 9.5 %collective-permute-start.1 = (bf16[128,256]{1,0:T(8,128)(2,1)}, bf16[128,256]{1,0:T(8,128)(2,1)S(1)}, u32[]{:S(2)}, u32[]{:S(2)}) collective-permute-start(bf16[128,256]{1,0:T(8,128)(2,1)} %get-tuple-element.15.refs_0_), channel_id=1, source_target_pairs={{0,16},{8,24},{16,0},{24,8},{1,17},{9,25},{17,1},{25,9},{2,18},{10... | collective-permute-start | bytes 196616 | tf_op jit(solution)/shard_map/ppermute | solution.py:459
  88.5 6.7 %collective-permute-start = (bf16[128,256]{1,0:T(8,128)(2,1)}, bf16[128,256]{1,0:T(8,128)(2,1)S(1)}, u32[]{:S(2)}, u32[]{:S(2)}) collective-permute-start(bf16[128,256]{1,0:T(8,128)(2,1)} %get-tuple-element.15.refs_0_), channel_id=1, source_target_pairs={{0,8},{8,16},{16,24},{24,0},{1,9},{9,17},{17,25},{25,1},{2,10},{10... | collective-permute-start | bytes 196616 | tf_op jit(solution)/shard_map/ppermute | solution.py:459
  90.6 21.5 %collective-permute-start.7 = (bf16[64,2048]{1,0:T(8,128)(2,1)}, bf16[64,2048]{1,0:T(8,128)(2,1)}, u32[]{:S(2)}, u32[]{:S(2)}) collective-permute-start(bf16[64,2048]{1,0:T(8,128)(2,1)} %get-tuple-element.18), channel_id=1, source_target_pairs={{0,6},{2,0},{4,2},{6,4},{1,7},{3,1},{5,3},{7,5},{8,14},{10,8},{12,... | collective-permute-start | bytes 786440 | tf_op jit(solution)/shard_map/ppermute | solution.py:442
  95.2 0.8 copy-start.3
  96.1 0.8 copy-start.1
  96.9 0.8 copy-start.6
  98.0 0.8 copy-start.2
  98.8 0.8 copy-start.5
  107.2 12.4 %all-to-all-start.2 = ((bf16[16,32,256]{2,1,0:T(8,128)(2,1)}), bf16[16,32,256]{2,1,0:T(8,128)(2,1)S(1)}, u32[]{:S(2)}, u32[]{:S(2)}) async-start(bf16[16,32,256]{2,1,0:T(8,128)(2,1)} %bitcast.6), calls=%async_computation.2 | async-start | bytes 524288 | tf_op jit(solution)/shard_map/all_to_all | solution.py:39
  121.7 11.8 %collective-permute-start.8 = (bf16[16,2048]{1,0:T(8,128)(2,1)S(1)}, bf16[16,2048]{1,0:T(8,128)(2,1)S(1)}, u32[]{:S(2)}, u32[]{:S(2)}) collective-permute-start(bf16[16,2048]{1,0:T(8,128)(2,1)S(1)} %get-tuple-element.20), channel_id=1, source_target_pairs={{0,1},{1,0},{2,3},{3,2},{4,5},{5,4},{6,7},{7,6},{8,9},{9,8},{10,11... | collective-permute-start | bytes 196616 | tf_op jit(solution)/shard_map/ppermute | solution.py:43
  133.5 0.8 copy-start.4
  147.1 5.1 %collective-permute-start.9 = (bf16[128,2048]{1,0:T(8,128)(2,1)S(1)}, bf16[128,2048]{1,0:T(8,128)(2,1)S(1)}, u32[]{:S(2)}, u32[]{:S(2)}) collective-permute-start(bf16[128,2048]{1,0:T(8,128)(2,1)S(1)} %bitcast.10), channel_id=1, source_target_pairs={{0,1},{1,0},{2,3},{3,2},{4,5},{5,4},{6,7},{7,6},{8,9},{9,8},{10,11... | collective-permute-start | bytes 1572872 | tf_op jit(solution)/shard_map/ppermute | solution.py:43
  153.5 3.8 %collective-permute-start.10 = (bf16[128,2048]{1,0:T(8,128)(2,1)S(1)}, bf16[128,2048]{1,0:T(8,128)(2,1)S(1)}, u32[]{:S(2)}, u32[]{:S(2)}) collective-permute-start(bf16[128,2048]{1,0:T(8,128)(2,1)S(1)} %shard_map.146), channel_id=1, source_target_pairs={{0,1},{1,0},{2,3},{3,2},{4,5},{5,4},{6,7},{7,6},{8,9},{9,8},{10,11... | collective-permute-start | bytes 1572872 | tf_op jit(solution)/shard_map/ppermute | solution.py:43
Sparse Core Ops, SparseCore 0:
  19.2 79.2 all-gather.1

commit v7 on v5

--- a/solution.py
+++ b/solution.py
@@ -223,8 +223,10 @@
         ]
         for i, part in enumerate(parts):
             stats = jnp.where(stat_lane == i, part, stats)
-        out[j, :, 0:128] = value_l.astype(jnp.bfloat16)
-        out[j, :, 128:256] = jnp.concatenate([value_s, stats], axis=1).astype(jnp.bfloat16)
+        whole = jnp.concatenate([value_l, jnp.concatenate([value_s, stats], axis=1)], axis=1)
+        for core in range(2):
+            picked = [whole[32 * x + 16 * core : 32 * x + 16 * core + 16] for x in range(n_x)]
+            out[2 * j + core] = jnp.concatenate(picked, axis=0).astype(jnp.bfloat16)
 
 
 def attention(place, query, mine, other, value_up_s, value_up_l):
@@ -232,7 +234,7 @@
     n_keys = 128 * mine.shape[1]
     return pl.pallas_call(
         attention_kernel,
-        out_shape=jax.ShapeDtypeStruct((n_y, rows, 256), jnp.bfloat16),
+        out_shape=jax.ShapeDtypeStruct((2 * n_y, rows // 2, 256), jnp.bfloat16),
         in_specs=[SMEM] + [VMEM] * 5,
         out_specs=VMEM,
         scratch_shapes=[pltpu.VMEM((depth, n_keys), jnp.bfloat16)],
@@ -241,45 +243,50 @@
     )(place, query, mine, other, value_up_s, value_up_l)
 
 
-def merge_kernel(parts, out_s, out_l, out):
-    n = parts.shape[0]
-
-    def merged(first, width, stat):
-        def stat_of(i, k):
-            at = 192 + stat + 3 * k
-            return (
-                parts[i, :, at : at + 1].astype(jnp.float32)
-                + parts[i, :, at + 1 : at + 2].astype(jnp.float32)
-            ) + parts[i, :, at + 2 : at + 3].astype(jnp.float32)
-
-        tops = [stat_of(i, 0) for i in range(n)]
-        top = tops[0]
-        for t in tops[1:]:
-            top = jnp.maximum(top, t)
-        shares = [stat_of(i, 1) * jnp.exp(tops[i] - top) for i in range(n)]
-        total = sum(shares[1:], shares[0])
-        acc = 0.0
-        for i in range(n):
-            acc = acc + parts[i, :, first : first + width].astype(jnp.float32) * (shares[i] / total)
-        return acc.astype(jnp.bfloat16)
-
-    large = merged(0, 128, 0)
-    small = merged(128, 64, 6)
-    mixed = jnp.dot(small, out_s[...], preferred_element_type=jnp.float32) + jnp.dot(
-        large, out_l[...], preferred_element_type=jnp.float32
-    )
-    out[...] = mixed.astype(jnp.bfloat16)
-
-
-def merge(parts, out_s, out_l):
+def merge_kernel(place, parts, own_s, own_l, their_s, their_l, out):
+    _, _, _, core = where_in(place[0])
+    n_y = parts.shape[0] // 2
+
+    def attended(column):
+        pieces = [parts[2 * i + column].astype(jnp.float32) for i in range(n_y)]
+
+        def merged(first, width, stat):
+            def stat_of(piece, which):
+                at = 192 + stat + 3 * which
+                return (piece[:, at : at + 1] + piece[:, at + 1 : at + 2]) + piece[:, at + 2 : at + 3]
+
+            tops = [stat_of(piece, 0) for piece in pieces]
+            top = tops[0]
+            for t in tops[1:]:
+                top = jnp.maximum(top, t)
+            shares = [stat_of(p, 1) * jnp.exp(t - top) for p, t in zip(pieces, tops)]
+            total = sum(shares[1:], shares[0])
+            acc = 0.0
+            for piece, share in zip(pieces, shares):
+                acc = acc + piece[:, first : first + width] * (share / total)
+            return acc.astype(jnp.bfloat16)
+
+        return merged(0, HEAD_LARGE, 0), merged(HEAD_LARGE, HEAD_SMALL, 6)
+
+    total = None
+    for column, small_w, large_w in ((core, own_s, own_l), (1 - core, their_s, their_l)):
+        large, small = attended(column)
+        term = jnp.dot(large, large_w[...], preferred_element_type=jnp.float32) + jnp.dot(
+            small, small_w[...], preferred_element_type=jnp.float32
+        )
+        total = term if total is None else total + term
+    out[...] = total.astype(jnp.bfloat16)
+
+
+def merge(place, parts, own_s, own_l, their_s, their_l):
     return pl.pallas_call(
         merge_kernel,
-        out_shape=jax.ShapeDtypeStruct((parts.shape[1], out_s.shape[1]), jnp.bfloat16),
-        in_specs=[VMEM] * 3,
+        out_shape=jax.ShapeDtypeStruct((parts.shape[1], own_s.shape[1]), jnp.bfloat16),
+        in_specs=[SMEM] + [VMEM] * 5,
         out_specs=VMEM,
         compiler_params=pltpu.CompilerParams(vmem_limit_bytes=8 * MIB),
         name="merge",
-    )(parts, out_s, out_l)
+    )(place, parts, own_s, own_l, their_s, their_l)
 
 
 def fetch_kernel(weights, out, arrived):
@@ -351,6 +358,9 @@
         over_y.reshape(-1, over_y.shape[2]), "z", axis=0, tiled=True
     )
 
+    their_small = partner(out_small)
+    their_large = partner(out_large)
+
     positions = (z * n_y + y) * row_count + jnp.arange(row_count, dtype=jnp.int32)
     inverse = 1.0 / rope_base ** (jnp.arange(0, ROPE, 2, dtype=jnp.float32) / ROPE)
     angles = positions.astype(jnp.float32)[None, :] * inverse[:, None]
@@ -374,9 +384,9 @@
     other = partner(mine)
 
     partial = attention(place, full, mine, other, value_up_small.T, value_up_large)
-    parts = exchanged(partial, ("yh", "yl"))
-    mixed_part = merge(parts, out_small, out_large)
-    tiles = exchanged(mixed_part.reshape(row_count // rows, rows, d), ("x", "c"))
+    parts = exchanged(partial, ("yh", "yl", "c"))
+    mixed_part = merge(place, parts, out_small, out_large, their_small, their_large)
+    tiles = exchanged(mixed_part.reshape(-1, rows, d), "x")
     mixed = jnp.sum(tiles.astype(jnp.float32), axis=0).astype(jnp.bfloat16)
     stream = (residual.astype(jnp.float32) + mixed.astype(jnp.float32)).astype(jnp.bfloat16)
     as_float = stream.astype(jnp.float32)

time: 162 us -> 162 us (level)
  blocking collectives: 81.7 us -> 72.3 us
  starting transfers between devices: 29.4 us -> 38.4 us
    all_to_all x4 -> x3, blocking collectives: 58.5 us -> 50.6 us  [exchanged(): return lax.all_to_all(chunks, axis, split_axis=0, concat_axis=0, tiled=True)]
    ppermute x3 -> x5, starting transfers between devices: 15.4 us -> 21.8 us  [partner(): return lax.ppermute(x, 'c', [(0, 1), (1, 0)])]
    ppermute x3, waiting for transfers between devices: 4.68 us -> 1.7 us  [shards(): lax.ppermute(query, ('yh', 'yl'), [(i, (i + k) % n_y) for i in range(n_y)])]
    all_to_all x1 -> x2, starting transfers between devices: 5.84 us -> 8.5 us  [exchanged(): return lax.all_to_all(chunks, axis, split_axis=0, concat_axis=0, tiled=True)]
    all_to_all x1 -> x2, waiting for transfers between devices: 9.37 us -> 12 us  [exchanged(): return lax.all_to_all(chunks, axis, split_axis=0, concat_axis=0, tiled=True)]
  transfers between devices with their start and end apart: 8 -> 11, of which waited for: 4 -> 4; matrix products, arithmetic and copies ran while one was open for 0% -> 0% of each run, Pallas kernels for 8% -> 8%
where the time goes in v7:
time: 162 us; the launch traced here: 161 us
  blocking collectives  72.3 us (45%)
  starting transfers between devices  38.4 us (24%)
  Pallas kernels  16.2 us (10%)
  waiting for transfers between devices  14.3 us (9%)
  between operations  13.7 us (8%)
  local copies, waits for them, and re-layouts  4.8 us (3%)
    all_to_all x3, blocking collectives, exchanged(): return lax.all_to_all(chunks, axis, split_axis=0, concat_axis=0, tiled=True)  50.6 us
    all_to_all x2, blocking collectives, from_everyone(): return lax.all_to_all(copies, axis, split_axis=0, concat_axis=0, tiled=True)  21.8 us
    ppermute x5, starting transfers between devices, partner(): return lax.ppermute(x, 'c', [(0, 1), (1, 0)])  21.8 us
    all_to_all x2, waiting for transfers between devices, exchanged(): return lax.all_to_all(chunks, axis, split_axis=0, concat_axis=0, tiled=True)  12 us
    all_to_all x2, starting transfers between devices, exchanged(): return lax.all_to_all(chunks, axis, split_axis=0, concat_axis=0, tiled=True)  8.5 us
    ppermute x3, starting transfers between devices, shards(): lax.ppermute(query, ('yh', 'yl'), [(i, (i + k) % n_y) for i in range(n_y)])  8.15 us
    pallas_call x1, Pallas kernels, attention(): pl.pallas_call(attention_kernel, out_shape=jax.ShapeDtypeStruct((2 * n_y,...  7.63 us
    unnamed x24, local copies, waits for them, and re-layouts  4.67 us
  transfers between devices with their start and end apart: 11, of which 4 were waited for; matrix products, arithmetic and copies ran while one was open for 0% of the time, Pallas kernels for 8%

profile of v7, /device:TPU:1, one launch (start us, length us, event | category | flops | bytes accessed | tf_op | source)
XLA Modules:
  0.0 161.0 jit_solution(12182161198248367757)
XLA Ops:
  6.6 1.7 %pack_weights.1 = bf16[4,32,1152]{2,1,0:T(8,128)(2,1)} custom-call(bf16[32,704]{1,0:T(8,128)(2,1)} %gate.1, bf16[32,704]{1,0:T(8,128)(2,1)} %up.1, bf16[32,704]{1,0:T(8,128)(2,1)} %down.1), custom_call_target="tpu_custom_call" | custom-call | tf_op jit(solution)/shard_map/pack_weights/pallas_call | solution.py:70
  8.3 10.8 %all_to_all.35 = bf16[4,32,1152]{2,1,0:T(8,128)(2,1)} all-to-all(bf16[4,32,1152]{2,1,0:T(8,128)(2,1)} %pack_weights.1), channel_id=1, replica_groups=mesh['z'=16,'yh'=2,'yl'=2,'x'=4,'c'=2] {'yh','yl'}, dimensions={0} | all-to-all | bytes 589824 | tf_op jit(solution)/shard_map/all_to_all | solution.py:39
  22.5 27.1 %all_to_all.36 = bf16[16,40,128]{2,1,0:T(8,128)(2,1)S(1)} all-to-all(bf16[16,40,128]{2,1,0:T(8,128)(2,1)S(1)} %get-tuple-element.10), channel_id=1, replica_groups=mesh['z'=16,'yh'=2,'yl'=2,'x'=4,'c'=2] {'z'}, dimensions={0} | all-to-all | bytes 327680 | tf_op jit(solution)/shard_map/all_to_all | solution.py:39
  49.7 11.6 %all_to_all.37.mine = bf16[4,16,40,128]{3,2,1,0:T(8,128)(2,1)S(1)} all-to-all(bf16[4,16,40,128]{3,2,1,0:T(8,128)(2,1)S(1)} %broadcast_in_dim.4), channel_id=1, replica_groups=mesh['z'=16,'yh'=2,'yl'=2,'x'=4,'c'=2] {'x'}, dimensions={0} | all-to-all | bytes 1310720 | tf_op jit(solution)/shard_map/all_to_all | solution.py:35
  61.3 9.8 %collective-permute-start.3 = (bf16[4,16,40,128]{3,2,1,0:T(8,128)(2,1)S(1)}, bf16[4,16,40,128]{3,2,1,0:T(8,128)(2,1)S(1)}, u32[]{:S(2)}, u32[]{:S(2)}) collective-permute-start(bf16[4,16,40,128]{3,2,1,0:T(8,128)(2,1)S(1)} %all_to_all.37.mine), channel_id=1, source_target_pairs={{0,1},{1,0},{2,3},{3,2},{4,5},{5,4},{6,7},{7,6},{8,9},{9,8},{10,11... | collective-permute-start | bytes 1966088 | tf_op jit(solution)/shard_map/ppermute | solution.py:43
  71.1 1.9 %collective-permute-start.5 = (bf16[128,2048]{1,0:T(8,128)(2,1)}, bf16[128,2048]{1,0:T(8,128)(2,1)S(1)}, u32[]{:S(2)}, u32[]{:S(2)}) collective-permute-start(bf16[128,2048]{1,0:T(8,128)(2,1)} %own_l.1), channel_id=1, source_target_pairs={{0,1},{1,0},{2,3},{3,2},{4,5},{5,4},{6,7},{7,6},{8,9},{9,8},{10,11... | collective-permute-start | bytes 1572872 | tf_op jit(solution)/shard_map/ppermute | solution.py:43
  73.0 2.2 %collective-permute-start.2 = (bf16[128,256]{1,0:T(8,128)(2,1)S(1)}, bf16[128,256]{1,0:T(8,128)(2,1)S(1)}, u32[]{:S(2)}, u32[]{:S(2)}) collective-permute-start(bf16[128,256]{1,0:T(8,128)(2,1)S(1)} %get-tuple-element.9.refs_0_), channel_id=1, source_target_pairs={{0,24},{8,0},{16,8},{24,16},{1,25},{9,1},{17,9},{25,17},{2,26},{10... | collective-permute-start | bytes 196616 | tf_op jit(solution)/shard_map/ppermute | solution.py:379
  75.2 4.0 %collective-permute-start.1 = (bf16[128,256]{1,0:T(8,128)(2,1)S(1)}, bf16[128,256]{1,0:T(8,128)(2,1)S(1)}, u32[]{:S(2)}, u32[]{:S(2)}) collective-permute-start(bf16[128,256]{1,0:T(8,128)(2,1)S(1)} %get-tuple-element.9.refs_0_), channel_id=1, source_target_pairs={{0,16},{8,24},{16,0},{24,8},{1,17},{9,25},{17,1},{25,9},{2,18},{10... | collective-permute-start | bytes 196616 | tf_op jit(solution)/shard_map/ppermute | solution.py:379
  79.3 1.9 %collective-permute-start = (bf16[128,256]{1,0:T(8,128)(2,1)S(1)}, bf16[128,256]{1,0:T(8,128)(2,1)S(1)}, u32[]{:S(2)}, u32[]{:S(2)}) collective-permute-start(bf16[128,256]{1,0:T(8,128)(2,1)S(1)} %get-tuple-element.9.refs_0_), channel_id=1, source_target_pairs={{0,8},{8,16},{16,24},{24,0},{1,9},{9,17},{17,25},{25,1},{2,10},{10... | collective-permute-start | bytes 196616 | tf_op jit(solution)/shard_map/ppermute | solution.py:379
  81.2 3.0 %collective-permute-start.4 = (bf16[64,2048]{1,0:T(8,128)(2,1)}, bf16[64,2048]{1,0:T(8,128)(2,1)S(1)}, u32[]{:S(2)}, u32[]{:S(2)}) collective-permute-start(bf16[64,2048]{1,0:T(8,128)(2,1)} %own_s.1), channel_id=1, source_target_pairs={{0,1},{1,0},{2,3},{3,2},{4,5},{5,4},{6,7},{7,6},{8,9},{9,8},{10,11... | collective-permute-start | bytes 786440 | tf_op jit(solution)/shard_map/ppermute | solution.py:43
  84.2 1.7 %collective-permute-done.refs_1_ = bf16[128,256]{1,0:T(8,128)(2,1)S(1)} collective-permute-done((bf16[128,256]{1,0:T(8,128)(2,1)S(1)}, bf16[128,256]{1,0:T(8,128)(2,1)S(1)}, u32[]{:S(2)}, u32[]{:S(2)}) %collective-permute-start) | collective-permute-done | bytes 65568 | tf_op jit(solution)/shard_map/ppermute | solution.py:379
  87.8 7.6 %attend.1 = bf16[8,64,256]{2,1,0:T(8,128)(2,1)} custom-call(s32[1]{0:T(128)} %bitcast.place, bf16[4,2,128,512]{3,2,1,0:T(8,128)(2,1)S(1)} %absorb.1.query, bf16[4,16,40,128]{3,2,1,0:T(8,128)(2,1)S(1)} %all_to_all.37.mine, bf16[4,16,40,128]{3,2,1,0:T(8,128)(2,1)S(1)} %collective-permute-done.3.other, bf16[64,256]{1,0:T(8,128)(2,1)S(1)} %bitcast.13, ...), custom_call_target="tpu_custom_call" | custom-call | tf_op jit(solution)/shard_map/attend/pallas_call | solution.py:235
  95.5 5.1 %all-to-all-start.2 = ((bf16[8,64,256]{2,1,0:T(8,128)(2,1)}), bf16[8,64,256]{2,1,0:T(8,128)(2,1)S(1)}, u32[]{:S(2)}, u32[]{:S(2)}) async-start(bf16[8,64,256]{2,1,0:T(8,128)(2,1)} %attend.1), calls=%async_computation.2 | async-start | bytes 524288 | tf_op jit(solution)/shard_map/all_to_all | solution.py:39
  100.6 6.5 %all-to-all-done.2.parts = bf16[8,64,256]{2,1,0:T(8,128)(2,1)S(1)} async-done(((bf16[8,64,256]{2,1,0:T(8,128)(2,1)}), bf16[8,64,256]{2,1,0:T(8,128)(2,1)S(1)}, u32[]{:S(2)}, u32[]{:S(2)}) %all-to-all-start.2) | async-done | bytes 262176 | tf_op jit(solution)/shard_map/all_to_all | solution.py:39
  107.1 1.5 merge.1
  108.5 3.4 %all-to-all-start.3 = ((bf16[4,16,2048]{2,1,0:T(8,128)(2,1)}), bf16[4,16,2048]{2,1,0:T(8,128)(2,1)S(1)}, u32[]{:S(2)}, u32[]{:S(2)}) async-start(bf16[4,16,2048]{2,1,0:T(8,128)(2,1)} %bitcast.6), calls=%async_computation.3 | async-start | bytes 524288 | tf_op jit(solution)/shard_map/all_to_all | solution.py:39
  112.0 5.5 %all-to-all-done.3 = bf16[4,16,2048]{2,1,0:T(8,128)(2,1)S(1)} async-done(((bf16[4,16,2048]{2,1,0:T(8,128)(2,1)}), bf16[4,16,2048]{2,1,0:T(8,128)(2,1)S(1)}, u32[]{:S(2)}, u32[]{:S(2)}) %all-to-all-start.3) | async-done | bytes 262176 | tf_op jit(solution)/shard_map/all_to_all | solution.py:39
  117.8 10.2 %all_to_all.38 = bf16[8,16,2048]{2,1,0:T(8,128)(2,1)S(1)} all-to-all(bf16[8,16,2048]{2,1,0:T(8,128)(2,1)S(1)} %broadcast_in_dim.5), channel_id=1, replica_groups=mesh['z'=16,'yh'=2,'yl'=2,'x'=4,'c'=2] {'yl','x'}, dimensions={0} | all-to-all | bytes 1048576 | tf_op jit(solution)/shard_map/all_to_all | solution.py:35
  128.0 5.2 %collective-permute-start.6 = (bf16[128,2048]{1,0:T(8,128)(2,1)S(1)}, bf16[128,2048]{1,0:T(8,128)(2,1)S(1)}, u32[]{:S(2)}, u32[]{:S(2)}) collective-permute-start(bf16[128,2048]{1,0:T(8,128)(2,1)S(1)} %bitcast.10), channel_id=1, source_target_pairs={{0,1},{1,0},{2,3},{3,2},{4,5},{5,4},{6,7},{7,6},{8,9},{9,8},{10,11... | collective-permute-start | bytes 1572872 | tf_op jit(solution)/shard_map/ppermute | solution.py:43
  133.2 2.3 %fetch.1.weights = bf16[2048,1152]{1,0:T(8,128)(2,1)S(1)} custom-call(bf16[2048,1152]{1,0:T(8,128)(2,1)} %all-gather.2.cloned.1.call-done.weights), custom_call_target="tpu_custom_call" | custom-call | tf_op jit(solution)/shard_map/fetch/pallas_call | solution.py:299
  135.5 1.3 shard_map.146
  136.8 1.9 %collective-permute-start.7 = (bf16[128,2048]{1,0:T(8,128)(2,1)S(1)}, bf16[128,2048]{1,0:T(8,128)(2,1)S(1)}, u32[]{:S(2)}, u32[]{:S(2)}) collective-permute-start(bf16[128,2048]{1,0:T(8,128)(2,1)S(1)} %shard_map.146), channel_id=1, source_target_pairs={{0,1},{1,0},{2,3},{3,2},{4,5},{5,4},{6,7},{7,6},{8,9},{9,8},{10,11... | collective-permute-start | bytes 1572872 | tf_op jit(solution)/shard_map/ppermute | solution.py:43
  138.8 1.3 shard_map.145
  140.7 12.6 %all_to_all.39 = bf16[8,16,2048]{2,1,0:T(8,128)(2,1)S(1)} all-to-all(bf16[8,16,2048]{2,1,0:T(8,128)(2,1)S(1)} %bitcast.17), channel_id=1, replica_groups=mesh['z'=16,'yh'=2,'yl'=2,'x'=4,'c'=2] {'yl','x'}, dimensions={0} | all-to-all | bytes 1048576 | tf_op jit(solution)/shard_map/all_to_all | solution.py:39
  (50 shorter events, 7.1 us)
Async XLA Ops:
  6.5 100.5 %copy-start = (bf16[128,2048]{1,0:T(8,128)(2,1)S(1)}, bf16[128,2048]{1,0:T(8,128)(2,1)}, u32[]{:S(2)}) copy-start(bf16[128,2048]{1,0:T(8,128)(2,1)} %own_l.1) | copy-start | bytes 1572868
  6.5 100.5 %copy-start.1 = (bf16[64,2048]{1,0:T(8,128)(2,1)S(1)}, bf16[64,2048]{1,0:T(8,128)(2,1)}, u32[]{:S(2)}) copy-start(bf16[64,2048]{1,0:T(8,128)(2,1)} %own_s.1) | copy-start | bytes 786436
  6.5 81.3 %copy-start.3 = (bf16[256,128]{1,0:T(8,128)(2,1)S(1)}, bf16[256,128]{1,0:T(8,128)(2,1)}, u32[]{:S(2)}) copy-start(bf16[256,128]{1,0:T(8,128)(2,1)} %value_up_l.1) | copy-start | bytes 196612
  6.5 81.3 %copy-start.6 = (bf16[256,64]{0,1:T(8,128)(2,1)S(1)}, bf16[256,64]{0,1:T(8,128)(2,1)}, u32[]{:S(2)}) copy-start(bf16[256,64]{0,1:T(8,128)(2,1)} %param.21) | copy-start | bytes 98308
  6.5 121.4 %all-gather.2.cloned.1.call-start = ((), (), s32[]{:S(2)}) async-start(), calls=%async_computation.7 | async-start | bytes 5013504 | tf_op jit(solution)/shard_map/all_gather | solution.py:357
  19.3 0.8 copy-start.4
  20.1 0.8 copy-start.5
  20.9 0.7 copy-start.8
  21.7 0.7 copy-start.9
  49.7 62.3 %copy-start.11 = (bf16[2048]{0:T(1024)(128)(2,1)S(1)}, bf16[2048]{0:T(1024)(128)(2,1)}, u32[]{:S(2)}) copy-start(bf16[2048]{0:T(1024)(128)(2,1)} %param.26) | copy-start | bytes 12292
  49.7 67.8 %copy-start.10 = (bf16[16,2048]{1,0:T(8,128)(2,1)S(1)}, bf16[16,2048]{1,0:T(8,128)(2,1)}, u32[]{:S(2)}) copy-start(bf16[16,2048]{1,0:T(8,128)(2,1)} %param.15) | copy-start | bytes 196612
  61.3 26.5 %collective-permute-start.3 = (bf16[4,16,40,128]{3,2,1,0:T(8,128)(2,1)S(1)}, bf16[4,16,40,128]{3,2,1,0:T(8,128)(2,1)S(1)}, u32[]{:S(2)}, u32[]{:S(2)}) collective-permute-start(bf16[4,16,40,128]{3,2,1,0:T(8,128)(2,1)S(1)} %all_to_all.37.mine), channel_id=1, source_target_pairs={{0,1},{1,0},{2,3},{3,2},{4,5},{5,4},{6,7},{7,6},{8,9},{9,8},{10,11... | collective-permute-start | bytes 1966088 | tf_op jit(solution)/shard_map/ppermute | solution.py:43
  71.1 29.5 %collective-permute-start.5 = (bf16[128,2048]{1,0:T(8,128)(2,1)}, bf16[128,2048]{1,0:T(8,128)(2,1)S(1)}, u32[]{:S(2)}, u32[]{:S(2)}) collective-permute-start(bf16[128,2048]{1,0:T(8,128)(2,1)} %own_l.1), channel_id=1, source_target_pairs={{0,1},{1,0},{2,3},{3,2},{4,5},{5,4},{6,7},{7,6},{8,9},{9,8},{10,11... | collective-permute-start | bytes 1572872 | tf_op jit(solution)/shard_map/ppermute | solution.py:43
  73.0 8.2 %collective-permute-start.2 = (bf16[128,256]{1,0:T(8,128)(2,1)S(1)}, bf16[128,256]{1,0:T(8,128)(2,1)S(1)}, u32[]{:S(2)}, u32[]{:S(2)}) collective-permute-start(bf16[128,256]{1,0:T(8,128)(2,1)S(1)} %get-tuple-element.9.refs_0_), channel_id=1, source_target_pairs={{0,24},{8,0},{16,8},{24,16},{1,25},{9,1},{17,9},{25,17},{2,26},{10... | collective-permute-start | bytes 196616 | tf_op jit(solution)/shard_map/ppermute | solution.py:379
  75.2 8.9 %collective-permute-start.1 = (bf16[128,256]{1,0:T(8,128)(2,1)S(1)}, bf16[128,256]{1,0:T(8,128)(2,1)S(1)}, u32[]{:S(2)}, u32[]{:S(2)}) collective-permute-start(bf16[128,256]{1,0:T(8,128)(2,1)S(1)} %get-tuple-element.9.refs_0_), channel_id=1, source_target_pairs={{0,16},{8,24},{16,0},{24,8},{1,17},{9,25},{17,1},{25,9},{2,18},{10... | collective-permute-start | bytes 196616 | tf_op jit(solution)/shard_map/ppermute | solution.py:379
  79.3 6.6 %collective-permute-start = (bf16[128,256]{1,0:T(8,128)(2,1)S(1)}, bf16[128,256]{1,0:T(8,128)(2,1)S(1)}, u32[]{:S(2)}, u32[]{:S(2)}) collective-permute-start(bf16[128,256]{1,0:T(8,128)(2,1)S(1)} %get-tuple-element.9.refs_0_), channel_id=1, source_target_pairs={{0,8},{8,16},{16,24},{24,0},{1,9},{9,17},{17,25},{25,1},{2,10},{10... | collective-permute-start | bytes 196616 | tf_op jit(solution)/shard_map/ppermute | solution.py:379
  81.2 19.4 %collective-permute-start.4 = (bf16[64,2048]{1,0:T(8,128)(2,1)}, bf16[64,2048]{1,0:T(8,128)(2,1)S(1)}, u32[]{:S(2)}, u32[]{:S(2)}) collective-permute-start(bf16[64,2048]{1,0:T(8,128)(2,1)} %own_s.1), channel_id=1, source_target_pairs={{0,1},{1,0},{2,3},{3,2},{4,5},{5,4},{6,7},{7,6},{8,9},{9,8},{10,11... | collective-permute-start | bytes 786440 | tf_op jit(solution)/shard_map/ppermute | solution.py:43
  85.9 0.8 copy-start.2
  86.8 0.8 copy-start.7
  95.5 11.6 %all-to-all-start.2 = ((bf16[8,64,256]{2,1,0:T(8,128)(2,1)}), bf16[8,64,256]{2,1,0:T(8,128)(2,1)S(1)}, u32[]{:S(2)}, u32[]{:S(2)}) async-start(bf16[8,64,256]{2,1,0:T(8,128)(2,1)} %attend.1), calls=%async_computation.2 | async-start | bytes 524288 | tf_op jit(solution)/shard_map/all_to_all | solution.py:39
  108.5 8.9 %all-to-all-start.3 = ((bf16[4,16,2048]{2,1,0:T(8,128)(2,1)}), bf16[4,16,2048]{2,1,0:T(8,128)(2,1)S(1)}, u32[]{:S(2)}, u32[]{:S(2)}) async-start(bf16[4,16,2048]{2,1,0:T(8,128)(2,1)} %bitcast.6), calls=%async_computation.3 | async-start | bytes 524288 | tf_op jit(solution)/shard_map/all_to_all | solution.py:39
  128.0 7.5 %collective-permute-start.6 = (bf16[128,2048]{1,0:T(8,128)(2,1)S(1)}, bf16[128,2048]{1,0:T(8,128)(2,1)S(1)}, u32[]{:S(2)}, u32[]{:S(2)}) collective-permute-start(bf16[128,2048]{1,0:T(8,128)(2,1)S(1)} %bitcast.10), channel_id=1, source_target_pairs={{0,1},{1,0},{2,3},{3,2},{4,5},{5,4},{6,7},{7,6},{8,9},{9,8},{10,11... | collective-permute-start | bytes 1572872 | tf_op jit(solution)/shard_map/ppermute | solution.py:43
  136.8 3.8 %collective-permute-start.7 = (bf16[128,2048]{1,0:T(8,128)(2,1)S(1)}, bf16[128,2048]{1,0:T(8,128)(2,1)S(1)}, u32[]{:S(2)}, u32[]{:S(2)}) collective-permute-start(bf16[128,2048]{1,0:T(8,128)(2,1)S(1)} %shard_map.146), channel_id=1, source_target_pairs={{0,1},{1,0},{2,3},{3,2},{4,5},{5,4},{6,7},{7,6},{8,9},{9,8},{10,11... | collective-permute-start | bytes 1572872 | tf_op jit(solution)/shard_map/ppermute | solution.py:43
Sparse Core Ops, SparseCore 0:
  19.3 79.8 all-gather.1

commit v8 on v7

--- a/solution.py
+++ b/solution.py
@@ -90,11 +90,9 @@
             [leading * cosine - trailing * sine, trailing * cosine + leading * sine], axis=0
         )
 
-    tall[0:256, :] = latent[...].astype(jnp.float32).T
-    tall[256 : 256 + ROPE, :] = turn(rope_key[...])
+    tall[...] = latent[...].astype(jnp.float32).T
     mine = tall[pl.ds(pl.multiple_of(64 * x + 32 * core, 32), 32), :]
-    ours = tall[pl.ds(pl.multiple_of(256 + 8 * x, 8), 8), :]
-    piece = jnp.concatenate([mine, ours], axis=0).astype(jnp.bfloat16)
+    piece = jnp.concatenate([mine, turn(rope_key[...])], axis=0).astype(jnp.bfloat16)
     for k in range(packed.shape[0]):
         packed[k] = piece
     upright = jnp.concatenate(
@@ -115,11 +113,11 @@
         prepare_kernel,
         out_shape=(
             jax.ShapeDtypeStruct((rows, 256), jnp.bfloat16),
-            jax.ShapeDtypeStruct((n_z, 40, rows), jnp.bfloat16),
+            jax.ShapeDtypeStruct((n_z, 32 + ROPE, rows), jnp.bfloat16),
         ),
         in_specs=[SMEM] + [VMEM] * 6,
         out_specs=(VMEM, VMEM),
-        scratch_shapes=[pltpu.VMEM((256 + ROPE, rows), jnp.float32)],
+        scratch_shapes=[pltpu.VMEM((256, rows), jnp.float32)],
         compiler_params=pltpu.CompilerParams(vmem_limit_bytes=4 * MIB),
         name="prepare",
     )(place, small, large, latent, rope_key, cosine, sine)
@@ -179,7 +177,7 @@
     )(place, query, key_up_s, key_up_l)
 
 
-def attention_kernel(place, query, mine, other, value_up_s, value_up_l, out, keys):
+def attention_kernel(place, query, mine, other, ropes, value_up_s, value_up_l, out, keys):
     z, y, _, c = where_in(place[0])
     n_x, n_z = mine.shape[0], mine.shape[1]
     n_y = query.shape[0]
@@ -190,10 +188,9 @@
         for x in range(n_x):
             here = pl.multiple_of(64 * x + 32 * c, 32)
             there = pl.multiple_of(64 * x + 32 * (1 - c), 32)
-            keys[pl.ds(here, 32), lanes] = mine[x, k, 0:32, :]
-            keys[pl.ds(there, 32), lanes] = other[x, k, 0:32, :]
-        ropes = [mine[x, k, 32:40, :].astype(jnp.float32) for x in range(n_x)]
-        keys[256 : 256 + ROPE, lanes] = jnp.concatenate(ropes, axis=0).astype(jnp.bfloat16)
+            keys[pl.ds(here, 32), lanes] = mine[x, k]
+            keys[pl.ds(there, 32), lanes] = other[x, k]
+        keys[256 : 256 + ROPE, lanes] = ropes[k, 32:, :]
         hidden_from = (k > z) | ((k == z) & (y > row))
         bias = jnp.where(hidden_from & (row < n_y), big_negative, 0.0)
         keys[288:384, lanes] = bias[0:96, :].astype(jnp.bfloat16)
@@ -229,18 +226,18 @@
             out[2 * j + core] = jnp.concatenate(picked, axis=0).astype(jnp.bfloat16)
 
 
-def attention(place, query, mine, other, value_up_s, value_up_l):
+def attention(place, query, mine, other, ropes, value_up_s, value_up_l):
     n_y, _, rows, depth = query.shape
     n_keys = 128 * mine.shape[1]
     return pl.pallas_call(
         attention_kernel,
         out_shape=jax.ShapeDtypeStruct((2 * n_y, rows // 2, 256), jnp.bfloat16),
-        in_specs=[SMEM] + [VMEM] * 5,
+        in_specs=[SMEM] + [VMEM] * 6,
         out_specs=VMEM,
         scratch_shapes=[pltpu.VMEM((depth, n_keys), jnp.bfloat16)],
         compiler_params=pltpu.CompilerParams(vmem_limit_bytes=36 * MIB),
         name="attend",
-    )(place, query, mine, other, value_up_s, value_up_l)
+    )(place, query, mine, other, ropes, value_up_s, value_up_l)
 
 
 def merge_kernel(place, parts, own_s, own_l, their_s, their_l, out):
@@ -380,10 +377,10 @@
         for k in range(1, n_y)
     ]
     full = absorb(place, join(place, queries), key_up_small.T, key_up_large)
-    mine = from_everyone(along_z, "x")
+    mine = from_everyone(along_z[:, :32], "x")
     other = partner(mine)
 
-    partial = attention(place, full, mine, other, value_up_small.T, value_up_large)
+    partial = attention(place, full, mine, other, along_z, value_up_small.T, value_up_large)
     parts = exchanged(partial, ("yh", "yl", "c"))
     mixed_part = merge(place, parts, out_small, out_large, their_small, their_large)
     tiles = exchanged(mixed_part.reshape(-1, rows, d), "x")
@@ -391,7 +388,8 @@
     stream = (residual.astype(jnp.float32) + mixed.astype(jnp.float32)).astype(jnp.bfloat16)
     as_float = stream.astype(jnp.float32)
     normed = as_float * lax.rsqrt(jnp.mean(as_float * as_float, axis=-1, keepdims=True) + norm_eps)
-    normed = (normed * norm_gain.astype(jnp.float32)[None, :]).astype(jnp.bfloat16)
+    gain = norm_gain.astype(jnp.float32)
+    normed = (normed * gain[None, :]).astype(jnp.bfloat16)
 
     here = from_everyone(normed, ("yl", "x")).reshape(-1, d)
     here, weights = lax.optimization_barrier((here, weights))

time: 162 us -> 164 us (1.012)
  starting transfers between devices: 38.4 us -> 40.5 us
    ppermute x5, starting transfers between devices: 21.8 us -> 24.6 us  [partner(): return lax.ppermute(x, 'c', [(0, 1), (1, 0)])]
where the time goes in v8:
time: 164 us; the launch traced here: 163 us
  blocking collectives  72.4 us (44%)
  starting transfers between devices  40.5 us (25%)
  Pallas kernels  16.2 us (10%)
  waiting for transfers between devices  14.3 us (9%)
  between operations  13.7 us (8%)
  local copies, waits for them, and re-layouts  4.8 us (3%)
    all_to_all x3, blocking collectives, exchanged(): return lax.all_to_all(chunks, axis, split_axis=0, concat_axis=0, tiled=True)  51.1 us
    ppermute x5, starting transfers between devices, partner(): return lax.ppermute(x, 'c', [(0, 1), (1, 0)])  24.6 us
    all_to_all x2, blocking collectives, from_everyone(): return lax.all_to_all(copies, axis, split_axis=0, concat_axis=0, tiled=True)  21.3 us
    all_to_all x2, waiting for transfers between devices, exchanged(): return lax.all_to_all(chunks, axis, split_axis=0, concat_axis=0, tiled=True)  12 us
    all_to_all x2, starting transfers between devices, exchanged(): return lax.all_to_all(chunks, axis, split_axis=0, concat_axis=0, tiled=True)  8.49 us
    pallas_call x1, Pallas kernels, attention(): pl.pallas_call(attention_kernel, out_shape=jax.ShapeDtypeStruct((2 * n_y,...  7.65 us
    ppermute x3, starting transfers between devices, shards(): lax.ppermute(query, ('yh', 'yl'), [(i, (i + k) % n_y) for i in range(n_y)])  7.32 us
    unnamed x24, local copies, waits for them, and re-layouts  4.67 us
  transfers between devices with their start and end apart: 11, of which 4 were waited for; matrix products, arithmetic and copies ran while one was open for 0% of the time, Pallas kernels for 8%

profile of v8, /device:TPU:1, one launch (start us, length us, event | category | flops | bytes accessed | tf_op | source)
XLA Modules:
  0.0 163.2 jit_solution(14588901401880558585)
XLA Ops:
  6.6 1.7 %pack_weights.1 = bf16[4,32,1152]{2,1,0:T(8,128)(2,1)} custom-call(bf16[32,704]{1,0:T(8,128)(2,1)} %gate.1, bf16[32,704]{1,0:T(8,128)(2,1)} %up.1, bf16[32,704]{1,0:T(8,128)(2,1)} %down.1), custom_call_target="tpu_custom_call" | custom-call | tf_op jit(solution)/shard_map/pack_weights/pallas_call | solution.py:70
  8.3 10.8 %all_to_all.35 = bf16[4,32,1152]{2,1,0:T(8,128)(2,1)} all-to-all(bf16[4,32,1152]{2,1,0:T(8,128)(2,1)} %pack_weights.1), channel_id=1, replica_groups=mesh['z'=16,'yh'=2,'yl'=2,'x'=4,'c'=2] {'yh','yl'}, dimensions={0} | all-to-all | bytes 589824 | tf_op jit(solution)/shard_map/all_to_all | solution.py:39
  22.5 27.6 %all_to_all.36.ropes = bf16[16,64,128]{2,1,0:T(8,128)(2,1)S(1)} all-to-all(bf16[16,64,128]{2,1,0:T(8,128)(2,1)S(1)} %get-tuple-element.10), channel_id=1, replica_groups=mesh['z'=16,'yh'=2,'yl'=2,'x'=4,'c'=2] {'z'}, dimensions={0} | all-to-all | bytes 524288 | tf_op jit(solution)/shard_map/all_to_all | solution.py:39
  50.2 10.9 %all_to_all.37.mine = bf16[4,16,32,128]{3,2,1,0:T(8,128)(2,1)S(1)} all-to-all(bf16[4,16,32,128]{3,2,1,0:T(8,128)(2,1)S(1)} %broadcast_in_dim.4), channel_id=1, replica_groups=mesh['z'=16,'yh'=2,'yl'=2,'x'=4,'c'=2] {'x'}, dimensions={0} | all-to-all | bytes 1048576 | tf_op jit(solution)/shard_map/all_to_all | solution.py:35
  61.1 12.8 %collective-permute-start.3 = (bf16[4,16,32,128]{3,2,1,0:T(8,128)(2,1)S(1)}, bf16[4,16,32,128]{3,2,1,0:T(8,128)(2,1)S(1)}, u32[]{:S(2)}, u32[]{:S(2)}) collective-permute-start(bf16[4,16,32,128]{3,2,1,0:T(8,128)(2,1)S(1)} %all_to_all.37.mine), channel_id=1, source_target_pairs={{0,1},{1,0},{2,3},{3,2},{4,5},{5,4},{6,7},{7,6},{8,9},{9,8},{10,11... | collective-permute-start | bytes 1572872 | tf_op jit(solution)/shard_map/ppermute | solution.py:43
  73.9 1.9 %collective-permute-start.5 = (bf16[128,2048]{1,0:T(8,128)(2,1)}, bf16[128,2048]{1,0:T(8,128)(2,1)S(1)}, u32[]{:S(2)}, u32[]{:S(2)}) collective-permute-start(bf16[128,2048]{1,0:T(8,128)(2,1)} %own_l.1), channel_id=1, source_target_pairs={{0,1},{1,0},{2,3},{3,2},{4,5},{5,4},{6,7},{7,6},{8,9},{9,8},{10,11... | collective-permute-start | bytes 1572872 | tf_op jit(solution)/shard_map/ppermute | solution.py:43
  75.9 2.3 %collective-permute-start.2 = (bf16[128,256]{1,0:T(8,128)(2,1)S(1)}, bf16[128,256]{1,0:T(8,128)(2,1)S(1)}, u32[]{:S(2)}, u32[]{:S(2)}) collective-permute-start(bf16[128,256]{1,0:T(8,128)(2,1)S(1)} %get-tuple-element.9.refs_0_), channel_id=1, source_target_pairs={{0,24},{8,0},{16,8},{24,16},{1,25},{9,1},{17,9},{25,17},{2,26},{10... | collective-permute-start | bytes 196616 | tf_op jit(solution)/shard_map/ppermute | solution.py:376
  78.2 3.1 %collective-permute-start.1 = (bf16[128,256]{1,0:T(8,128)(2,1)S(1)}, bf16[128,256]{1,0:T(8,128)(2,1)S(1)}, u32[]{:S(2)}, u32[]{:S(2)}) collective-permute-start(bf16[128,256]{1,0:T(8,128)(2,1)S(1)} %get-tuple-element.9.refs_0_), channel_id=1, source_target_pairs={{0,16},{8,24},{16,0},{24,8},{1,17},{9,25},{17,1},{25,9},{2,18},{10... | collective-permute-start | bytes 196616 | tf_op jit(solution)/shard_map/ppermute | solution.py:376
  81.3 1.9 %collective-permute-start = (bf16[128,256]{1,0:T(8,128)(2,1)S(1)}, bf16[128,256]{1,0:T(8,128)(2,1)S(1)}, u32[]{:S(2)}, u32[]{:S(2)}) collective-permute-start(bf16[128,256]{1,0:T(8,128)(2,1)S(1)} %get-tuple-element.9.refs_0_), channel_id=1, source_target_pairs={{0,8},{8,16},{16,24},{24,0},{1,9},{9,17},{17,25},{25,1},{2,10},{10... | collective-permute-start | bytes 196616 | tf_op jit(solution)/shard_map/ppermute | solution.py:376
  83.2 3.0 %collective-permute-start.4 = (bf16[64,2048]{1,0:T(8,128)(2,1)}, bf16[64,2048]{1,0:T(8,128)(2,1)S(1)}, u32[]{:S(2)}, u32[]{:S(2)}) collective-permute-start(bf16[64,2048]{1,0:T(8,128)(2,1)} %own_s.1), channel_id=1, source_target_pairs={{0,1},{1,0},{2,3},{3,2},{4,5},{5,4},{6,7},{7,6},{8,9},{9,8},{10,11... | collective-permute-start | bytes 786440 | tf_op jit(solution)/shard_map/ppermute | solution.py:43
  86.2 1.7 %collective-permute-done.refs_1_ = bf16[128,256]{1,0:T(8,128)(2,1)S(1)} collective-permute-done((bf16[128,256]{1,0:T(8,128)(2,1)S(1)}, bf16[128,256]{1,0:T(8,128)(2,1)S(1)}, u32[]{:S(2)}, u32[]{:S(2)}) %collective-permute-start) | collective-permute-done | bytes 65568 | tf_op jit(solution)/shard_map/ppermute | solution.py:376
  89.9 7.6 %attend.1 = bf16[8,64,256]{2,1,0:T(8,128)(2,1)} custom-call(s32[1]{0:T(128)} %bitcast.place, bf16[4,2,128,512]{3,2,1,0:T(8,128)(2,1)S(1)} %absorb.1.query, bf16[4,16,32,128]{3,2,1,0:T(8,128)(2,1)S(1)} %all_to_all.37.mine, bf16[4,16,32,128]{3,2,1,0:T(8,128)(2,1)S(1)} %collective-permute-done.3.other, bf16[16,64,128]{2,1,0:T(8,128)(2,1)S(1)} %all_to_all.36.ropes, ...), custom_call_target="tpu_custom_call" | custom-call | tf_op jit(solution)/shard_map/attend/pallas_call | solution.py:232
  97.5 5.1 %all-to-all-start.2 = ((bf16[8,64,256]{2,1,0:T(8,128)(2,1)}), bf16[8,64,256]{2,1,0:T(8,128)(2,1)S(1)}, u32[]{:S(2)}, u32[]{:S(2)}) async-start(bf16[8,64,256]{2,1,0:T(8,128)(2,1)} %attend.1), calls=%async_computation.2 | async-start | bytes 524288 | tf_op jit(solution)/shard_map/all_to_all | solution.py:39
  102.6 6.5 %all-to-all-done.2.parts = bf16[8,64,256]{2,1,0:T(8,128)(2,1)S(1)} async-done(((bf16[8,64,256]{2,1,0:T(8,128)(2,1)}), bf16[8,64,256]{2,1,0:T(8,128)(2,1)S(1)}, u32[]{:S(2)}, u32[]{:S(2)}) %all-to-all-start.2) | async-done | bytes 262176 | tf_op jit(solution)/shard_map/all_to_all | solution.py:39
  109.1 1.5 merge.1
  110.6 3.4 %all-to-all-start.3 = ((bf16[4,16,2048]{2,1,0:T(8,128)(2,1)}), bf16[4,16,2048]{2,1,0:T(8,128)(2,1)S(1)}, u32[]{:S(2)}, u32[]{:S(2)}) async-start(bf16[4,16,2048]{2,1,0:T(8,128)(2,1)} %bitcast.6), calls=%async_computation.3 | async-start | bytes 524288 | tf_op jit(solution)/shard_map/all_to_all | solution.py:39
  114.1 5.5 %all-to-all-done.3 = bf16[4,16,2048]{2,1,0:T(8,128)(2,1)S(1)} async-done(((bf16[4,16,2048]{2,1,0:T(8,128)(2,1)}), bf16[4,16,2048]{2,1,0:T(8,128)(2,1)S(1)}, u32[]{:S(2)}, u32[]{:S(2)}) %all-to-all-start.3) | async-done | bytes 262176 | tf_op jit(solution)/shard_map/all_to_all | solution.py:39
  119.9 10.5 %all_to_all.38 = bf16[8,16,2048]{2,1,0:T(8,128)(2,1)S(1)} all-to-all(bf16[8,16,2048]{2,1,0:T(8,128)(2,1)S(1)} %broadcast_in_dim.5), channel_id=1, replica_groups=mesh['z'=16,'yh'=2,'yl'=2,'x'=4,'c'=2] {'yl','x'}, dimensions={0} | all-to-all | bytes 1048576 | tf_op jit(solution)/shard_map/all_to_all | solution.py:35
  130.4 5.0 %collective-permute-start.6 = (bf16[128,2048]{1,0:T(8,128)(2,1)S(1)}, bf16[128,2048]{1,0:T(8,128)(2,1)S(1)}, u32[]{:S(2)}, u32[]{:S(2)}) collective-permute-start(bf16[128,2048]{1,0:T(8,128)(2,1)S(1)} %bitcast.10), channel_id=1, source_target_pairs={{0,1},{1,0},{2,3},{3,2},{4,5},{5,4},{6,7},{7,6},{8,9},{9,8},{10,11... | collective-permute-start | bytes 1572872 | tf_op jit(solution)/shard_map/ppermute | solution.py:43
  135.4 2.3 %fetch.1.weights = bf16[2048,1152]{1,0:T(8,128)(2,1)S(1)} custom-call(bf16[2048,1152]{1,0:T(8,128)(2,1)} %all-gather.2.cloned.1.call-done.weights), custom_call_target="tpu_custom_call" | custom-call | tf_op jit(solution)/shard_map/fetch/pallas_call | solution.py:296
  137.7 1.3 shard_map.146
  139.0 1.9 %collective-permute-start.7 = (bf16[128,2048]{1,0:T(8,128)(2,1)S(1)}, bf16[128,2048]{1,0:T(8,128)(2,1)S(1)}, u32[]{:S(2)}, u32[]{:S(2)}) collective-permute-start(bf16[128,2048]{1,0:T(8,128)(2,1)S(1)} %shard_map.146), channel_id=1, source_target_pairs={{0,1},{1,0},{2,3},{3,2},{4,5},{5,4},{6,7},{7,6},{8,9},{9,8},{10,11... | collective-permute-start | bytes 1572872 | tf_op jit(solution)/shard_map/ppermute | solution.py:43
  141.0 1.3 shard_map.145
  142.9 12.6 %all_to_all.39 = bf16[8,16,2048]{2,1,0:T(8,128)(2,1)S(1)} all-to-all(bf16[8,16,2048]{2,1,0:T(8,128)(2,1)S(1)} %bitcast.17), channel_id=1, replica_groups=mesh['z'=16,'yh'=2,'yl'=2,'x'=4,'c'=2] {'yl','x'}, dimensions={0} | all-to-all | bytes 1048576 | tf_op jit(solution)/shard_map/all_to_all | solution.py:39
  (51 shorter events, 7.1 us)
Async XLA Ops:
  6.5 102.6 %copy-start = (bf16[128,2048]{1,0:T(8,128)(2,1)S(1)}, bf16[128,2048]{1,0:T(8,128)(2,1)}, u32[]{:S(2)}) copy-start(bf16[128,2048]{1,0:T(8,128)(2,1)} %own_l.1) | copy-start | bytes 1572868
  6.5 102.6 %copy-start.1 = (bf16[64,2048]{1,0:T(8,128)(2,1)S(1)}, bf16[64,2048]{1,0:T(8,128)(2,1)}, u32[]{:S(2)}) copy-start(bf16[64,2048]{1,0:T(8,128)(2,1)} %own_s.1) | copy-start | bytes 786436
  6.5 83.3 %copy-start.3 = (bf16[256,128]{1,0:T(8,128)(2,1)S(1)}, bf16[256,128]{1,0:T(8,128)(2,1)}, u32[]{:S(2)}) copy-start(bf16[256,128]{1,0:T(8,128)(2,1)} %value_up_l.1) | copy-start | bytes 196612
  6.5 83.3 %copy-start.6 = (bf16[256,64]{0,1:T(8,128)(2,1)S(1)}, bf16[256,64]{0,1:T(8,128)(2,1)}, u32[]{:S(2)}) copy-start(bf16[256,64]{0,1:T(8,128)(2,1)} %param.21) | copy-start | bytes 98308
  6.5 123.8 %all-gather.2.cloned.1.call-start = ((), (), s32[]{:S(2)}) async-start(), calls=%async_computation.7 | async-start | bytes 5013504 | tf_op jit(solution)/shard_map/all_gather | solution.py:354
  19.3 0.8 copy-start.4
  20.1 0.8 copy-start.5
  20.9 0.7 copy-start.8
  21.7 0.7 copy-start.9
  50.1 63.9 %copy-start.11 = (bf16[2048]{0:T(1024)(128)(2,1)S(1)}, bf16[2048]{0:T(1024)(128)(2,1)}, u32[]{:S(2)}) copy-start(bf16[2048]{0:T(1024)(128)(2,1)} %param.26) | copy-start | bytes 12292
  50.2 69.4 %copy-start.10 = (bf16[16,2048]{1,0:T(8,128)(2,1)S(1)}, bf16[16,2048]{1,0:T(8,128)(2,1)}, u32[]{:S(2)}) copy-start(bf16[16,2048]{1,0:T(8,128)(2,1)} %param.15) | copy-start | bytes 196612
  61.1 28.7 %collective-permute-start.3 = (bf16[4,16,32,128]{3,2,1,0:T(8,128)(2,1)S(1)}, bf16[4,16,32,128]{3,2,1,0:T(8,128)(2,1)S(1)}, u32[]{:S(2)}, u32[]{:S(2)}) collective-permute-start(bf16[4,16,32,128]{3,2,1,0:T(8,128)(2,1)S(1)} %all_to_all.37.mine), channel_id=1, source_target_pairs={{0,1},{1,0},{2,3},{3,2},{4,5},{5,4},{6,7},{7,6},{8,9},{9,8},{10,11... | collective-permute-start | bytes 1572872 | tf_op jit(solution)/shard_map/ppermute | solution.py:43
  73.9 28.7 %collective-permute-start.5 = (bf16[128,2048]{1,0:T(8,128)(2,1)}, bf16[128,2048]{1,0:T(8,128)(2,1)S(1)}, u32[]{:S(2)}, u32[]{:S(2)}) collective-permute-start(bf16[128,2048]{1,0:T(8,128)(2,1)} %own_l.1), channel_id=1, source_target_pairs={{0,1},{1,0},{2,3},{3,2},{4,5},{5,4},{6,7},{7,6},{8,9},{9,8},{10,11... | collective-permute-start | bytes 1572872 | tf_op jit(solution)/shard_map/ppermute | solution.py:43
  75.9 7.3 %collective-permute-start.2 = (bf16[128,256]{1,0:T(8,128)(2,1)S(1)}, bf16[128,256]{1,0:T(8,128)(2,1)S(1)}, u32[]{:S(2)}, u32[]{:S(2)}) collective-permute-start(bf16[128,256]{1,0:T(8,128)(2,1)S(1)} %get-tuple-element.9.refs_0_), channel_id=1, source_target_pairs={{0,24},{8,0},{16,8},{24,16},{1,25},{9,1},{17,9},{25,17},{2,26},{10... | collective-permute-start | bytes 196616 | tf_op jit(solution)/shard_map/ppermute | solution.py:376
  78.2 8.0 %collective-permute-start.1 = (bf16[128,256]{1,0:T(8,128)(2,1)S(1)}, bf16[128,256]{1,0:T(8,128)(2,1)S(1)}, u32[]{:S(2)}, u32[]{:S(2)}) collective-permute-start(bf16[128,256]{1,0:T(8,128)(2,1)S(1)} %get-tuple-element.9.refs_0_), channel_id=1, source_target_pairs={{0,16},{8,24},{16,0},{24,8},{1,17},{9,25},{17,1},{25,9},{2,18},{10... | collective-permute-start | bytes 196616 | tf_op jit(solution)/shard_map/ppermute | solution.py:376
  81.3 6.6 %collective-permute-start = (bf16[128,256]{1,0:T(8,128)(2,1)S(1)}, bf16[128,256]{1,0:T(8,128)(2,1)S(1)}, u32[]{:S(2)}, u32[]{:S(2)}) collective-permute-start(bf16[128,256]{1,0:T(8,128)(2,1)S(1)} %get-tuple-element.9.refs_0_), channel_id=1, source_target_pairs={{0,8},{8,16},{16,24},{24,0},{1,9},{9,17},{17,25},{25,1},{2,10},{10... | collective-permute-start | bytes 196616 | tf_op jit(solution)/shard_map/ppermute | solution.py:376
  83.2 19.4 %collective-permute-start.4 = (bf16[64,2048]{1,0:T(8,128)(2,1)}, bf16[64,2048]{1,0:T(8,128)(2,1)S(1)}, u32[]{:S(2)}, u32[]{:S(2)}) collective-permute-start(bf16[64,2048]{1,0:T(8,128)(2,1)} %own_s.1), channel_id=1, source_target_pairs={{0,1},{1,0},{2,3},{3,2},{4,5},{5,4},{6,7},{7,6},{8,9},{9,8},{10,11... | collective-permute-start | bytes 786440 | tf_op jit(solution)/shard_map/ppermute | solution.py:43
  87.9 0.8 copy-start.2
  88.8 0.8 copy-start.7
  97.5 11.6 %all-to-all-start.2 = ((bf16[8,64,256]{2,1,0:T(8,128)(2,1)}), bf16[8,64,256]{2,1,0:T(8,128)(2,1)S(1)}, u32[]{:S(2)}, u32[]{:S(2)}) async-start(bf16[8,64,256]{2,1,0:T(8,128)(2,1)} %attend.1), calls=%async_computation.2 | async-start | bytes 524288 | tf_op jit(solution)/shard_map/all_to_all | solution.py:39
  110.6 8.9 %all-to-all-start.3 = ((bf16[4,16,2048]{2,1,0:T(8,128)(2,1)}), bf16[4,16,2048]{2,1,0:T(8,128)(2,1)S(1)}, u32[]{:S(2)}, u32[]{:S(2)}) async-start(bf16[4,16,2048]{2,1,0:T(8,128)(2,1)} %bitcast.6), calls=%async_computation.3 | async-start | bytes 524288 | tf_op jit(solution)/shard_map/all_to_all | solution.py:39
  130.4 7.4 %collective-permute-start.6 = (bf16[128,2048]{1,0:T(8,128)(2,1)S(1)}, bf16[128,2048]{1,0:T(8,128)(2,1)S(1)}, u32[]{:S(2)}, u32[]{:S(2)}) collective-permute-start(bf16[128,2048]{1,0:T(8,128)(2,1)S(1)} %bitcast.10), channel_id=1, source_target_pairs={{0,1},{1,0},{2,3},{3,2},{4,5},{5,4},{6,7},{7,6},{8,9},{9,8},{10,11... | collective-permute-start | bytes 1572872 | tf_op jit(solution)/shard_map/ppermute | solution.py:43
  139.0 3.8 %collective-permute-start.7 = (bf16[128,2048]{1,0:T(8,128)(2,1)S(1)}, bf16[128,2048]{1,0:T(8,128)(2,1)S(1)}, u32[]{:S(2)}, u32[]{:S(2)}) collective-permute-start(bf16[128,2048]{1,0:T(8,128)(2,1)S(1)} %shard_map.146), channel_id=1, source_target_pairs={{0,1},{1,0},{2,3},{3,2},{4,5},{5,4},{6,7},{7,6},{8,9},{9,8},{10,11... | collective-permute-start | bytes 1572872 | tf_op jit(solution)/shard_map/ppermute | solution.py:43
Sparse Core Ops, SparseCore 0:
  19.3 83.8 all-gather.1

commit v9 on v8

--- a/solution.py
+++ b/solution.py
@@ -55,14 +55,13 @@
     cut = gate.shape[1] // 2
     room = out.shape[2] // 3
     depth = gate.shape[0]
-    blank = jnp.zeros((depth, room - cut), jnp.float32)
+    blank = jnp.zeros((depth, room - cut), jnp.bfloat16)
     for k, w in enumerate((gate, up, down)):
-        whole = w[...].astype(jnp.float32)
-        for j in range(2):
-            half = jnp.concatenate([whole[:, cut * j : cut * (j + 1)], blank], axis=1)
-            half = half.astype(jnp.bfloat16)
-            for i in range(out.shape[0] // 2):
-                out[2 * i + j, :, room * k : room * (k + 1)] = half
+        first = jnp.concatenate([w[:, 0:cut], blank], axis=1)
+        second = jnp.concatenate([w[:, cut:], blank], axis=1)
+        for i in range(out.shape[0] // 2):
+            out[2 * i, :, room * k : room * (k + 1)] = first
+            out[2 * i + 1, :, room * k : room * (k + 1)] = second
 
 
 def pack_weights(gate, up, down, n_y):
@@ -287,9 +286,18 @@
 
 
 def fetch_kernel(weights, out, arrived):
-    copy = pltpu.make_async_copy(weights, out, arrived)
-    copy.start()
-    copy.wait()
+    pieces = arrived.shape[0]
+    rows = weights.shape[0] // pieces
+    copies = [
+        pltpu.make_async_copy(
+            weights.at[pl.ds(rows * i, rows), :], out.at[pl.ds(rows * i, rows), :], arrived.at[i]
+        )
+        for i in range(pieces)
+    ]
+    for copy in copies:
+        copy.start()
+    for copy in copies:
+        copy.wait()
 
 
 def fetch(weights):
@@ -298,7 +306,7 @@
         out_shape=jax.ShapeDtypeStruct(weights.shape, weights.dtype),
         in_specs=[pl.BlockSpec(memory_space=pltpu.HBM)],
         out_specs=VMEM,
-        scratch_shapes=[pltpu.SemaphoreType.DMA],
+        scratch_shapes=[pltpu.SemaphoreType.DMA((4,))],
         compiler_params=pltpu.CompilerParams(vmem_limit_bytes=46 * MIB),
         name="fetch",
     )(weights)

time: 164 us -> 164 us (level)
  no operation moved by 1% of the time
where the time goes in v9:
time: 164 us; the launch traced here: 163 us
  blocking collectives  72.3 us (44%)
  starting transfers between devices  40.5 us (25%)
  Pallas kernels  16.2 us (10%)
  waiting for transfers between devices  14.3 us (9%)
  between operations  13.7 us (8%)
  local copies, waits for them, and re-layouts  4.8 us (3%)
    all_to_all x3, blocking collectives, exchanged(): return lax.all_to_all(chunks, axis, split_axis=0, concat_axis=0, tiled=True)  51.1 us
    ppermute x5, starting transfers between devices, partner(): return lax.ppermute(x, 'c', [(0, 1), (1, 0)])  24.7 us
    all_to_all x2, blocking collectives, from_everyone(): return lax.all_to_all(copies, axis, split_axis=0, concat_axis=0, tiled=True)  21.3 us
    all_to_all x2, waiting for transfers between devices, exchanged(): return lax.all_to_all(chunks, axis, split_axis=0, concat_axis=0, tiled=True)  12 us
    all_to_all x2, starting transfers between devices, exchanged(): return lax.all_to_all(chunks, axis, split_axis=0, concat_axis=0, tiled=True)  8.5 us
    pallas_call x1, Pallas kernels, attention(): pl.pallas_call(attention_kernel, out_shape=jax.ShapeDtypeStruct((2 * n_y,...  7.64 us
    ppermute x3, starting transfers between devices, shards(): lax.ppermute(query, ('yh', 'yl'), [(i, (i + k) % n_y) for i in range(n_y)])  7.32 us
    unnamed x24, local copies, waits for them, and re-layouts  4.67 us
  transfers between devices with their start and end apart: 11, of which 4 were waited for; matrix products, arithmetic and copies ran while one was open for 0% of the time, Pallas kernels for 8%

profile of v9, /device:TPU:1, one launch (start us, length us, event | category | flops | bytes accessed | tf_op | source)
XLA Modules:
  0.0 163.2 jit_solution(15002886937675027847)
XLA Ops:
  6.6 1.7 %pack_weights.1 = bf16[4,32,1152]{2,1,0:T(8,128)(2,1)} custom-call(bf16[32,704]{1,0:T(8,128)(2,1)} %gate.1, bf16[32,704]{1,0:T(8,128)(2,1)} %up.1, bf16[32,704]{1,0:T(8,128)(2,1)} %down.1), custom_call_target="tpu_custom_call" | custom-call | tf_op jit(solution)/shard_map/pack_weights/pallas_call | solution.py:69
  8.3 10.8 %all_to_all.35 = bf16[4,32,1152]{2,1,0:T(8,128)(2,1)} all-to-all(bf16[4,32,1152]{2,1,0:T(8,128)(2,1)} %pack_weights.1), channel_id=1, replica_groups=mesh['z'=16,'yh'=2,'yl'=2,'x'=4,'c'=2] {'yh','yl'}, dimensions={0} | all-to-all | bytes 589824 | tf_op jit(solution)/shard_map/all_to_all | solution.py:39
  22.5 27.6 %all_to_all.36.ropes = bf16[16,64,128]{2,1,0:T(8,128)(2,1)S(1)} all-to-all(bf16[16,64,128]{2,1,0:T(8,128)(2,1)S(1)} %get-tuple-element.10), channel_id=1, replica_groups=mesh['z'=16,'yh'=2,'yl'=2,'x'=4,'c'=2] {'z'}, dimensions={0} | all-to-all | bytes 524288 | tf_op jit(solution)/shard_map/all_to_all | solution.py:39
  50.2 10.9 %all_to_all.37.mine = bf16[4,16,32,128]{3,2,1,0:T(8,128)(2,1)S(1)} all-to-all(bf16[4,16,32,128]{3,2,1,0:T(8,128)(2,1)S(1)} %broadcast_in_dim.4), channel_id=1, replica_groups=mesh['z'=16,'yh'=2,'yl'=2,'x'=4,'c'=2] {'x'}, dimensions={0} | all-to-all | bytes 1048576 | tf_op jit(solution)/shard_map/all_to_all | solution.py:35
  61.1 12.8 %collective-permute-start.3 = (bf16[4,16,32,128]{3,2,1,0:T(8,128)(2,1)S(1)}, bf16[4,16,32,128]{3,2,1,0:T(8,128)(2,1)S(1)}, u32[]{:S(2)}, u32[]{:S(2)}) collective-permute-start(bf16[4,16,32,128]{3,2,1,0:T(8,128)(2,1)S(1)} %all_to_all.37.mine), channel_id=1, source_target_pairs={{0,1},{1,0},{2,3},{3,2},{4,5},{5,4},{6,7},{7,6},{8,9},{9,8},{10,11... | collective-permute-start | bytes 1572872 | tf_op jit(solution)/shard_map/ppermute | solution.py:43
  73.9 1.9 %collective-permute-start.5 = (bf16[128,2048]{1,0:T(8,128)(2,1)}, bf16[128,2048]{1,0:T(8,128)(2,1)S(1)}, u32[]{:S(2)}, u32[]{:S(2)}) collective-permute-start(bf16[128,2048]{1,0:T(8,128)(2,1)} %own_l.1), channel_id=1, source_target_pairs={{0,1},{1,0},{2,3},{3,2},{4,5},{5,4},{6,7},{7,6},{8,9},{9,8},{10,11... | collective-permute-start | bytes 1572872 | tf_op jit(solution)/shard_map/ppermute | solution.py:43
  75.9 2.3 %collective-permute-start.2 = (bf16[128,256]{1,0:T(8,128)(2,1)S(1)}, bf16[128,256]{1,0:T(8,128)(2,1)S(1)}, u32[]{:S(2)}, u32[]{:S(2)}) collective-permute-start(bf16[128,256]{1,0:T(8,128)(2,1)S(1)} %get-tuple-element.9.refs_0_), channel_id=1, source_target_pairs={{0,24},{8,0},{16,8},{24,16},{1,25},{9,1},{17,9},{25,17},{2,26},{10... | collective-permute-start | bytes 196616 | tf_op jit(solution)/shard_map/ppermute | solution.py:384
  78.2 3.1 %collective-permute-start.1 = (bf16[128,256]{1,0:T(8,128)(2,1)S(1)}, bf16[128,256]{1,0:T(8,128)(2,1)S(1)}, u32[]{:S(2)}, u32[]{:S(2)}) collective-permute-start(bf16[128,256]{1,0:T(8,128)(2,1)S(1)} %get-tuple-element.9.refs_0_), channel_id=1, source_target_pairs={{0,16},{8,24},{16,0},{24,8},{1,17},{9,25},{17,1},{25,9},{2,18},{10... | collective-permute-start | bytes 196616 | tf_op jit(solution)/shard_map/ppermute | solution.py:384
  81.3 1.9 %collective-permute-start = (bf16[128,256]{1,0:T(8,128)(2,1)S(1)}, bf16[128,256]{1,0:T(8,128)(2,1)S(1)}, u32[]{:S(2)}, u32[]{:S(2)}) collective-permute-start(bf16[128,256]{1,0:T(8,128)(2,1)S(1)} %get-tuple-element.9.refs_0_), channel_id=1, source_target_pairs={{0,8},{8,16},{16,24},{24,0},{1,9},{9,17},{17,25},{25,1},{2,10},{10... | collective-permute-start | bytes 196616 | tf_op jit(solution)/shard_map/ppermute | solution.py:384
  83.2 3.0 %collective-permute-start.4 = (bf16[64,2048]{1,0:T(8,128)(2,1)}, bf16[64,2048]{1,0:T(8,128)(2,1)S(1)}, u32[]{:S(2)}, u32[]{:S(2)}) collective-permute-start(bf16[64,2048]{1,0:T(8,128)(2,1)} %own_s.1), channel_id=1, source_target_pairs={{0,1},{1,0},{2,3},{3,2},{4,5},{5,4},{6,7},{7,6},{8,9},{9,8},{10,11... | collective-permute-start | bytes 786440 | tf_op jit(solution)/shard_map/ppermute | solution.py:43
  86.2 1.7 %collective-permute-done.refs_1_ = bf16[128,256]{1,0:T(8,128)(2,1)S(1)} collective-permute-done((bf16[128,256]{1,0:T(8,128)(2,1)S(1)}, bf16[128,256]{1,0:T(8,128)(2,1)S(1)}, u32[]{:S(2)}, u32[]{:S(2)}) %collective-permute-start) | collective-permute-done | bytes 65568 | tf_op jit(solution)/shard_map/ppermute | solution.py:384
  89.8 7.6 %attend.1 = bf16[8,64,256]{2,1,0:T(8,128)(2,1)} custom-call(s32[1]{0:T(128)} %bitcast.place, bf16[4,2,128,512]{3,2,1,0:T(8,128)(2,1)S(1)} %absorb.1.query, bf16[4,16,32,128]{3,2,1,0:T(8,128)(2,1)S(1)} %all_to_all.37.mine, bf16[4,16,32,128]{3,2,1,0:T(8,128)(2,1)S(1)} %collective-permute-done.3.other, bf16[16,64,128]{2,1,0:T(8,128)(2,1)S(1)} %all_to_all.36.ropes, ...), custom_call_target="tpu_custom_call" | custom-call | tf_op jit(solution)/shard_map/attend/pallas_call | solution.py:231
  97.5 5.1 %all-to-all-start.2 = ((bf16[8,64,256]{2,1,0:T(8,128)(2,1)}), bf16[8,64,256]{2,1,0:T(8,128)(2,1)S(1)}, u32[]{:S(2)}, u32[]{:S(2)}) async-start(bf16[8,64,256]{2,1,0:T(8,128)(2,1)} %attend.1), calls=%async_computation.2 | async-start | bytes 524288 | tf_op jit(solution)/shard_map/all_to_all | solution.py:39
  102.6 6.5 %all-to-all-done.2.parts = bf16[8,64,256]{2,1,0:T(8,128)(2,1)S(1)} async-done(((bf16[8,64,256]{2,1,0:T(8,128)(2,1)}), bf16[8,64,256]{2,1,0:T(8,128)(2,1)S(1)}, u32[]{:S(2)}, u32[]{:S(2)}) %all-to-all-start.2) | async-done | bytes 262176 | tf_op jit(solution)/shard_map/all_to_all | solution.py:39
  109.1 1.5 merge.1
  110.6 3.4 %all-to-all-start.3 = ((bf16[4,16,2048]{2,1,0:T(8,128)(2,1)}), bf16[4,16,2048]{2,1,0:T(8,128)(2,1)S(1)}, u32[]{:S(2)}, u32[]{:S(2)}) async-start(bf16[4,16,2048]{2,1,0:T(8,128)(2,1)} %bitcast.6), calls=%async_computation.3 | async-start | bytes 524288 | tf_op jit(solution)/shard_map/all_to_all | solution.py:39
  114.1 5.5 %all-to-all-done.3 = bf16[4,16,2048]{2,1,0:T(8,128)(2,1)S(1)} async-done(((bf16[4,16,2048]{2,1,0:T(8,128)(2,1)}), bf16[4,16,2048]{2,1,0:T(8,128)(2,1)S(1)}, u32[]{:S(2)}, u32[]{:S(2)}) %all-to-all-start.3) | async-done | bytes 262176 | tf_op jit(solution)/shard_map/all_to_all | solution.py:39
  119.9 10.4 %all_to_all.38 = bf16[8,16,2048]{2,1,0:T(8,128)(2,1)S(1)} all-to-all(bf16[8,16,2048]{2,1,0:T(8,128)(2,1)S(1)} %broadcast_in_dim.5), channel_id=1, replica_groups=mesh['z'=16,'yh'=2,'yl'=2,'x'=4,'c'=2] {'yl','x'}, dimensions={0} | all-to-all | bytes 1048576 | tf_op jit(solution)/shard_map/all_to_all | solution.py:35
  130.3 5.0 %collective-permute-start.6 = (bf16[128,2048]{1,0:T(8,128)(2,1)S(1)}, bf16[128,2048]{1,0:T(8,128)(2,1)S(1)}, u32[]{:S(2)}, u32[]{:S(2)}) collective-permute-start(bf16[128,2048]{1,0:T(8,128)(2,1)S(1)} %bitcast.10), channel_id=1, source_target_pairs={{0,1},{1,0},{2,3},{3,2},{4,5},{5,4},{6,7},{7,6},{8,9},{9,8},{10,11... | collective-permute-start | bytes 1572872 | tf_op jit(solution)/shard_map/ppermute | solution.py:43
  135.3 2.4 %fetch.1.weights = bf16[2048,1152]{1,0:T(8,128)(2,1)S(1)} custom-call(bf16[2048,1152]{1,0:T(8,128)(2,1)} %all-gather.2.cloned.1.call-done.weights), custom_call_target="tpu_custom_call" | custom-call | tf_op jit(solution)/shard_map/fetch/pallas_call | solution.py:304
  137.7 1.3 shard_map.146
  139.0 1.9 %collective-permute-start.7 = (bf16[128,2048]{1,0:T(8,128)(2,1)S(1)}, bf16[128,2048]{1,0:T(8,128)(2,1)S(1)}, u32[]{:S(2)}, u32[]{:S(2)}) collective-permute-start(bf16[128,2048]{1,0:T(8,128)(2,1)S(1)} %shard_map.146), channel_id=1, source_target_pairs={{0,1},{1,0},{2,3},{3,2},{4,5},{5,4},{6,7},{7,6},{8,9},{9,8},{10,11... | collective-permute-start | bytes 1572872 | tf_op jit(solution)/shard_map/ppermute | solution.py:43
  140.9 1.3 shard_map.145
  142.9 12.6 %all_to_all.39 = bf16[8,16,2048]{2,1,0:T(8,128)(2,1)S(1)} all-to-all(bf16[8,16,2048]{2,1,0:T(8,128)(2,1)S(1)} %bitcast.17), channel_id=1, replica_groups=mesh['z'=16,'yh'=2,'yl'=2,'x'=4,'c'=2] {'yl','x'}, dimensions={0} | all-to-all | bytes 1048576 | tf_op jit(solution)/shard_map/all_to_all | solution.py:39
  (51 shorter events, 7.1 us)
Async XLA Ops:
  6.5 102.6 %copy-start = (bf16[128,2048]{1,0:T(8,128)(2,1)S(1)}, bf16[128,2048]{1,0:T(8,128)(2,1)}, u32[]{:S(2)}) copy-start(bf16[128,2048]{1,0:T(8,128)(2,1)} %own_l.1) | copy-start | bytes 1572868
  6.5 102.6 %copy-start.1 = (bf16[64,2048]{1,0:T(8,128)(2,1)S(1)}, bf16[64,2048]{1,0:T(8,128)(2,1)}, u32[]{:S(2)}) copy-start(bf16[64,2048]{1,0:T(8,128)(2,1)} %own_s.1) | copy-start | bytes 786436
  6.5 83.3 %copy-start.3 = (bf16[256,128]{1,0:T(8,128)(2,1)S(1)}, bf16[256,128]{1,0:T(8,128)(2,1)}, u32[]{:S(2)}) copy-start(bf16[256,128]{1,0:T(8,128)(2,1)} %value_up_l.1) | copy-start | bytes 196612
  6.5 83.3 %copy-start.6 = (bf16[256,64]{0,1:T(8,128)(2,1)S(1)}, bf16[256,64]{0,1:T(8,128)(2,1)}, u32[]{:S(2)}) copy-start(bf16[256,64]{0,1:T(8,128)(2,1)} %param.21) | copy-start | bytes 98308
  6.5 123.7 %all-gather.2.cloned.1.call-start = ((), (), s32[]{:S(2)}) async-start(), calls=%async_computation.7 | async-start | bytes 5013504 | tf_op jit(solution)/shard_map/all_gather | solution.py:362
  19.3 0.8 copy-start.4
  20.1 0.8 copy-start.5
  20.9 0.7 copy-start.8
  21.7 0.7 copy-start.9
  50.1 63.9 %copy-start.11 = (bf16[2048]{0:T(1024)(128)(2,1)S(1)}, bf16[2048]{0:T(1024)(128)(2,1)}, u32[]{:S(2)}) copy-start(bf16[2048]{0:T(1024)(128)(2,1)} %param.26) | copy-start | bytes 12292
  50.2 69.4 %copy-start.10 = (bf16[16,2048]{1,0:T(8,128)(2,1)S(1)}, bf16[16,2048]{1,0:T(8,128)(2,1)}, u32[]{:S(2)}) copy-start(bf16[16,2048]{1,0:T(8,128)(2,1)} %param.15) | copy-start | bytes 196612
  61.1 28.7 %collective-permute-start.3 = (bf16[4,16,32,128]{3,2,1,0:T(8,128)(2,1)S(1)}, bf16[4,16,32,128]{3,2,1,0:T(8,128)(2,1)S(1)}, u32[]{:S(2)}, u32[]{:S(2)}) collective-permute-start(bf16[4,16,32,128]{3,2,1,0:T(8,128)(2,1)S(1)} %all_to_all.37.mine), channel_id=1, source_target_pairs={{0,1},{1,0},{2,3},{3,2},{4,5},{5,4},{6,7},{7,6},{8,9},{9,8},{10,11... | collective-permute-start | bytes 1572872 | tf_op jit(solution)/shard_map/ppermute | solution.py:43
  73.9 28.7 %collective-permute-start.5 = (bf16[128,2048]{1,0:T(8,128)(2,1)}, bf16[128,2048]{1,0:T(8,128)(2,1)S(1)}, u32[]{:S(2)}, u32[]{:S(2)}) collective-permute-start(bf16[128,2048]{1,0:T(8,128)(2,1)} %own_l.1), channel_id=1, source_target_pairs={{0,1},{1,0},{2,3},{3,2},{4,5},{5,4},{6,7},{7,6},{8,9},{9,8},{10,11... | collective-permute-start | bytes 1572872 | tf_op jit(solution)/shard_map/ppermute | solution.py:43
  75.9 7.3 %collective-permute-start.2 = (bf16[128,256]{1,0:T(8,128)(2,1)S(1)}, bf16[128,256]{1,0:T(8,128)(2,1)S(1)}, u32[]{:S(2)}, u32[]{:S(2)}) collective-permute-start(bf16[128,256]{1,0:T(8,128)(2,1)S(1)} %get-tuple-element.9.refs_0_), channel_id=1, source_target_pairs={{0,24},{8,0},{16,8},{24,16},{1,25},{9,1},{17,9},{25,17},{2,26},{10... | collective-permute-start | bytes 196616 | tf_op jit(solution)/shard_map/ppermute | solution.py:384
  78.2 8.0 %collective-permute-start.1 = (bf16[128,256]{1,0:T(8,128)(2,1)S(1)}, bf16[128,256]{1,0:T(8,128)(2,1)S(1)}, u32[]{:S(2)}, u32[]{:S(2)}) collective-permute-start(bf16[128,256]{1,0:T(8,128)(2,1)S(1)} %get-tuple-element.9.refs_0_), channel_id=1, source_target_pairs={{0,16},{8,24},{16,0},{24,8},{1,17},{9,25},{17,1},{25,9},{2,18},{10... | collective-permute-start | bytes 196616 | tf_op jit(solution)/shard_map/ppermute | solution.py:384
  81.3 6.6 %collective-permute-start = (bf16[128,256]{1,0:T(8,128)(2,1)S(1)}, bf16[128,256]{1,0:T(8,128)(2,1)S(1)}, u32[]{:S(2)}, u32[]{:S(2)}) collective-permute-start(bf16[128,256]{1,0:T(8,128)(2,1)S(1)} %get-tuple-element.9.refs_0_), channel_id=1, source_target_pairs={{0,8},{8,16},{16,24},{24,0},{1,9},{9,17},{17,25},{25,1},{2,10},{10... | collective-permute-start | bytes 196616 | tf_op jit(solution)/shard_map/ppermute | solution.py:384
  83.2 19.4 %collective-permute-start.4 = (bf16[64,2048]{1,0:T(8,128)(2,1)}, bf16[64,2048]{1,0:T(8,128)(2,1)S(1)}, u32[]{:S(2)}, u32[]{:S(2)}) collective-permute-start(bf16[64,2048]{1,0:T(8,128)(2,1)} %own_s.1), channel_id=1, source_target_pairs={{0,1},{1,0},{2,3},{3,2},{4,5},{5,4},{6,7},{7,6},{8,9},{9,8},{10,11... | collective-permute-start | bytes 786440 | tf_op jit(solution)/shard_map/ppermute | solution.py:43
  87.9 0.8 copy-start.2
  88.8 0.8 copy-start.7
  97.5 11.6 %all-to-all-start.2 = ((bf16[8,64,256]{2,1,0:T(8,128)(2,1)}), bf16[8,64,256]{2,1,0:T(8,128)(2,1)S(1)}, u32[]{:S(2)}, u32[]{:S(2)}) async-start(bf16[8,64,256]{2,1,0:T(8,128)(2,1)} %attend.1), calls=%async_computation.2 | async-start | bytes 524288 | tf_op jit(solution)/shard_map/all_to_all | solution.py:39
  110.6 8.9 %all-to-all-start.3 = ((bf16[4,16,2048]{2,1,0:T(8,128)(2,1)}), bf16[4,16,2048]{2,1,0:T(8,128)(2,1)S(1)}, u32[]{:S(2)}, u32[]{:S(2)}) async-start(bf16[4,16,2048]{2,1,0:T(8,128)(2,1)} %bitcast.6), calls=%async_computation.3 | async-start | bytes 524288 | tf_op jit(solution)/shard_map/all_to_all | solution.py:39
  130.3 7.4 %collective-permute-start.6 = (bf16[128,2048]{1,0:T(8,128)(2,1)S(1)}, bf16[128,2048]{1,0:T(8,128)(2,1)S(1)}, u32[]{:S(2)}, u32[]{:S(2)}) collective-permute-start(bf16[128,2048]{1,0:T(8,128)(2,1)S(1)} %bitcast.10), channel_id=1, source_target_pairs={{0,1},{1,0},{2,3},{3,2},{4,5},{5,4},{6,7},{7,6},{8,9},{9,8},{10,11... | collective-permute-start | bytes 1572872 | tf_op jit(solution)/shard_map/ppermute | solution.py:43
  139.0 3.8 %collective-permute-start.7 = (bf16[128,2048]{1,0:T(8,128)(2,1)S(1)}, bf16[128,2048]{1,0:T(8,128)(2,1)S(1)}, u32[]{:S(2)}, u32[]{:S(2)}) collective-permute-start(bf16[128,2048]{1,0:T(8,128)(2,1)S(1)} %shard_map.146), channel_id=1, source_target_pairs={{0,1},{1,0},{2,3},{3,2},{4,5},{5,4},{6,7},{7,6},{8,9},{9,8},{10,11... | collective-permute-start | bytes 1572872 | tf_op jit(solution)/shard_map/ppermute | solution.py:43
Sparse Core Ops, SparseCore 0:
  19.3 83.8 all-gather.1
